TPU v7x, 512 devices: a whole 4x8x8 slice. The times are simulated.
512 devices in a mesh: sp: 32 (over z, x), tp: 16 (over y, core).
Axes of the slice: x: 4, y: 8, z: 8, core: 2. Of those that a mesh axis runs over, the one named last changes fastest.
Arguments:
- layer_input: bfloat16 [32, 6144, 2048], P('sp', 'tp'), may hold values from -6 to 6
- input_gain: float32 [2048], replicated, may hold values from 0.1 to 1.9
- key_weight: bfloat16 [2048, 512], P('sp', 'tp'), may hold values from -0.125 to 0.125
- value_weight: bfloat16 [2048, 512], P('sp', 'tp'), may hold values from -0.125 to 0.125
- key_gain: float32 [128], replicated, may hold values from 0.1 to 1.9
- stop_shift: bfloat16 [32, 4, 6144], P('sp', None, 'tp'), may hold values from -20 to 0
- new_query: bfloat16 [32, 16, 128], P('sp', 'tp'), may hold values from -6 to 6
- query_gain: float32 [128], replicated, may hold values from 0.1 to 1.9
- out_gain: float32 [128], replicated, may hold values from 0.1 to 1.9
Outputs:
- key_cache: bfloat16 [32, 16, 6144, 128], P('sp', 'tp')
- value_cache: bfloat16 [32, 16, 6144, 128], P('sp', 'tp')
- shift_cache: bfloat16 [32, 16, 6144], P('sp', 'tp')
- first_read: bfloat16 [32, 16, 128], P('sp', 'tp')
All inputs are finite; a program needn't handle non-finite values.
Results may differ from a plain program's by a relative error of at most 0.013.
Values may be sent and summed in bfloat16 or wider, within the bound.
No kernel may reach another device: no remote copies, remote signals or barrier semaphores. Data moves between devices by JAX's collectives and lax.ppermute only.
A program may use at most 64 MiB of HBM per device.

v0:
```python
import jax
import jax.numpy as jnp
from jax import lax
from jax.sharding import PartitionSpec as P

KVH = 4


epsilon = 1e-06


def joined_along(tiles, dim):
    tiles = jnp.moveaxis(tiles, 0, dim)
    dims = tiles.shape
    return tiles.reshape(*dims[:dim], dims[dim] * dims[dim + 1], *dims[dim + 2 :])


def sent_to_all(x, axis):
    copies = jnp.broadcast_to(x, (lax.axis_size(axis), *x.shape))
    return lax.all_to_all(copies, axis, split_axis=0, concat_axis=0, tiled=True)


def collect(x, axis, dim):
    return joined_along(sent_to_all(x, axis), dim)


def in_one_piece(arrays, axis, split_dim, concat_dim, along):
    columns = [a.reshape(*a.shape[:along], -1) for a in arrays]
    both = jnp.concatenate(columns, axis=along)
    out, at, outs = (
        lax.all_to_all(both, axis, split_axis=split_dim, concat_axis=concat_dim, tiled=True),
        0,
        [],
    )
    for a, column in zip(arrays, columns):
        section = out[..., at : at + column.shape[along]]
        outs.append(section.reshape(*section.shape[:along], *a.shape[along:]))
        at += column.shape[along]
    return tuple(outs)


def as_sent(x):

    def short(part):
        return part.astype(jnp.bfloat16) if part.dtype == jnp.float32 else part

    return jax.tree.map(short, x)


def partner_2(x, axis, distance):
    return lax.ppermute(x, axis, [(i, i ^ 1 << distance) for i in range(lax.axis_size(axis))])


def row_norm(value_entries, scaling):
    return (
        value_entries
        * lax.rsqrt(jnp.mean(value_entries * value_entries, axis=-1, keepdims=True) + epsilon)
        * scaling
    )


def shards(
    layer_input,
    input_gain,
    key_weight,
    value_weight,
    key_gain,
    stop_shift,
    new_query,
    query_gain,
    out_gain,
):
    groups = lax.axis_size("tp")
    copies = groups // KVH
    row_count = layer_input.shape[1]
    head_size = new_query.shape[2]
    score_scale = 1.0 / head_size**0.5
    normed = row_norm(layer_input[0].astype(jnp.float32), input_gain).astype(jnp.bfloat16)
    stacked = jnp.stack((key_weight, value_weight), 0)
    full_depth = collect(stacked, "sp", 1)
    projected = jnp.einsum(
        "rd,kdc->krc",
        normed,
        lax.all_gather(full_depth, "tp", axis=2, tiled=True),
        preferred_element_type=jnp.float32,
    )
    key_rows = row_norm(projected[0].reshape(row_count, KVH, head_size), key_gain).astype(
        jnp.bfloat16
    )
    value_rows = projected[1].reshape(row_count, KVH, head_size).astype(jnp.bfloat16)
    local_shift = stop_shift[0]
    share = row_count // copies
    key_pieces = (
        key_rows.reshape(copies, share, KVH, head_size)
        .transpose(2, 0, 1, 3)
        .reshape(groups, share, head_size)
    )
    value_parts = (
        value_rows.reshape(copies, share, KVH, head_size)
        .transpose(2, 0, 1, 3)
        .reshape(groups, share, head_size)
    )
    shift_parts = local_shift.reshape(KVH, copies, share).reshape(groups, share)
    key_got, value_got, shift_got = in_one_piece(
        (key_pieces, value_parts, shift_parts), "tp", 0, 0, 2
    )
    held = (key_got[None], value_got[None], shift_got[None])
    position = lax.axis_index("tp")
    for bit in range(copies.bit_length() - 1):
        partner = jax.tree.map(
            lambda part, own: part.astype(own.dtype), partner_2(as_sent(held), "tp", bit), held
        )
        upper = position >> bit & 1 == 1
        held = tuple(
            (
                jnp.where(
                    upper, jnp.concatenate((theirs, mine), 0), jnp.concatenate((mine, theirs), 0)
                )
                for mine, theirs in zip(held, partner)
            )
        )
    key_line = held[0].transpose(1, 0, 2, 3).reshape(groups * row_count, head_size)
    value_line = held[1].transpose(1, 0, 2, 3).reshape(groups * row_count, head_size)
    shift_line = held[2].transpose(1, 0, 2).reshape(groups * row_count)
    length = key_line.shape[0]
    query_rows = row_norm(new_query[0].astype(jnp.float32), query_gain).astype(jnp.bfloat16)
    scores = (
        jnp.einsum("qd,ld->ql", query_rows, key_line, preferred_element_type=jnp.float32)
        * score_scale
    )
    scores = scores + shift_line.astype(jnp.float32)[None, :]
    log_keep = jax.nn.log_sigmoid(-scores)
    inside = lax.cumsum(log_keep, axis=1, reverse=True) - log_keep
    weights = jnp.exp(jax.nn.log_sigmoid(scores) + inside).astype(jnp.bfloat16)
    read_sum = jnp.dot(weights, value_line, preferred_element_type=jnp.float32)
    first_out = row_norm(read_sum, out_gain).astype(jnp.bfloat16)
    return (
        key_line.reshape(1, 1, length, head_size),
        value_line.reshape(1, 1, length, head_size),
        shift_line.reshape(1, 1, length),
        first_out[None],
    )


def solution(mesh):
    placed = (
        P("sp", "tp", None),
        P(),
        P("sp", "tp"),
        P("sp", "tp"),
        P(),
        P("sp", None, "tp"),
        P("sp", "tp", None),
        P(),
        P(),
    )
    return jax.shard_map(
        shards,
        mesh=mesh,
        in_specs=placed,
        out_specs=(
            P("sp", "tp", None, None),
            P("sp", "tp", None, None),
            P("sp", "tp", None),
            P("sp", "tp", None),
        ),
        check_vma=False,
    )
```

profile of v0, /device:TPU:1, one launch (start us, length us, event | category | flops | bytes accessed | tf_op | source)
XLA Modules:
  0.0 176.8 jit_solution(10606632775169427298)
XLA Ops:
  7.2 0.7 pad_maximum_fusion.1
  8.4 24.8 %all_to_all.10 = bf16[32,2,2048]{2,1,0:T(2,128)(2,1)S(1)} all-to-all(bf16[32,2,2048]{2,1,0:T(2,128)(2,1)S(1)} %reshape.183), channel_id=1, replica_groups=mesh['sp'=32,'tp'=16] {'sp'}, dimensions={0} | all-to-all | bytes 524288 | tf_op jit(solution)/shard_map/all_to_all | solution.py:20
  34.0 1.2 reshape.165
  35.3 0.7 reshape_reshape_reshape_squeeze.4
  36.4 41.1 %all-gather.2.cloned.1.call-done = bf16[2,2048,512]{1,2,0:T(8,128)(2,1)} async-done(((bf16[2,2048,32]{1,2,0:T(8,128)(2,1)}), bf16[2,2048,512]{1,2,0:T(8,128)(2,1)}) %all-gather.2.cloned.1.call-update) | async-done | bytes 4194320 | tf_op jit(solution)/shard_map/all_gather | solution.py:84
  77.4 4.6 %fusion.9 = f32[2,384,512]{1,2,0:T(8,128)S(1)} fusion(bf16[2,2048,512]{1,2,0:T(8,128)(2,1)} %all-gather.2.cloned.1.call-done, bf16[1,384,2048]{2,1,0:T(8,128)(2,1)S(1)} %copy-done.3, f32[2048]{0:T(1024)S(1)} %copy-done.10, f32[384]{0:T(512)S(1)} %add_rsqrt_fusion.1), kind=kOutput, calls=%fused_computation.12 | convolution fusion | flops 1613758464 | bytes 7349760 | tf_op jit(solution)/shard_map/rd,kdc->krc/dot_general | solution.py:81
  84.2 0.8 copy.39
  85.1 33.9 %all_to_all.11 = bf16[16,96,257]{1,2,0:T(8,128)(2,1)S(1)} all-to-all(bf16[16,96,257]{1,2,0:T(8,128)(2,1)S(1)} %copy.39), channel_id=1, replica_groups=mesh['sp'=32,'tp'=16] {'tp'}, dimensions={0} | all-to-all | bytes 1579008 | tf_op jit(solution)/shard_map/all_to_all | solution.py:31
  119.3 2.3 %collective-permute-start = (bf16[1,16,96,128]{3,2,0,1:T(8,128)(2,1)S(1)}, bf16[1,16,96,128]{3,2,0,1:T(8,128)(2,1)S(1)}, u32[]{:S(2)}, u32[]{:S(2)}) collective-permute-start(bf16[1,16,96,128]{3,2,0,1:T(8,128)(2,1)S(1)} %bitcast.90), channel_id=1, source_target_pairs={{0,1},{1,0},{2,3},{3,2},{4,5},{5,4},{6,7},{7,6},{8,9},{9,8},{10,11... | collective-permute-start | bytes 1179656 | tf_op jit(solution)/shard_map/ppermute | solution.py:51
  121.6 1.3 collective-permute-done
  123.0 2.3 %collective-permute-start.1 = (bf16[2,16,96,128]{3,2,0,1:T(8,128)(2,1)S(1)}, bf16[2,16,96,128]{3,2,0,1:T(8,128)(2,1)}, u32[]{:S(2)}, u32[]{:S(2)}) collective-permute-start(bf16[2,16,96,128]{3,2,0,1:T(8,128)(2,1)S(1)} %maximum_select_fusion.2), channel_id=1, source_target_pairs={{0,2},{1,3},{2,0},{3,1},{4,6},{5,7},{6,4},{7,5},{8,10},{9,11},{10,... | collective-permute-start | bytes 2359304 | tf_op jit(solution)/shard_map/ppermute | solution.py:51
  125.6 2.6 %collective-permute-start.2 = (bf16[1,16,96,128]{3,2,0,1:T(8,128)(2,1)S(1)}, bf16[1,16,96,128]{3,2,0,1:T(8,128)(2,1)S(1)}, u32[]{:S(2)}, u32[]{:S(2)}) collective-permute-start(bf16[1,16,96,128]{3,2,0,1:T(8,128)(2,1)S(1)} %bitcast.88), channel_id=1, source_target_pairs={{0,1},{1,0},{2,3},{3,2},{4,5},{5,4},{6,7},{7,6},{8,9},{9,8},{10,11... | collective-permute-start | bytes 1179656 | tf_op jit(solution)/shard_map/ppermute | solution.py:51
  128.2 1.9 %collective-permute-start.4 = (bf16[1,16,96]{2,1,0:T(8,128)(2,1)S(1)}, bf16[1,16,96]{2,1,0:T(8,128)(2,1)S(1)}, u32[]{:S(2)}, u32[]{:S(2)}) collective-permute-start(bf16[1,16,96]{2,1,0:T(8,128)(2,1)S(1)} %bitcast.99), channel_id=1, source_target_pairs={{0,1},{1,0},{2,3},{3,2},{4,5},{5,4},{6,7},{7,6},{8,9},{9,8},{10,11... | collective-permute-start | bytes 9224 | tf_op jit(solution)/shard_map/ppermute | solution.py:51
  130.1 1.1 collective-permute-done.4
  131.3 2.9 %collective-permute-start.5 = (bf16[2,16,96]{2,1,0:T(8,128)(2,1)S(1)}, bf16[2,16,96]{2,1,0:T(8,128)(2,1)S(1)}, u32[]{:S(2)}, u32[]{:S(2)}) collective-permute-start(bf16[2,16,96]{2,1,0:T(8,128)(2,1)S(1)} %maximum_select_fusion.5), channel_id=1, source_target_pairs={{0,2},{1,3},{2,0},{3,1},{4,6},{5,7},{6,4},{7,5},{8,10},{9,11},{10,... | collective-permute-start | bytes 18440 | tf_op jit(solution)/shard_map/ppermute | solution.py:51
  135.5 8.4 %collective-permute-done.5 = bf16[2,16,96]{2,1,0:T(8,128)(2,1)S(1)} collective-permute-done((bf16[2,16,96]{2,1,0:T(8,128)(2,1)S(1)}, bf16[2,16,96]{2,1,0:T(8,128)(2,1)S(1)}, u32[]{:S(2)}, u32[]{:S(2)}) %collective-permute-start.5) | collective-permute-done | bytes 6176 | tf_op jit(solution)/shard_map/ppermute | solution.py:51
  144.0 0.7 reshape.176
  144.7 0.7 reshape_reshape.11
  145.5 2.5 %collective-permute-start.3 = (bf16[2,16,96,128]{3,2,0,1:T(8,128)(2,1)S(1)}, bf16[2,16,96,128]{3,2,0,1:T(8,128)(2,1)}, u32[]{:S(2)}, u32[]{:S(2)}) collective-permute-start(bf16[2,16,96,128]{3,2,0,1:T(8,128)(2,1)S(1)} %maximum_select_fusion.3), channel_id=1, source_target_pairs={{0,2},{1,3},{2,0},{3,1},{4,6},{5,7},{6,4},{7,5},{8,10},{9,11},{10,... | collective-permute-start | bytes 2359304 | tf_op jit(solution)/shard_map/ppermute | solution.py:51
  147.9 1.6 maximum_select_fusion
  150.3 1.2 reduce-window.6
  152.3 13.3 %collective-permute-done.3 = bf16[2,16,96,128]{3,2,0,1:T(8,128)(2,1)} collective-permute-done((bf16[2,16,96,128]{3,2,0,1:T(8,128)(2,1)S(1)}, bf16[2,16,96,128]{3,2,0,1:T(8,128)(2,1)}, u32[]{:S(2)}, u32[]{:S(2)}) %collective-permute-start.3) | collective-permute-done | bytes 786464 | tf_op jit(solution)/shard_map/ppermute | solution.py:51
  165.6 2.1 %maximum_select_fusion.1 = bf16[4,16,96,128]{3,2,0,1:T(8,128)(2,1)S(1)} fusion(bf16[2,16,96,128]{3,2,0,1:T(8,128)(2,1)} %copy-done.2, bf16[2,16,96,128]{3,2,0,1:T(8,128)(2,1)} %collective-permute-done.3, pred[]{:T(512)S(6)} %eq.6), kind=kLoop, calls=%fused_computation.8 | loop fusion | flops 2359296 | bytes 3145729 | tf_op jit(solution)/shard_map/jit(_where)/select_n | solution.py:116
  167.7 1.0 multiply_reduce_fusion
  (67 shorter events, 7.2 us)
Async XLA Ops:
  7.2 70.3 %all-gather.2.cloned.1.call-start = ((), (), s32[]{:S(2)}) async-start(), calls=%async_computation.2 | async-start | bytes 4456448 | tf_op jit(solution)/shard_map/all_gather | solution.py:84
  33.6 1.6 copy-start.5
  33.6 2.3 %copy-start.3 = (bf16[1,384,2048]{2,1,0:T(8,128)(2,1)S(1)}, bf16[1,384,2048]{2,1,0:T(8,128)(2,1)}, u32[]{:S(2)}) copy-start(bf16[1,384,2048]{2,1,0:T(8,128)(2,1)} %param.9) | copy-start | bytes 4718596
  34.0 43.4 %copy-start.10 = (f32[2048]{0:T(1024)S(1)}, f32[2048]{0:T(1024)}, u32[]{:S(2)}) copy-start(f32[2048]{0:T(1024)} %param.10) | copy-start | bytes 24580
  82.5 0.7 copy-start.6
  119.0 15.2 %copy-start.8 = (bf16[1,1,128]{2,1,0:T(2,128)(2,1)S(1)}, bf16[1,1,128]{2,1,0:T(2,128)(2,1)}, u32[]{:S(2)}) copy-start(bf16[1,1,128]{2,1,0:T(2,128)(2,1)} %param.15) | copy-start | bytes 772
  119.3 3.6 %collective-permute-start = (bf16[1,16,96,128]{3,2,0,1:T(8,128)(2,1)S(1)}, bf16[1,16,96,128]{3,2,0,1:T(8,128)(2,1)S(1)}, u32[]{:S(2)}, u32[]{:S(2)}) collective-permute-start(bf16[1,16,96,128]{3,2,0,1:T(8,128)(2,1)S(1)} %bitcast.90), channel_id=1, source_target_pairs={{0,1},{1,0},{2,3},{3,2},{4,5},{5,4},{6,7},{7,6},{8,9},{9,8},{10,11... | collective-permute-start | bytes 1179656 | tf_op jit(solution)/shard_map/ppermute | solution.py:51
  123.0 24.9 %collective-permute-start.1 = (bf16[2,16,96,128]{3,2,0,1:T(8,128)(2,1)S(1)}, bf16[2,16,96,128]{3,2,0,1:T(8,128)(2,1)}, u32[]{:S(2)}, u32[]{:S(2)}) collective-permute-start(bf16[2,16,96,128]{3,2,0,1:T(8,128)(2,1)S(1)} %maximum_select_fusion.2), channel_id=1, source_target_pairs={{0,2},{1,3},{2,0},{3,1},{4,6},{5,7},{6,4},{7,5},{8,10},{9,11},{10,... | collective-permute-start | bytes 2359304 | tf_op jit(solution)/shard_map/ppermute | solution.py:51
  125.6 19.8 %collective-permute-start.2 = (bf16[1,16,96,128]{3,2,0,1:T(8,128)(2,1)S(1)}, bf16[1,16,96,128]{3,2,0,1:T(8,128)(2,1)S(1)}, u32[]{:S(2)}, u32[]{:S(2)}) collective-permute-start(bf16[1,16,96,128]{3,2,0,1:T(8,128)(2,1)S(1)} %bitcast.88), channel_id=1, source_target_pairs={{0,1},{1,0},{2,3},{3,2},{4,5},{5,4},{6,7},{7,6},{8,9},{9,8},{10,11... | collective-permute-start | bytes 1179656 | tf_op jit(solution)/shard_map/ppermute | solution.py:51
  128.2 3.1 %collective-permute-start.4 = (bf16[1,16,96]{2,1,0:T(8,128)(2,1)S(1)}, bf16[1,16,96]{2,1,0:T(8,128)(2,1)S(1)}, u32[]{:S(2)}, u32[]{:S(2)}) collective-permute-start(bf16[1,16,96]{2,1,0:T(8,128)(2,1)S(1)} %bitcast.99), channel_id=1, source_target_pairs={{0,1},{1,0},{2,3},{3,2},{4,5},{5,4},{6,7},{7,6},{8,9},{9,8},{10,11... | collective-permute-start | bytes 9224 | tf_op jit(solution)/shard_map/ppermute | solution.py:51
  131.3 12.7 %collective-permute-start.5 = (bf16[2,16,96]{2,1,0:T(8,128)(2,1)S(1)}, bf16[2,16,96]{2,1,0:T(8,128)(2,1)S(1)}, u32[]{:S(2)}, u32[]{:S(2)}) collective-permute-start(bf16[2,16,96]{2,1,0:T(8,128)(2,1)S(1)} %maximum_select_fusion.5), channel_id=1, source_target_pairs={{0,2},{1,3},{2,0},{3,1},{4,6},{5,7},{6,4},{7,5},{8,10},{9,11},{10,... | collective-permute-start | bytes 18440 | tf_op jit(solution)/shard_map/ppermute | solution.py:51
  145.4 6.9 %copy-start.2 = (bf16[2,16,96,128]{3,2,0,1:T(8,128)(2,1)}, bf16[2,16,96,128]{3,2,0,1:T(8,128)(2,1)S(1)}, u32[]{:S(2)}) copy-start(bf16[2,16,96,128]{3,2,0,1:T(8,128)(2,1)S(1)} %maximum_select_fusion.3) | copy-start | bytes 2359300
  145.5 4.1 %copy-start.7 = (f32[128]{0:T(128)S(1)}, f32[128]{0:T(128)}, u32[]{:S(2)}) copy-start(f32[128]{0:T(128)} %param.16) | copy-start | bytes 1540
  145.5 20.1 %collective-permute-start.3 = (bf16[2,16,96,128]{3,2,0,1:T(8,128)(2,1)S(1)}, bf16[2,16,96,128]{3,2,0,1:T(8,128)(2,1)}, u32[]{:S(2)}, u32[]{:S(2)}) collective-permute-start(bf16[2,16,96,128]{3,2,0,1:T(8,128)(2,1)S(1)} %maximum_select_fusion.3), channel_id=1, source_target_pairs={{0,2},{1,3},{2,0},{3,1},{4,6},{5,7},{6,4},{7,5},{8,10},{9,11},{10,... | collective-permute-start | bytes 2359304 | tf_op jit(solution)/shard_map/ppermute | solution.py:51
  149.5 18.2 %copy-start = (bf16[4,16,96,128]{3,2,0,1:T(8,128)(2,1)}, bf16[4,16,96,128]{3,2,0,1:T(8,128)(2,1)S(1)}, u32[]{:S(2)}) copy-start(bf16[4,16,96,128]{3,2,0,1:T(8,128)(2,1)S(1)} %maximum_select_fusion) | copy-start | bytes 4718596
  149.5 0.8 copy-start.4
  167.7 2.3 %copy-start.1 = (bf16[4,16,96,128]{3,2,0,1:T(8,128)(2,1)}, bf16[4,16,96,128]{3,2,0,1:T(8,128)(2,1)S(1)}, u32[]{:S(2)}) copy-start(bf16[4,16,96,128]{3,2,0,1:T(8,128)(2,1)S(1)} %maximum_select_fusion.1) | copy-start | bytes 4718596
  167.7 1.7 copy-start.9
Sparse Core Ops, SparseCore 0:
  35.4 42.0 all-gather.1
where the time goes:
time: 178 us; the launch traced here: 177 us
  waiting for transfers between devices  65.2 us (37%)
  blocking collectives  58.7 us (33%)
  between operations  15.9 us (9%)
  starting transfers between devices  14.6 us (8%)
  other arithmetic  8.59 us (5%)
  local copies, waits for them, and re-layouts  7.83 us (4%)
  matrix products  6.12 us (3%)
    all_gather x1, waiting for transfers between devices, shards(): lax.all_gather(full_depth, 'tp', axis=2, tiled=True)  41.1 us
    all_to_all x1, blocking collectives, in_one_piece(): lax.all_to_all(both, axis, split_axis=split_dim, concat_axis=concat_dim,...  33.9 us
    all_to_all x1, blocking collectives, sent_to_all(): return lax.all_to_all(copies, axis, split_axis=0, concat_axis=0, tiled=True)  24.8 us
    ppermute x6, waiting for transfers between devices, partner_2(): lax.ppermute(x, axis, [(i, i ^ 1 << distance) for i in range(lax.axis_siz...  24.1 us
    ppermute x6, starting transfers between devices, partner_2(): lax.ppermute(x, axis, [(i, i ^ 1 << distance) for i in range(lax.axis_siz...  14.5 us
    dot_general x1, matrix products, shards(): jnp.einsum('rd,kdc->krc', normed, lax.all_gather(full_depth, 'tp', axis=2...  4.61 us
    select_n x5, other arithmetic, shards(): jnp.where(upper, jnp.concatenate((theirs, mine), 0), jnp.concatenate((min...  3.88 us
  transfers between devices with their start and end apart: 7, of which 5 were waited for; matrix products, arithmetic and copies ran while one was open for 4% of the time, Pallas kernels for 0%

commit v1 on v0

v1 whole, which is shorter than its diff:
```python
import jax
import jax.numpy as jnp
from jax import lax
from jax.experimental import pallas as pl
from jax.experimental.pallas import tpu as pltpu
from jax.sharding import PartitionSpec as P

KVH = 4
NX = 4
epsilon = 1e-06


def row_norm(value_entries, scaling):
    return (
        value_entries
        * lax.rsqrt(jnp.mean(value_entries * value_entries, axis=-1, keepdims=True) + epsilon)
        * scaling
    )


def moved_sp(x, dz, dx):
    n = lax.axis_size("sp")
    nz = n // NX
    pairs = []
    for i in range(n):
        z, c = (i // NX + dz) % nz, (i % NX + dx) % NX
        pairs.append((i, z * NX + c))
    return lax.ppermute(x, "sp", pairs)


def moved_y(x, target):
    n = lax.axis_size("tp")
    return lax.ppermute(x, "tp", [(i, target(i // 2) % (n // 2) * 2 + i % 2) for i in range(n)])


def swapped(x):
    return lax.ppermute(x, "tp", [(i, i ^ 1) for i in range(lax.axis_size("tp"))])


def step_to(distance):
    sign = -1 if distance % 2 else 1
    return lambda y: y + sign * distance if y % 2 == 0 else y - sign * distance


def packed(w):
    rows, cols = w.shape
    n = 128 // cols
    return w.reshape(n, rows // n, cols).transpose(1, 0, 2).reshape(rows // n, 128)


def build_body(recv, whole, low, high, *, blocks):
    lane = lax.broadcasted_iota(jnp.int32, (16 * blocks, 128), 1) // 32
    half = blocks // 2
    for head in range(KVH):
        parts = [recv[4 * head + t, : 16 * blocks, :].astype(jnp.float32) for t in range(4)]
        for q in range(4):
            out = None
            for t in range(4):
                shift = 32 * ((t - q) % 4)
                turned = pltpu.roll(parts[t], shift, 1) if shift else parts[t]
                out = turned if out is None else jnp.where(lane == t, turned, out)
            out = out.astype(jnp.bfloat16).reshape(blocks, 16, 128)
            cols = slice(128 * head, 128 * head + 128)
            whole[:, q, :, cols] = out
            low[:, q, :, cols] = out[:half]
            high[:, q, :, cols] = out[half:]


def project_body(meta, own, other, w0, wl, wr, wu, wd, gain, *rest):
    outs, wide, line = rest[:4], rest[4], rest[5]
    cls, core = meta[0], meta[1]

    def put(ref, c, at, first, count):
        for b in range(count):
            x = lax.rem(c + 2 * ((first + b) % 2), NX)
            to = pl.multiple_of(256 * (first + b) + 64 * x, 64)
            wide[pl.ds(to, 64), :] = ref[64 * (at + b) : 64 * (at + b) + 64, :]

    put(w0, cls, 0, 0, 8)
    put(wl, lax.rem(cls + 3, NX), 0, 0, 8)
    put(wr, lax.rem(cls + 1, NX), 0, 0, 8)
    put(wu, lax.rem(cls + 2, NX), 0, 0, 4)
    put(wd, lax.rem(cls + 2, NX), 0, 4, 4)
    rows = own.shape[0]
    is_key = core == 0
    for ref, place in ((own, core), (other, 1 - core)):
        acc = jnp.dot(ref[...], wide[...], preferred_element_type=jnp.float32)
        to = pl.multiple_of(place * rows, 128)
        for head in range(KVH):
            a = acc[:, 128 * head : 128 * head + 128]
            normed = row_norm(a, gain[...])
            line[pl.ds(to, rows), 128 * head : 128 * head + 128] = jnp.where(
                is_key, normed, a
            ).astype(jnp.bfloat16)
    for slot in range(4):
        at = pl.multiple_of(128 * meta[2 + slot], 128)
        outs[slot][...] = line[:, pl.ds(at, 128)]


def read_body(meta, query, query_gain, out_gain, shift, *rest, size, blocks, scale):
    mine, theirs = rest[:8], rest[8:11]
    keys, values, first = rest[11:14]
    score_ref, weight_ref, sems = rest[14:]
    theirs_of = [
        (0, 0),
        (0, 1),
        (0, 2),
        (1, 0),
        (1, 3),
        (1, 1),
        (1, 2),
        (2, 0),
    ]
    per = size // 128

    def their(j):
        part, at = theirs_of[j]
        return theirs[part].at[pl.ds(at * size, size), :]

    q = row_norm(query[...].astype(jnp.float32), query_gain[...]).astype(jnp.bfloat16)
    q = jnp.broadcast_to(q, (16, 128))

    def run(key_of, value_of):
        copies = []
        for j in range(8):
            at = pl.multiple_of(meta[2 + j] * size, 128)
            copies.append(
                pltpu.make_async_copy(key_of(j), keys.at[pl.ds(at, size), :], sems.at[j])
            )
            copies.append(
                pltpu.make_async_copy(value_of(j), values.at[pl.ds(at, size), :], sems.at[8 + j])
            )
        for c in copies:
            c.start()
        for j in range(8):
            s = lax.dot_general(
                q, key_of(j)[...], (((1,), (1,)), ((), ())), preferred_element_type=jnp.float32
            )
            for i in range(per):
                score_ref[pl.ds(meta[2 + j] * per + i, 1), :] = s[0:1, 128 * i : 128 * i + 128]
        s = score_ref[...] * scale + shift[...].astype(jnp.float32)
        keep = jax.nn.log_sigmoid(-s)
        lower = lax.broadcasted_iota(jnp.int32, (128, 128), 0)
        tri = (lower > lax.broadcasted_iota(jnp.int32, (128, 128), 1)).astype(jnp.float32)
        inside = jnp.dot(
            keep, tri, precision=lax.Precision.HIGHEST, preferred_element_type=jnp.float32
        )
        row = lax.broadcasted_iota(jnp.int32, (blocks, blocks), 0)
        up = (lax.broadcasted_iota(jnp.int32, (blocks, blocks), 1) > row).astype(jnp.float32)
        later = jnp.dot(
            up, keep, precision=lax.Precision.HIGHEST, preferred_element_type=jnp.float32
        )
        inside = inside + jnp.sum(later, axis=1, keepdims=True)
        weight_ref[...] = jnp.exp(jax.nn.log_sigmoid(s) + inside)
        total = jnp.zeros((16, 128), jnp.float32)
        for j in range(8):
            ref = value_of(j)
            for i in range(per):
                w = weight_ref[pl.ds(meta[2 + j] * per + i, 1), :].astype(jnp.bfloat16)
                total = total + jnp.dot(
                    jnp.broadcast_to(w, (16, 128)),
                    ref[128 * i : 128 * i + 128, :],
                    preferred_element_type=jnp.float32,
                )
        first[...] = row_norm(total[0:1], out_gain[...]).astype(jnp.bfloat16)
        for c in copies:
            c.wait()

    @pl.when(meta[1] == 0)
    def _():
        run(lambda j: mine[j], their)

    @pl.when(meta[1] == 1)
    def _():
        run(their, lambda j: mine[j])


def in_vmem(n):
    return [pl.BlockSpec(memory_space=pltpu.VMEM)] * n


def in_smem():
    return [pl.BlockSpec(memory_space=pltpu.SMEM)]


def shards(
    layer_input,
    input_gain,
    key_weight,
    value_weight,
    key_gain,
    stop_shift,
    new_query,
    query_gain,
    out_gain,
):
    groups = lax.axis_size("tp")
    n_sp = lax.axis_size("sp")
    nz, ny = n_sp // NX, groups // 2
    rows = layer_input.shape[1]
    size = 2 * rows
    head_size = new_query.shape[2]
    length = rows * groups
    place = lax.axis_index("tp")
    y, core = place // 2, place % 2
    at_sp = lax.axis_index("sp")
    cls = (at_sp % NX + 2 * (at_sp // NX)) % NX

    own = jnp.concatenate((packed(key_weight), packed(value_weight)), 0)
    classes = [[z * NX + (c + 2 * z) % NX for z in range(nz)] for c in range(NX)]
    got = lax.all_to_all(
        jnp.broadcast_to(own, (nz, *own.shape)),
        "sp",
        split_axis=0,
        concat_axis=0,
        tiled=True,
        axis_index_groups=classes,
    )
    deep = 16 * nz
    both = got.reshape(nz, 2, 16, 128).transpose(1, 0, 2, 3).reshape(2, deep, 128)
    shifts = jnp.pad(stop_shift[0].reshape(KVH, rows // 128, 128), ((0, 0), (0, 13), (0, 0)))
    sent = jnp.concatenate(
        (
            jnp.broadcast_to(both[None], (ny, 2, deep, 128)).reshape(groups, deep, 128),
            jnp.repeat(shifts, groups // KVH, axis=0),
        ),
        axis=1,
    )
    recv = lax.all_to_all(sent, "tp", split_axis=0, concat_axis=0, tiled=True)
    shift_line = recv[:, deep : deep + rows // 128, :].reshape(length // 128, 128)
    cols = KVH * head_size
    w0, low, high = pl.pallas_call(
        lambda *refs: build_body(*refs, blocks=nz),
        out_shape=(
            jax.ShapeDtypeStruct((nz, 4, 16, cols), jnp.bfloat16),
            jax.ShapeDtypeStruct((nz // 2, 4, 16, cols), jnp.bfloat16),
            jax.ShapeDtypeStruct((nz // 2, 4, 16, cols), jnp.bfloat16),
        ),
        in_specs=in_vmem(1),
        out_specs=tuple(in_vmem(3)),
        name="build",
    )(recv)
    w0 = w0.reshape(nz * 64, cols)
    low, high = low.reshape(nz * 32, cols), high.reshape(nz * 32, cols)
    wl = moved_sp(w0, 0, 1)
    wr = moved_sp(w0, 0, -1)
    wu = moved_sp(low, 1, 0)
    wd = moved_sp(high, -1, 0)

    normed = row_norm(layer_input[0].astype(jnp.float32), input_gain).astype(jnp.bfloat16)
    other = swapped(normed)

    pair = y // 2
    sign = jnp.where(y % 2 == 0, -1, 1)
    heads = [pair, pair + sign, pair - sign, pair + 2]
    meta = jnp.stack([cls, core] + [(h + KVH) % KVH for h in heads]).astype(jnp.int32)
    slots = pl.pallas_call(
        project_body,
        out_shape=tuple(jax.ShapeDtypeStruct((size, head_size), jnp.bfloat16) for _ in range(4)),
        in_specs=in_smem() + in_vmem(8),
        out_specs=tuple(in_vmem(4)),
        scratch_shapes=[
            pltpu.VMEM((n_sp * 64, cols), jnp.bfloat16),
            pltpu.VMEM((size, cols), jnp.bfloat16),
        ],
        name="project",
    )(meta, normed, other, w0, wl, wr, wu, wd, key_gain.reshape(1, head_size))

    across = lambda at: at ^ 1
    mine0 = slots[0]
    p1 = moved_y(slots[1], step_to(1))
    p2 = moved_y(slots[2], step_to(2))
    p3 = moved_y(slots[3], step_to(3))
    f0 = moved_y(mine0, across)
    f1 = moved_y(p1, across)
    f2 = moved_y(p2, across)
    f3 = moved_y(p3, across)
    t1 = swapped(jnp.concatenate((mine0, f0, p1), 0))
    t2 = swapped(jnp.concatenate((p2, f1, f2, p3), 0))
    t3 = swapped(f3)
    beside = y + 1 - 2 * (y % 2)
    sources = [y, beside] + [y + sign * d for d in (1, 2, 3)] + [beside - sign * d for d in (1, 2, 3)]
    meta2 = jnp.stack([y, core] + [(s + ny) % ny for s in sources]).astype(jnp.int32)
    key_line, value_line, first_out = pl.pallas_call(
        lambda *refs: read_body(
            *refs, size=size, blocks=length // 128, scale=1.0 / head_size**0.5
        ),
        out_shape=(
            jax.ShapeDtypeStruct((length, head_size), jnp.bfloat16),
            jax.ShapeDtypeStruct((length, head_size), jnp.bfloat16),
            jax.ShapeDtypeStruct((1, head_size), jnp.bfloat16),
        ),
        in_specs=in_smem() + in_vmem(15),
        out_specs=(
            pl.BlockSpec(memory_space=pl.ANY),
            pl.BlockSpec(memory_space=pl.ANY),
            pl.BlockSpec(memory_space=pltpu.VMEM),
        ),
        scratch_shapes=[
            pltpu.VMEM((length // 128, 128), jnp.float32),
            pltpu.VMEM((length // 128, 128), jnp.float32),
            pltpu.SemaphoreType.DMA((16,)),
        ],
        name="read",
    )(
        meta2,
        new_query[0],
        query_gain.reshape(1, head_size),
        out_gain.reshape(1, head_size),
        shift_line,
        mine0,
        f0,
        p1,
        p2,
        p3,
        f1,
        f2,
        f3,
        t1,
        t2,
        t3,
    )
    return (
        key_line.reshape(1, 1, length, head_size),
        value_line.reshape(1, 1, length, head_size),
        shift_line.reshape(1, 1, length),
        first_out[None],
    )


def solution(mesh):
    placed = (
        P("sp", "tp", None),
        P(),
        P("sp", "tp"),
        P("sp", "tp"),
        P(),
        P("sp", None, "tp"),
        P("sp", "tp", None),
        P(),
        P(),
    )
    return jax.shard_map(
        shards,
        mesh=mesh,
        in_specs=placed,
        out_specs=(
            P("sp", "tp", None, None),
            P("sp", "tp", None, None),
            P("sp", "tp", None),
            P("sp", "tp", None),
        ),
        check_vma=False,
    )
```

time: 178 us -> 142 us (0.80)
  blocking collectives: 58.7 us -> 0 us
  starting transfers between devices: 14.6 us -> 66.6 us
  waiting for transfers between devices: 65.2 us -> 47 us
  between operations: 15.9 us -> 1.27 us
  Pallas kernels: 0 us -> 14.2 us
  matrix products: 6.12 us -> 0 us
  other arithmetic: 8.59 us -> 3.18 us
    all_to_all x2 -> x0, blocking collectives: 58.7 us -> none  [the longest x1 33.9 us: in_one_piece(): lax.all_to_all(both, axis, split_axis=split_dim, concat_axis=concat_dim,...]
    all_gather x1 -> x0, waiting for transfers between devices: 41.1 us -> none  [shards(): lax.all_gather(full_depth, 'tp', axis=2, tiled=True)]
    ppermute x6 -> x15, starting transfers between devices: 14.5 us -> 44.3 us  [the longest x7 18.6 us: moved_y(): lax.ppermute(x, 'tp', [(i, target(i // 2) % (n // 2) * 2 + i % 2) for i i...]
    all_to_all x0 -> x2, starting transfers between devices: none -> 22.3 us  [the longest x1 13.3 us: shards(): lax.all_to_all(jnp.broadcast_to(own, (nz, *own.shape)), 'sp', split_axis=...]
    all_to_all x0 -> x2, waiting for transfers between devices: none -> 22 us  [the longest x1 16.1 us: shards(): recv = lax.all_to_all(sent, 'tp', split_axis=0, concat_axis=0, tiled=True)]
    pallas_call x0 -> x3, Pallas kernels: none -> 14.2 us  [the longest x1 6.19 us: shards(): pl.pallas_call(lambda *refs: read_body(*refs, size=size, blocks=length //...]
    dot_general x3 -> x0, matrix products: 6.12 us -> none  [the longest x1 4.61 us: shards(): jnp.einsum('rd,kdc->krc', normed, lax.all_gather(full_depth, 'tp', axis=2...]
    select_n x5 -> x0, other arithmetic: 3.88 us -> none  [shards(): jnp.where(upper, jnp.concatenate((theirs, mine), 0), jnp.concatenate((min...]
  transfers between devices with their start and end apart: 7 -> 17, of which waited for: 5 -> 8; matrix products, arithmetic and copies ran while one was open for 4% -> 4% of each run, Pallas kernels for 0% -> 2%
where the time goes in v1:
time: 142 us; the launch traced here: 141 us
  starting transfers between devices  66.6 us (47%)
  waiting for transfers between devices  47 us (33%)
  Pallas kernels  14.2 us (10%)
  local copies, waits for them, and re-layouts  8.44 us (6%)
  other arithmetic  3.18 us (2%)
    ppermute x7, waiting for transfers between devices, moved_y(): lax.ppermute(x, 'tp', [(i, target(i // 2) % (n // 2) * 2 + i % 2) for i i...  19.3 us
    ppermute x7, starting transfers between devices, moved_y(): lax.ppermute(x, 'tp', [(i, target(i // 2) % (n // 2) * 2 + i % 2) for i i...  18.6 us
    all_to_all x1, waiting for transfers between devices, shards(): recv = lax.all_to_all(sent, 'tp', split_axis=0, concat_axis=0, tiled=True)  16.1 us
    all_to_all x1, starting transfers between devices, shards(): lax.all_to_all(jnp.broadcast_to(own, (nz, *own.shape)), 'sp', split_axis=...  13.3 us
    ppermute x4, starting transfers between devices, moved_sp(): return lax.ppermute(x, 'sp', pairs)  13 us
    ppermute x4, starting transfers between devices, swapped(): lax.ppermute(x, 'tp', [(i, i ^ 1) for i in range(lax.axis_size('tp'))])  12.7 us
    all_to_all x1, starting transfers between devices, shards(): recv = lax.all_to_all(sent, 'tp', split_axis=0, concat_axis=0, tiled=True)  8.97 us
    pallas_call x1, Pallas kernels, shards(): pl.pallas_call(lambda *refs: read_body(*refs, size=size, blocks=length //...  6.19 us
  transfers between devices with their start and end apart: 17, of which 8 were waited for; matrix products, arithmetic and copies ran while one was open for 4% of the time, Pallas kernels for 2%

profile of v1, /device:TPU:1, one launch (start us, length us, event | category | flops | bytes accessed | tf_op | source)
XLA Modules:
  0.0 140.7 jit_solution(1438813704089724071)
XLA Ops:
  3.1 13.3 %all-to-all-start = ((bf16[8,32,128]{2,1,0:T(8,128)(2,1)}), bf16[8,32,128]{2,1,0:T(8,128)(2,1)S(1)}, u32[]{:S(2)}, u32[]{:S(2)}) async-start(bf16[8,32,128]{2,1,0:T(8,128)(2,1)} %broadcast_in_dim.18), calls=%async_computation | async-start | bytes 131072 | tf_op jit(solution)/shard_map/all_to_all | solution.py:211
  18.9 5.9 %all-to-all-done = bf16[8,32,128]{2,1,0:T(8,128)(2,1)S(1)} async-done(((bf16[8,32,128]{2,1,0:T(8,128)(2,1)}), bf16[8,32,128]{2,1,0:T(8,128)(2,1)S(1)}, u32[]{:S(2)}, u32[]{:S(2)}) %all-to-all-start) | async-done | bytes 65568 | tf_op jit(solution)/shard_map/all_to_all | solution.py:211
  25.7 9.0 %all-to-all-start.1 = ((bf16[16,144,128]{2,1,0:T(8,128)(2,1)}), bf16[16,144,128]{2,1,0:T(8,128)(2,1)}, u32[]{:S(2)}, u32[]{:S(2)}) async-start(bf16[16,144,128]{2,1,0:T(8,128)(2,1)} %pad_maximum_fusion.1), calls=%async_computation.1 | async-start | bytes 1179648 | tf_op jit(solution)/shard_map/all_to_all | solution.py:229
  35.2 2.1 %collective-permute-start = (bf16[384,2048]{1,0:T(8,128)(2,1)S(1)}, bf16[384,2048]{1,0:T(8,128)(2,1)S(1)}, u32[]{:S(2)}, u32[]{:S(2)}) collective-permute-start(bf16[384,2048]{1,0:T(8,128)(2,1)S(1)} %fusion.2.own), channel_id=1, source_target_pairs={{0,1},{1,0},{2,3},{3,2},{4,5},{5,4},{6,7},{7,6},{8,9},{9,8},{10,11... | collective-permute-start | bytes 4718600 | tf_op jit(solution)/shard_map/ppermute | solution.py:37
  37.2 16.1 %all-to-all-done.1.refs_0_ = bf16[16,144,128]{2,1,0:T(8,128)(2,1)} async-done(((bf16[16,144,128]{2,1,0:T(8,128)(2,1)}), bf16[16,144,128]{2,1,0:T(8,128)(2,1)}, u32[]{:S(2)}, u32[]{:S(2)}) %all-to-all-start.1) | async-done | bytes 589856 | tf_op jit(solution)/shard_map/all_to_all | solution.py:229
  53.4 2.5 %build.1 = (bf16[8,4,16,512]{3,2,1,0:T(8,128)(2,1)}, bf16[4,4,16,512]{3,2,1,0:T(8,128)(2,1)}, bf16[4,4,16,512]{3,2,1,0:T(8,128)(2,1)}) custom-call(bf16[16,144,128]{2,1,0:T(8,128)(2,1)} %all-to-all-done.1.refs_0_), custom_call_target="tpu_custom_call" | custom-call | tf_op jit(solution)/shard_map/build/pallas_call | solution.py:232
  55.9 2.2 %collective-permute-start.1 = (bf16[512,512]{1,0:T(8,128)(2,1)}, bf16[512,512]{1,0:T(8,128)(2,1)}, u32[]{:S(2)}, u32[]{:S(2)}) collective-permute-start(bf16[512,512]{1,0:T(8,128)(2,1)} %bitcast.43), channel_id=1, source_target_pairs={{0,16},{16,32},{32,48},{48,0},{64,80},{80,96},{96,112},{112,64},{1... | collective-permute-start | bytes 1572872 | tf_op jit(solution)/shard_map/ppermute | solution.py:28
  58.1 4.2 %collective-permute-start.2 = (bf16[512,512]{1,0:T(8,128)(2,1)}, bf16[512,512]{1,0:T(8,128)(2,1)}, u32[]{:S(2)}, u32[]{:S(2)}) collective-permute-start(bf16[512,512]{1,0:T(8,128)(2,1)} %bitcast.44), channel_id=1, source_target_pairs={{0,48},{16,0},{32,16},{48,32},{64,112},{80,64},{96,80},{112,96},{1... | collective-permute-start | bytes 1572872 | tf_op jit(solution)/shard_map/ppermute | solution.py:28
  62.4 1.9 %collective-permute-start.3 = (bf16[256,512]{1,0:T(8,128)(2,1)}, bf16[256,512]{1,0:T(8,128)(2,1)S(1)}, u32[]{:S(2)}, u32[]{:S(2)}) collective-permute-start(bf16[256,512]{1,0:T(8,128)(2,1)} %bitcast.59), channel_id=1, source_target_pairs={{0,64},{16,80},{32,96},{48,112},{64,128},{80,144},{96,160},{112,17... | collective-permute-start | bytes 786440 | tf_op jit(solution)/shard_map/ppermute | solution.py:28
  64.3 4.6 %collective-permute-start.4 = (bf16[256,512]{1,0:T(8,128)(2,1)}, bf16[256,512]{1,0:T(8,128)(2,1)}, u32[]{:S(2)}, u32[]{:S(2)}) collective-permute-start(bf16[256,512]{1,0:T(8,128)(2,1)} %bitcast.58), channel_id=1, source_target_pairs={{0,448},{16,464},{32,480},{48,496},{64,0},{80,16},{96,32},{112,48}... | collective-permute-start | bytes 786440 | tf_op jit(solution)/shard_map/ppermute | solution.py:28
  69.6 3.8 %collective-permute-done.3.wu = bf16[256,512]{1,0:T(8,128)(2,1)S(1)} collective-permute-done((bf16[256,512]{1,0:T(8,128)(2,1)}, bf16[256,512]{1,0:T(8,128)(2,1)S(1)}, u32[]{:S(2)}, u32[]{:S(2)}) %collective-permute-start.3) | collective-permute-done | bytes 262176 | tf_op jit(solution)/shard_map/ppermute | solution.py:28
  76.4 5.5 %project.1 = (bf16[768,128]{1,0:T(8,128)(2,1)}, bf16[768,128]{1,0:T(8,128)(2,1)}, bf16[768,128]{1,0:T(8,128)(2,1)}, bf16[768,128]{1,0:T(8,128)(2,1)}) custom-call(s32[6]{0:T(128)} %stack.68.meta, bf16[384,2048]{1,0:T(8,128)(2,1)} %copy-done.1, bf16[384,2048]{1,0:T(8,128)(2,1)} %copy-done.2, bf16[512,512]{1,0:T(8,128)(2,1)} %bitcast.45, ...), custom_call_target="tpu_custom_call" | custom-call | tf_op jit(solution)/shard_map/project/pallas_call | solution.py:257
  81.9 2.0 %collective-permute-start.6 = (bf16[768,128]{1,0:T(8,128)(2,1)}, bf16[768,128]{1,0:T(8,128)(2,1)S(1)}, u32[]{:S(2)}, u32[]{:S(2)}) collective-permute-start(bf16[768,128]{1,0:T(8,128)(2,1)} %get-tuple-element.18), channel_id=1, source_target_pairs={{0,14},{1,15},{2,4},{3,5},{4,2},{5,3},{6,8},{7,9},{8,6},{9,7},{10,... | collective-permute-start | bytes 589832 | tf_op jit(solution)/shard_map/ppermute | solution.py:33
  84.0 1.9 %collective-permute-start.7 = (bf16[768,128]{1,0:T(8,128)(2,1)}, bf16[768,128]{1,0:T(8,128)(2,1)S(1)}, u32[]{:S(2)}, u32[]{:S(2)}) collective-permute-start(bf16[768,128]{1,0:T(8,128)(2,1)} %get-tuple-element.19), channel_id=1, source_target_pairs={{0,4},{1,5},{2,14},{3,15},{4,8},{5,9},{6,2},{7,3},{8,12},{9,13},{1... | collective-permute-start | bytes 589832 | tf_op jit(solution)/shard_map/ppermute | solution.py:33
  85.9 4.0 %collective-permute-start.8 = (bf16[768,128]{1,0:T(8,128)(2,1)}, bf16[768,128]{1,0:T(8,128)(2,1)S(1)}, u32[]{:S(2)}, u32[]{:S(2)}) collective-permute-start(bf16[768,128]{1,0:T(8,128)(2,1)} %get-tuple-element.20), channel_id=1, source_target_pairs={{0,10},{1,11},{2,8},{3,9},{4,14},{5,15},{6,12},{7,13},{8,2},{9,3},... | collective-permute-start | bytes 589832 | tf_op jit(solution)/shard_map/ppermute | solution.py:33
  89.9 10.0 %collective-permute-done.6.refs_7_ = bf16[768,128]{1,0:T(8,128)(2,1)S(1)} collective-permute-done((bf16[768,128]{1,0:T(8,128)(2,1)}, bf16[768,128]{1,0:T(8,128)(2,1)S(1)}, u32[]{:S(2)}, u32[]{:S(2)}) %collective-permute-start.6) | collective-permute-done | bytes 196640 | tf_op jit(solution)/shard_map/ppermute | solution.py:33
  101.8 3.4 %collective-permute-start.10 = (bf16[768,128]{1,0:T(8,128)(2,1)S(1)}, bf16[768,128]{1,0:T(8,128)(2,1)S(1)}, u32[]{:S(2)}, u32[]{:S(2)}) collective-permute-start(bf16[768,128]{1,0:T(8,128)(2,1)S(1)} %collective-permute-done.7.refs_8_), channel_id=1, source_target_pairs={{0,2},{1,3},{2,0},{3,1},{4,6},{5,7},{6,4},{7,5},{8,10},{9,11},{10,... | collective-permute-start | bytes 589832 | tf_op jit(solution)/shard_map/ppermute | solution.py:33
  107.5 4.2 %collective-permute-done.10.refs_11_ = bf16[768,128]{1,0:T(8,128)(2,1)S(1)} collective-permute-done((bf16[768,128]{1,0:T(8,128)(2,1)S(1)}, bf16[768,128]{1,0:T(8,128)(2,1)S(1)}, u32[]{:S(2)}, u32[]{:S(2)}) %collective-permute-start.10) | collective-permute-done | bytes 196640 | tf_op jit(solution)/shard_map/ppermute | solution.py:33
  111.8 5.6 %collective-permute-start.13 = (bf16[3072,128]{1,0:T(8,128)(2,1)S(1)}, bf16[3072,128]{1,0:T(8,128)(2,1)S(1)}, u32[]{:S(2)}, u32[]{:S(2)}) collective-permute-start(bf16[3072,128]{1,0:T(8,128)(2,1)S(1)} %pad_maximum_fusion), channel_id=1, source_target_pairs={{0,1},{1,0},{2,3},{3,2},{4,5},{5,4},{6,7},{7,6},{8,9},{9,8},{10,11... | collective-permute-start | bytes 2359304 | tf_op jit(solution)/shard_map/ppermute | solution.py:37
  117.5 2.0 %collective-permute-start.12 = (bf16[2304,128]{1,0:T(8,128)(2,1)S(1)}, bf16[2304,128]{1,0:T(8,128)(2,1)}, u32[]{:S(2)}, u32[]{:S(2)}) collective-permute-start(bf16[2304,128]{1,0:T(8,128)(2,1)S(1)} %pad_maximum_fusion.2), channel_id=1, source_target_pairs={{0,1},{1,0},{2,3},{3,2},{4,5},{5,4},{6,7},{7,6},{8,9},{9,8},{10,11... | collective-permute-start | bytes 1769480 | tf_op jit(solution)/shard_map/ppermute | solution.py:37
  119.5 3.5 %collective-permute-start.11 = (bf16[768,128]{1,0:T(8,128)(2,1)S(1)}, bf16[768,128]{1,0:T(8,128)(2,1)S(1)}, u32[]{:S(2)}, u32[]{:S(2)}) collective-permute-start(bf16[768,128]{1,0:T(8,128)(2,1)S(1)} %collective-permute-done.8.refs_9_), channel_id=1, source_target_pairs={{0,2},{1,3},{2,0},{3,1},{4,6},{5,7},{6,4},{7,5},{8,10},{9,11},{10,... | collective-permute-start | bytes 589832 | tf_op jit(solution)/shard_map/ppermute | solution.py:33
  123.0 4.7 %collective-permute-done.11.refs_12_ = bf16[768,128]{1,0:T(8,128)(2,1)S(1)} collective-permute-done((bf16[768,128]{1,0:T(8,128)(2,1)S(1)}, bf16[768,128]{1,0:T(8,128)(2,1)S(1)}, u32[]{:S(2)}, u32[]{:S(2)}) %collective-permute-start.11) | collective-permute-done | bytes 196640 | tf_op jit(solution)/shard_map/ppermute | solution.py:33
  127.8 3.0 %collective-permute-start.14 = (bf16[768,128]{1,0:T(8,128)(2,1)S(1)}, bf16[768,128]{1,0:T(8,128)(2,1)}, u32[]{:S(2)}, u32[]{:S(2)}) collective-permute-start(bf16[768,128]{1,0:T(8,128)(2,1)S(1)} %collective-permute-done.11.refs_12_), channel_id=1, source_target_pairs={{0,1},{1,0},{2,3},{3,2},{4,5},{5,4},{6,7},{7,6},{8,9},{9,8},{10,11... | collective-permute-start | bytes 589832 | tf_op jit(solution)/shard_map/ppermute | solution.py:37
  134.5 6.2 %read.1 = (bf16[6144,128]{1,0:T(8,128)(2,1)}, bf16[6144,128]{1,0:T(8,128)(2,1)}, bf16[1,128]{1,0:T(2,128)(2,1)}) custom-call(s32[10]{0:T(128)} %stack.62.refs_0_, bf16[1,128]{1,0:T(2,128)(2,1)} %bitcast.53, f32[1,128]{1,0:T(1,128)} %bitcast.54, f32[1,128]{1,0:T(1,128)} %bitcast.55, bf16[48,128]{1,0:T(8,128)(2,1)} %reshape.77.refs_4_, ...), custom_call_target="tpu_custom_call" | custom-call | tf_op jit(solution)/shard_map/read/pallas_call | solution.py:284
  (65 shorter events, 17.7 us)
Async XLA Ops:
  3.1 21.7 %all-to-all-start = ((bf16[8,32,128]{2,1,0:T(8,128)(2,1)}), bf16[8,32,128]{2,1,0:T(8,128)(2,1)S(1)}, u32[]{:S(2)}, u32[]{:S(2)}) async-start(bf16[8,32,128]{2,1,0:T(8,128)(2,1)} %broadcast_in_dim.18), calls=%async_computation | async-start | bytes 131072 | tf_op jit(solution)/shard_map/all_to_all | solution.py:211
  25.7 27.6 %all-to-all-start.1 = ((bf16[16,144,128]{2,1,0:T(8,128)(2,1)}), bf16[16,144,128]{2,1,0:T(8,128)(2,1)}, u32[]{:S(2)}, u32[]{:S(2)}) async-start(bf16[16,144,128]{2,1,0:T(8,128)(2,1)} %pad_maximum_fusion.1), calls=%async_computation.1 | async-start | bytes 1179648 | tf_op jit(solution)/shard_map/all_to_all | solution.py:229
  35.2 40.2 %copy-start.1 = (bf16[384,2048]{1,0:T(8,128)(2,1)}, bf16[384,2048]{1,0:T(8,128)(2,1)S(1)}, u32[]{:S(2)}) copy-start(bf16[384,2048]{1,0:T(8,128)(2,1)S(1)} %fusion.2.own) | copy-start | bytes 4718596
  35.2 40.1 %collective-permute-start = (bf16[384,2048]{1,0:T(8,128)(2,1)S(1)}, bf16[384,2048]{1,0:T(8,128)(2,1)S(1)}, u32[]{:S(2)}, u32[]{:S(2)}) collective-permute-start(bf16[384,2048]{1,0:T(8,128)(2,1)S(1)} %fusion.2.own), channel_id=1, source_target_pairs={{0,1},{1,0},{2,3},{3,2},{4,5},{5,4},{6,7},{7,6},{8,9},{9,8},{10,11... | collective-permute-start | bytes 4718600 | tf_op jit(solution)/shard_map/ppermute | solution.py:37
  55.9 19.4 %collective-permute-start.1 = (bf16[512,512]{1,0:T(8,128)(2,1)}, bf16[512,512]{1,0:T(8,128)(2,1)}, u32[]{:S(2)}, u32[]{:S(2)}) collective-permute-start(bf16[512,512]{1,0:T(8,128)(2,1)} %bitcast.43), channel_id=1, source_target_pairs={{0,16},{16,32},{32,48},{48,0},{64,80},{80,96},{96,112},{112,64},{1... | collective-permute-start | bytes 1572872 | tf_op jit(solution)/shard_map/ppermute | solution.py:28
  58.1 17.2 %collective-permute-start.2 = (bf16[512,512]{1,0:T(8,128)(2,1)}, bf16[512,512]{1,0:T(8,128)(2,1)}, u32[]{:S(2)}, u32[]{:S(2)}) collective-permute-start(bf16[512,512]{1,0:T(8,128)(2,1)} %bitcast.44), channel_id=1, source_target_pairs={{0,48},{16,0},{32,16},{48,32},{64,112},{80,64},{96,80},{112,96},{1... | collective-permute-start | bytes 1572872 | tf_op jit(solution)/shard_map/ppermute | solution.py:28
  62.4 11.0 %collective-permute-start.3 = (bf16[256,512]{1,0:T(8,128)(2,1)}, bf16[256,512]{1,0:T(8,128)(2,1)S(1)}, u32[]{:S(2)}, u32[]{:S(2)}) collective-permute-start(bf16[256,512]{1,0:T(8,128)(2,1)} %bitcast.59), channel_id=1, source_target_pairs={{0,64},{16,80},{32,96},{48,112},{64,128},{80,144},{96,160},{112,17... | collective-permute-start | bytes 786440 | tf_op jit(solution)/shard_map/ppermute | solution.py:28
  64.3 11.0 %collective-permute-start.4 = (bf16[256,512]{1,0:T(8,128)(2,1)}, bf16[256,512]{1,0:T(8,128)(2,1)}, u32[]{:S(2)}, u32[]{:S(2)}) collective-permute-start(bf16[256,512]{1,0:T(8,128)(2,1)} %bitcast.58), channel_id=1, source_target_pairs={{0,448},{16,464},{32,480},{48,496},{64,0},{80,16},{96,32},{112,48}... | collective-permute-start | bytes 786440 | tf_op jit(solution)/shard_map/ppermute | solution.py:28
  81.9 35.5 %copy-start.4 = (bf16[768,128]{1,0:T(8,128)(2,1)S(1)}, bf16[768,128]{1,0:T(8,128)(2,1)}, u32[]{:S(2)}) copy-start(bf16[768,128]{1,0:T(8,128)(2,1)} %get-tuple-element.17.refs_5_) | copy-start | bytes 589828
  81.9 18.0 %collective-permute-start.6 = (bf16[768,128]{1,0:T(8,128)(2,1)}, bf16[768,128]{1,0:T(8,128)(2,1)S(1)}, u32[]{:S(2)}, u32[]{:S(2)}) collective-permute-start(bf16[768,128]{1,0:T(8,128)(2,1)} %get-tuple-element.18), channel_id=1, source_target_pairs={{0,14},{1,15},{2,4},{3,5},{4,2},{5,3},{6,8},{7,9},{8,6},{9,7},{10,... | collective-permute-start | bytes 589832 | tf_op jit(solution)/shard_map/ppermute | solution.py:33
  84.0 17.8 %collective-permute-start.7 = (bf16[768,128]{1,0:T(8,128)(2,1)}, bf16[768,128]{1,0:T(8,128)(2,1)S(1)}, u32[]{:S(2)}, u32[]{:S(2)}) collective-permute-start(bf16[768,128]{1,0:T(8,128)(2,1)} %get-tuple-element.19), channel_id=1, source_target_pairs={{0,4},{1,5},{2,14},{3,15},{4,8},{5,9},{6,2},{7,3},{8,12},{9,13},{1... | collective-permute-start | bytes 589832 | tf_op jit(solution)/shard_map/ppermute | solution.py:33
  85.9 21.2 %collective-permute-start.8 = (bf16[768,128]{1,0:T(8,128)(2,1)}, bf16[768,128]{1,0:T(8,128)(2,1)S(1)}, u32[]{:S(2)}, u32[]{:S(2)}) collective-permute-start(bf16[768,128]{1,0:T(8,128)(2,1)} %get-tuple-element.20), channel_id=1, source_target_pairs={{0,10},{1,11},{2,8},{3,9},{4,14},{5,15},{6,12},{7,13},{8,2},{9,3},... | collective-permute-start | bytes 589832 | tf_op jit(solution)/shard_map/ppermute | solution.py:33
  99.9 33.7 %copy-start.5 = (bf16[768,128]{1,0:T(8,128)(2,1)}, bf16[768,128]{1,0:T(8,128)(2,1)S(1)}, u32[]{:S(2)}) copy-start(bf16[768,128]{1,0:T(8,128)(2,1)S(1)} %collective-permute-done.6.refs_7_) | copy-start | bytes 589828
  99.9 7.6 %collective-permute-start.9 = (bf16[768,128]{1,0:T(8,128)(2,1)S(1)}, bf16[768,128]{1,0:T(8,128)(2,1)S(1)}, u32[]{:S(2)}, u32[]{:S(2)}) collective-permute-start(bf16[768,128]{1,0:T(8,128)(2,1)S(1)} %collective-permute-done.6.refs_7_), channel_id=1, source_target_pairs={{0,2},{1,3},{2,0},{3,1},{4,6},{5,7},{6,4},{7,5},{8,10},{9,11},{10,... | collective-permute-start | bytes 589832 | tf_op jit(solution)/shard_map/ppermute | solution.py:33
  101.8 31.8 %copy-start.6 = (bf16[768,128]{1,0:T(8,128)(2,1)}, bf16[768,128]{1,0:T(8,128)(2,1)S(1)}, u32[]{:S(2)}) copy-start(bf16[768,128]{1,0:T(8,128)(2,1)S(1)} %collective-permute-done.7.refs_8_) | copy-start | bytes 589828
  101.8 9.9 %collective-permute-start.10 = (bf16[768,128]{1,0:T(8,128)(2,1)S(1)}, bf16[768,128]{1,0:T(8,128)(2,1)S(1)}, u32[]{:S(2)}, u32[]{:S(2)}) collective-permute-start(bf16[768,128]{1,0:T(8,128)(2,1)S(1)} %collective-permute-done.7.refs_8_), channel_id=1, source_target_pairs={{0,2},{1,3},{2,0},{3,1},{4,6},{5,7},{6,4},{7,5},{8,10},{9,11},{10,... | collective-permute-start | bytes 589832 | tf_op jit(solution)/shard_map/ppermute | solution.py:33
  105.2 12.2 %collective-permute-start.5 = (bf16[768,128]{1,0:T(8,128)(2,1)}, bf16[768,128]{1,0:T(8,128)(2,1)S(1)}, u32[]{:S(2)}, u32[]{:S(2)}) collective-permute-start(bf16[768,128]{1,0:T(8,128)(2,1)} %get-tuple-element.17.refs_5_), channel_id=1, source_target_pairs={{0,2},{1,3},{2,0},{3,1},{4,6},{5,7},{6,4},{7,5},{8,10},{9,11},{10,... | collective-permute-start | bytes 589832 | tf_op jit(solution)/shard_map/ppermute | solution.py:33
  107.1 26.5 %copy-start.7 = (bf16[768,128]{1,0:T(8,128)(2,1)}, bf16[768,128]{1,0:T(8,128)(2,1)S(1)}, u32[]{:S(2)}) copy-start(bf16[768,128]{1,0:T(8,128)(2,1)S(1)} %collective-permute-done.8.refs_9_) | copy-start | bytes 589828
  107.5 26.1 %copy-start.8 = (bf16[768,128]{1,0:T(8,128)(2,1)}, bf16[768,128]{1,0:T(8,128)(2,1)S(1)}, u32[]{:S(2)}) copy-start(bf16[768,128]{1,0:T(8,128)(2,1)S(1)} %collective-permute-done.9.refs_10_) | copy-start | bytes 589828
  111.7 21.9 %copy-start.9 = (bf16[768,128]{1,0:T(8,128)(2,1)}, bf16[768,128]{1,0:T(8,128)(2,1)S(1)}, u32[]{:S(2)}) copy-start(bf16[768,128]{1,0:T(8,128)(2,1)S(1)} %collective-permute-done.10.refs_11_) | copy-start | bytes 589828
  111.8 21.8 %collective-permute-start.13 = (bf16[3072,128]{1,0:T(8,128)(2,1)S(1)}, bf16[3072,128]{1,0:T(8,128)(2,1)S(1)}, u32[]{:S(2)}, u32[]{:S(2)}) collective-permute-start(bf16[3072,128]{1,0:T(8,128)(2,1)S(1)} %pad_maximum_fusion), channel_id=1, source_target_pairs={{0,1},{1,0},{2,3},{3,2},{4,5},{5,4},{6,7},{7,6},{8,9},{9,8},{10,11... | collective-permute-start | bytes 2359304 | tf_op jit(solution)/shard_map/ppermute | solution.py:37
  117.5 16.1 %collective-permute-start.12 = (bf16[2304,128]{1,0:T(8,128)(2,1)S(1)}, bf16[2304,128]{1,0:T(8,128)(2,1)}, u32[]{:S(2)}, u32[]{:S(2)}) collective-permute-start(bf16[2304,128]{1,0:T(8,128)(2,1)S(1)} %pad_maximum_fusion.2), channel_id=1, source_target_pairs={{0,1},{1,0},{2,3},{3,2},{4,5},{5,4},{6,7},{7,6},{8,9},{9,8},{10,11... | collective-permute-start | bytes 1769480 | tf_op jit(solution)/shard_map/ppermute | solution.py:37
  119.5 8.3 %collective-permute-start.11 = (bf16[768,128]{1,0:T(8,128)(2,1)S(1)}, bf16[768,128]{1,0:T(8,128)(2,1)S(1)}, u32[]{:S(2)}, u32[]{:S(2)}) collective-permute-start(bf16[768,128]{1,0:T(8,128)(2,1)S(1)} %collective-permute-done.8.refs_9_), channel_id=1, source_target_pairs={{0,2},{1,3},{2,0},{3,1},{4,6},{5,7},{6,4},{7,5},{8,10},{9,11},{10,... | collective-permute-start | bytes 589832 | tf_op jit(solution)/shard_map/ppermute | solution.py:33
  127.8 5.8 %collective-permute-start.14 = (bf16[768,128]{1,0:T(8,128)(2,1)S(1)}, bf16[768,128]{1,0:T(8,128)(2,1)}, u32[]{:S(2)}, u32[]{:S(2)}) collective-permute-start(bf16[768,128]{1,0:T(8,128)(2,1)S(1)} %collective-permute-done.11.refs_12_), channel_id=1, source_target_pairs={{0,1},{1,0},{2,3},{3,2},{4,5},{5,4},{6,7},{7,6},{8,9},{9,8},{10,11... | collective-permute-start | bytes 589832 | tf_op jit(solution)/shard_map/ppermute | solution.py:37
  (7 other events, 46.0 us)

commit v2 on v1

v2 whole, which is shorter than its diff:
```python
import jax
import jax.numpy as jnp
from jax import lax
from jax.experimental import pallas as pl
from jax.experimental.pallas import tpu as pltpu
from jax.sharding import PartitionSpec as P

KVH = 4
NX = 4
CLASSES = 4
epsilon = 1e-06


def row_norm(value_entries, scaling):
    return (
        value_entries
        * lax.rsqrt(jnp.mean(value_entries * value_entries, axis=-1, keepdims=True) + epsilon)
        * scaling
    )


def moved_sp(x, dz, dx):
    n = lax.axis_size("sp")
    nz = n // NX
    pairs = []
    for i in range(n):
        z, c = (i // NX + dz) % nz, (i % NX + dx) % NX
        pairs.append((i, z * NX + c))
    return lax.ppermute(x, "sp", pairs)


def moved_y(x, target):
    n = lax.axis_size("tp")
    return lax.ppermute(
        x, "tp", [(i, target(i // 2) % (n // 2) * 2 + i % 2) for i in range(n)]
    )


def swapped(x):
    return lax.ppermute(x, "tp", [(i, i ^ 1) for i in range(lax.axis_size("tp"))])


def step_to(distance):
    sign = -1 if distance % 2 else 1
    return lambda y: y + sign * distance if y % 2 == 0 else y - sign * distance


def chip_and_core():
    place = lax.axis_index("tp")
    return lax.div(place, 2), lax.rem(place, 2)


def own_class():
    at = lax.axis_index("sp")
    return lax.rem(lax.rem(at, NX) + 2 * lax.div(at, NX), CLASSES)


def pack_body(key_t, value_t, shift, out):
    groups = out.shape[0]
    zeros = jnp.zeros((13, 128), jnp.float32)
    rows = []
    for ref in (key_t, value_t):
        w = ref[...].astype(jnp.float32)
        rows.append(jnp.concatenate((w[:16], w[16:]), axis=1).astype(jnp.bfloat16))
    lines = shift[...].astype(jnp.float32)
    for head in range(KVH):
        parts = [lines[head : head + 1, 128 * i : 128 * i + 128] for i in range(3)]
        tail = jnp.concatenate((*parts, zeros), axis=0).astype(jnp.bfloat16)
        for i in range(groups // KVH):
            peer = head * (groups // KVH) + i
            out[peer, :16, :] = rows[peer % 2]
            out[peer, 16:, :] = tail


def build_body(recv, blocks, shift48, shift_line, tall, lines):
    groups = recv.shape[0]
    for t in range(groups):
        a = recv[t, :16, :].astype(jnp.float32)
        tall[32 * t : 32 * t + 16, :] = a[:, :64].astype(jnp.bfloat16)
        tall[32 * t + 16 : 32 * t + 32, :] = a[:, 64:].astype(jnp.bfloat16)
        tail = recv[t, 16:, :].astype(jnp.float32)
        lines[3 * t : 3 * t + 3, :] = tail[:3]
    i = lax.broadcasted_iota(jnp.int32, (64, 64), 0)
    eye = (i == lax.broadcasted_iota(jnp.int32, (64, 64), 1)).astype(jnp.bfloat16)
    wide = lax.dot_general(
        eye, tall[...], (((1,), (1,)), ((), ())), preferred_element_type=jnp.float32
    ).astype(jnp.bfloat16)
    for b in range(blocks.shape[0]):
        blocks[b] = wide
    shift48[...] = lines[...]
    for r in range(3 * groups):
        shift_line[0, :, 128 * r : 128 * r + 128] = lines[r : r + 1, :].astype(jnp.bfloat16)


def norm_body(x, gain, out):
    n = row_norm(x[...].astype(jnp.float32), gain[...])
    width = out.shape[1] // CLASSES
    for c in range(CLASSES):
        for m in range(width // 128):
            a = 512 * m + 64 * c
            b = 512 * m + 256 + 64 * ((c + 2) % CLASSES)
            both = jnp.concatenate((n[:, a : a + 64], n[:, b : b + 64]), axis=1)
            out[:, width * c + 128 * m : width * c + 128 * m + 128] = both.astype(jnp.bfloat16)


def columns(ref, c, at, count):
    width = ref.shape[1] // CLASSES
    return ref[:, pl.ds(pl.multiple_of(c * width + at, 128), count)]


def first_body(own, other, w0, acc):
    c = own_class()
    for i, ref in enumerate((own, other)):
        x = columns(ref, c, 0, w0.shape[0])
        acc[i] = jnp.dot(x, w0[...], preferred_element_type=jnp.float32)


def sides_body(own, other, wl, wr, acc, out):
    c = own_class()
    for i, ref in enumerate((own, other)):
        total = acc[i]
        for w, step in ((wl, 3), (wr, 1)):
            x = columns(ref, lax.rem(c + step, CLASSES), 0, w.shape[0])
            total = total + jnp.dot(x, w[...], preferred_element_type=jnp.float32)
        out[i] = total


def last_body(own, other, wu, wd, acc, gain, *rest):
    outs, line = rest[:4], rest[4]
    c = lax.rem(own_class() + 2, CLASSES)
    y, core = chip_and_core()
    rows, half = own.shape[0], wu.shape[0]
    is_key = core == 0
    for i, ref in enumerate((own, other)):
        total = acc[i]
        for w, at in ((wu, 0), (wd, half)):
            x = columns(ref, c, at, half)
            total = total + jnp.dot(x, w[...], preferred_element_type=jnp.float32)
        to = pl.multiple_of((core if i == 0 else 1 - core) * rows, 128)
        for head in range(KVH):
            a = total[:, 128 * head : 128 * head + 128]
            line[pl.ds(to, rows), 128 * head : 128 * head + 128] = jnp.where(
                is_key, row_norm(a, gain[...]), a
            ).astype(jnp.bfloat16)
    pair = lax.div(y, 2)
    sign = 2 * lax.rem(y, 2) - 1
    for slot, head in enumerate((pair, pair + sign, pair - sign, pair + 2)):
        at = pl.multiple_of(128 * lax.rem(head + KVH, KVH), 128)
        outs[slot][...] = line[:, pl.ds(at, 128)]


def read_body(query, query_gain, out_gain, shift, *rest, size, scale, chips):
    mine, theirs = rest[:8], rest[8:11]
    keys, values, first = rest[11:14]
    score_ref, weight_ref, sems = rest[14:]
    theirs_of = [(0, 0), (0, 1), (0, 2), (1, 0), (1, 3), (1, 1), (1, 2), (2, 0)]
    per = size // 128
    blocks = chips * per
    y, core = chip_and_core()
    sign = 2 * lax.rem(y, 2) - 1
    beside = y - sign
    sources = [y, beside] + [y + sign * d for d in (1, 2, 3)] + [beside - sign * d for d in (1, 2, 3)]
    sources = [lax.rem(s + chips, chips) for s in sources]

    def their(j):
        part, at = theirs_of[j]
        return theirs[part].at[pl.ds(at * size, size), :]

    q = row_norm(query[...].astype(jnp.float32), query_gain[...]).astype(jnp.bfloat16)
    rows = lax.broadcasted_iota(jnp.int32, (128, 128), 0)
    lanes = lax.broadcasted_iota(jnp.int32, (128, 128), 1)
    on = rows == lanes
    q_all = jnp.broadcast_to(q, (128, 128))
    ones = jnp.ones((128, 128), jnp.bfloat16)

    def run(key_of, value_of):
        copies = []
        for j in range(8):
            at = pl.multiple_of(sources[j] * size, 128)
            copies.append(
                pltpu.make_async_copy(key_of(j), keys.at[pl.ds(at, size), :], sems.at[j])
            )
            copies.append(
                pltpu.make_async_copy(value_of(j), values.at[pl.ds(at, size), :], sems.at[8 + j])
            )
        for c in copies:
            c.start()
        for j in range(8):
            s = lax.dot_general(
                key_of(j)[...], q_all, (((1,), (1,)), ((), ())), preferred_element_type=jnp.float32
            )
            for i in range(per):
                line = jnp.sum(
                    jnp.where(on, s[128 * i : 128 * i + 128], 0.0), axis=0, keepdims=True
                )
                score_ref[pl.ds(sources[j] * per + i, 1), :] = line
        s = score_ref[...] * scale + shift[...]
        keep = jax.nn.log_sigmoid(-s)
        inside = jnp.dot(
            keep,
            (rows > lanes).astype(jnp.float32),
            precision=lax.Precision.HIGHEST,
            preferred_element_type=jnp.float32,
        )
        at_row = lax.broadcasted_iota(jnp.int32, (blocks, blocks), 0)
        up = (lax.broadcasted_iota(jnp.int32, (blocks, blocks), 1) > at_row).astype(jnp.float32)
        later = jnp.dot(
            up, keep, precision=lax.Precision.HIGHEST, preferred_element_type=jnp.float32
        )
        inside = inside + jnp.sum(later, axis=1, keepdims=True)
        weight_ref[...] = jnp.exp(jax.nn.log_sigmoid(s) + inside)
        total = jnp.zeros((128, 128), jnp.float32)
        for j in range(8):
            ref = value_of(j)
            for i in range(per):
                w = weight_ref[pl.ds(sources[j] * per + i, 1), :]
                spread = jnp.where(on, w, 0.0).astype(jnp.bfloat16)
                spread = jnp.dot(spread, ones, preferred_element_type=jnp.float32)
                total = total + spread * ref[128 * i : 128 * i + 128, :].astype(jnp.float32)
        total = jnp.sum(total, axis=0, keepdims=True)
        first[...] = row_norm(total, out_gain[...]).astype(jnp.bfloat16)
        for c in copies:
            c.wait()

    @pl.when(core == 0)
    def _():
        run(lambda j: mine[j], their)

    @pl.when(core == 1)
    def _():
        run(their, lambda j: mine[j])


def in_vmem(n):
    return [pl.BlockSpec(memory_space=pltpu.VMEM)] * n


def shape(*dims, dtype=jnp.bfloat16):
    return jax.ShapeDtypeStruct(dims, dtype)


def shards(
    layer_input,
    input_gain,
    key_weight,
    value_weight,
    key_gain,
    stop_shift,
    new_query,
    query_gain,
    out_gain,
):
    groups = lax.axis_size("tp")
    n_sp = lax.axis_size("sp")
    nz, ny = n_sp // NX, groups // 2
    rows, width = layer_input.shape[1:]
    size = 2 * rows
    head_size = new_query.shape[2]
    length = rows * groups
    cols = KVH * head_size
    deep = width // n_sp

    sent = pl.pallas_call(
        pack_body,
        out_shape=shape(groups, 32, 128),
        in_specs=in_vmem(3),
        out_specs=in_vmem(1)[0],
        name="pack",
    )(key_weight.T, value_weight.T, stop_shift[0])
    recv = lax.all_to_all(sent, "tp", split_axis=0, concat_axis=0, tiled=True)
    own = pl.pallas_call(
        norm_body,
        grid=(4,),
        out_shape=shape(rows, width),
        in_specs=[
            pl.BlockSpec((rows // 4, width), lambda i: (i, 0)),
            pl.BlockSpec((1, width), lambda i: (0, 0)),
        ],
        out_specs=pl.BlockSpec((rows // 4, width), lambda i: (i, 0)),
        name="norm",
    )(layer_input[0], input_gain.reshape(1, width))
    other = swapped(own)
    blocks, shift48, shift_line = pl.pallas_call(
        build_body,
        out_shape=(
            shape(nz, deep, cols),
            shape(length // 128, 128, dtype=jnp.float32),
            shape(1, 1, length),
        ),
        in_specs=in_vmem(1),
        out_specs=tuple(in_vmem(3)),
        scratch_shapes=[
            pltpu.VMEM((cols, deep), jnp.bfloat16),
            pltpu.VMEM((length // 128, 128), jnp.float32),
        ],
        name="build",
    )(recv)

    classes = [[z * NX + (c + 2 * z) % NX for z in range(nz)] for c in range(CLASSES)]
    got = lax.all_to_all(
        blocks, "sp", split_axis=0, concat_axis=0, tiled=True, axis_index_groups=classes
    )
    w0 = got.reshape(nz * deep, cols)
    half = nz * deep // 2
    wl = moved_sp(w0, 0, 1)
    wr = moved_sp(w0, 0, -1)
    wu = moved_sp(w0[:half], 1, 0)
    wd = moved_sp(w0[half:], -1, 0)
    acc_shape = shape(2, rows, cols, dtype=jnp.float32)
    acc = pl.pallas_call(
        first_body,
        out_shape=acc_shape,
        in_specs=in_vmem(3),
        out_specs=in_vmem(1)[0],
        cost_estimate=pl.CostEstimate(flops=4 * rows * half * cols * 2, bytes_accessed=0, transcendentals=0),
        name="first",
    )(own, other, w0)
    acc = pl.pallas_call(
        sides_body,
        out_shape=acc_shape,
        in_specs=in_vmem(5),
        out_specs=in_vmem(1)[0],
        input_output_aliases={4: 0},
        cost_estimate=pl.CostEstimate(flops=8 * rows * half * cols * 2, bytes_accessed=0, transcendentals=0),
        name="sides",
    )(own, other, wl, wr, acc)
    slots = pl.pallas_call(
        last_body,
        out_shape=tuple(shape(size, head_size) for _ in range(4)),
        in_specs=in_vmem(6),
        out_specs=tuple(in_vmem(4)),
        scratch_shapes=[pltpu.VMEM((size, cols), jnp.bfloat16)],
        cost_estimate=pl.CostEstimate(flops=4 * rows * half * cols * 2, bytes_accessed=0, transcendentals=0),
        name="last",
    )(own, other, wu, wd, acc, key_gain.reshape(1, head_size))

    def across(at):
        return at ^ 1

    mine = slots[0]
    p1 = moved_y(slots[1], step_to(1))
    p2 = moved_y(slots[2], step_to(2))
    p3 = moved_y(slots[3], step_to(3))
    f0 = moved_y(mine, across)
    f1 = moved_y(p1, across)
    f2 = moved_y(p2, across)
    f3 = moved_y(p3, across)
    t1 = swapped(jnp.concatenate((mine, f0, p1), 0))
    t2 = swapped(jnp.concatenate((p2, f1, f2, p3), 0))
    t3 = swapped(f3)
    key_line, value_line, first_out = pl.pallas_call(
        lambda *refs: read_body(*refs, size=size, scale=1.0 / head_size**0.5, chips=ny),
        out_shape=(
            shape(length, head_size),
            shape(length, head_size),
            shape(1, head_size),
        ),
        in_specs=in_vmem(15),
        out_specs=(
            pl.BlockSpec(memory_space=pl.ANY),
            pl.BlockSpec(memory_space=pl.ANY),
            pl.BlockSpec(memory_space=pltpu.VMEM),
        ),
        scratch_shapes=[
            pltpu.VMEM((length // 128, 128), jnp.float32),
            pltpu.VMEM((length // 128, 128), jnp.float32),
            pltpu.SemaphoreType.DMA((16,)),
        ],
        name="read",
    )(
        new_query[0],
        query_gain.reshape(1, head_size),
        out_gain.reshape(1, head_size),
        shift48,
        mine,
        f0,
        p1,
        p2,
        p3,
        f1,
        f2,
        f3,
        t1,
        t2,
        t3,
    )
    return (
        key_line.reshape(1, 1, length, head_size),
        value_line.reshape(1, 1, length, head_size),
        shift_line,
        first_out[None],
    )


def solution(mesh):
    placed = (
        P("sp", "tp", None),
        P(),
        P("sp", "tp"),
        P("sp", "tp"),
        P(),
        P("sp", None, "tp"),
        P("sp", "tp", None),
        P(),
        P(),
    )
    return jax.shard_map(
        shards,
        mesh=mesh,
        in_specs=placed,
        out_specs=(
            P("sp", "tp", None, None),
            P("sp", "tp", None, None),
            P("sp", "tp", None),
            P("sp", "tp", None),
        ),
        check_vma=False,
    )
```

time: 142 us -> 137 us (0.965)
  waiting for transfers between devices: 47 us -> 14.9 us
  blocking collectives: 0 us -> 28.6 us
  Pallas kernels: 14.2 us -> 26.3 us
  starting transfers between devices: 66.6 us -> 59.7 us
  local copies, waits for them, and re-layouts: 8.44 us -> 5.21 us
  other arithmetic: 3.18 us -> 0.09 us
    all_to_all x0 -> x1, blocking collectives: none -> 28.6 us  [shards(): lax.all_to_all(blocks, 'sp', split_axis=0, concat_axis=0, tiled=True, axi...]
    all_to_all x1 -> x0, starting transfers between devices: 13.3 us -> none  [shards(): lax.all_to_all(jnp.broadcast_to(own, (nz, *own.shape)), 'sp', split_axis=...]
    all_to_all x1, waiting for transfers between devices: 16.1 us -> 2.86 us  [shards(): recv = lax.all_to_all(sent, 'tp', split_axis=0, concat_axis=0, tiled=True)]
    pallas_call x3 -> x7, Pallas kernels: 14.2 us -> 26.3 us  [the longest x1 5.52 us: shards(): pl.pallas_call(lambda *refs: read_body(*refs, size=size, scale=1.0 / head...]
    ppermute x7, waiting for transfers between devices: 19.3 us -> 11 us  [moved_y(): lax.ppermute(x, 'tp', [(i, target(i // 2) % (n // 2) * 2 + i % 2) for i i...]
    all_to_all x1 -> x0, waiting for transfers between devices: 5.87 us -> none  [shards(): lax.all_to_all(jnp.broadcast_to(own, (nz, *own.shape)), 'sp', split_axis=...]
    ppermute x4, waiting for transfers between devices: 5.7 us -> 0.01 us  [moved_sp(): return lax.ppermute(x, 'sp', pairs)]
    ppermute x4, starting transfers between devices: 12.7 us -> 17 us  [swapped(): lax.ppermute(x, 'tp', [(i, i ^ 1) for i in range(lax.axis_size('tp'))])]
  transfers between devices with their start and end apart: 17 -> 16, of which waited for: 8 -> 5; matrix products, arithmetic and copies ran while one was open for 4% -> 1% of each run, Pallas kernels for 2% -> 11%
where the time goes in v2:
time: 137 us; the launch traced here: 136 us
  starting transfers between devices  59.7 us (44%)
  blocking collectives  28.6 us (21%)
  Pallas kernels  26.3 us (19%)
  waiting for transfers between devices  14.9 us (11%)
  local copies, waits for them, and re-layouts  5.21 us (4%)
    all_to_all x1, blocking collectives, shards(): lax.all_to_all(blocks, 'sp', split_axis=0, concat_axis=0, tiled=True, axi...  28.6 us
    ppermute x7, starting transfers between devices, moved_y(): lax.ppermute(x, 'tp', [(i, target(i // 2) % (n // 2) * 2 + i % 2) for i i...  20.7 us
    ppermute x4, starting transfers between devices, swapped(): lax.ppermute(x, 'tp', [(i, i ^ 1) for i in range(lax.axis_size('tp'))])  17 us
    ppermute x4, starting transfers between devices, moved_sp(): return lax.ppermute(x, 'sp', pairs)  11.8 us
    ppermute x7, waiting for transfers between devices, moved_y(): lax.ppermute(x, 'tp', [(i, target(i // 2) % (n // 2) * 2 + i % 2) for i i...  11 us
    all_to_all x1, starting transfers between devices, shards(): recv = lax.all_to_all(sent, 'tp', split_axis=0, concat_axis=0, tiled=True)  10.1 us
    pallas_call x1, Pallas kernels, shards(): pl.pallas_call(lambda *refs: read_body(*refs, size=size, scale=1.0 / head...  5.52 us
    pallas_call x1, Pallas kernels, shards(): pl.pallas_call(sides_body, out_shape=acc_shape, in_specs=in_vmem(5), out_...  4.83 us
  transfers between devices with their start and end apart: 16, of which 5 were waited for; matrix products, arithmetic and copies ran while one was open for 1% of the time, Pallas kernels for 11%

profile of v2, /device:TPU:1, one launch (start us, length us, event | category | flops | bytes accessed | tf_op | source)
XLA Modules:
  0.0 135.7 jit_solution(7680941632886044300)
XLA Ops:
  2.1 10.1 %all-to-all-start = ((bf16[16,32,128]{2,1,0:T(8,128)(2,1)}), bf16[16,32,128]{2,1,0:T(8,128)(2,1)S(1)}, u32[]{:S(2)}, u32[]{:S(2)}) async-start(bf16[16,32,128]{2,1,0:T(8,128)(2,1)} %pack.1), calls=%async_computation | async-start | bytes 262144 | tf_op jit(solution)/shard_map/all_to_all | solution.py:270
  12.2 4.2 %norm.1.own = bf16[384,2048]{1,0:T(8,128)(2,1)} custom-call(bf16[384,2048]{1,0:T(8,128)(2,1)} %bitcast.18, f32[1,2048]{1,0:T(1,128)} %bitcast.20), custom_call_target="tpu_custom_call" | custom-call | tf_op jit(solution)/shard_map/norm/pallas_call | solution.py:271
  16.4 2.1 %collective-permute-start = (bf16[384,2048]{1,0:T(8,128)(2,1)}, bf16[384,2048]{1,0:T(8,128)(2,1)S(1)}, u32[]{:S(2)}, u32[]{:S(2)}) collective-permute-start(bf16[384,2048]{1,0:T(8,128)(2,1)} %norm.1.own), channel_id=1, source_target_pairs={{0,1},{1,0},{2,3},{3,2},{4,5},{5,4},{6,7},{7,6},{8,9},{9,8},{10,11... | collective-permute-start | bytes 4718600 | tf_op jit(solution)/shard_map/ppermute | solution.py:40
  18.5 2.9 %all-to-all-done.recv = bf16[16,32,128]{2,1,0:T(8,128)(2,1)S(1)} async-done(((bf16[16,32,128]{2,1,0:T(8,128)(2,1)}), bf16[16,32,128]{2,1,0:T(8,128)(2,1)S(1)}, u32[]{:S(2)}, u32[]{:S(2)}) %all-to-all-start) | async-done | bytes 131104 | tf_op jit(solution)/shard_map/all_to_all | solution.py:270
  22.1 2.0 %build.1 = (bf16[8,64,512]{2,1,0:T(8,128)(2,1)}, f32[48,128]{1,0:T(8,128)}, bf16[1,1,6144]{2,1,0:T(2,128)(2,1)}) custom-call(bf16[16,32,128]{2,1,0:T(8,128)(2,1)} %copy-done.13), custom_call_target="tpu_custom_call" | custom-call | tf_op jit(solution)/shard_map/build/pallas_call | solution.py:283
  24.0 28.6 %all_to_all.10 = bf16[8,64,512]{2,1,0:T(8,128)(2,1)S(1)} all-to-all(bf16[8,64,512]{2,1,0:T(8,128)(2,1)} %get-tuple-element.15), channel_id=1, replica_groups={{0,96,128,224,256,352,384,480},{16,112,144,240,272,368,400,496},{32,64,..., dimensions={0} | all-to-all | bytes 1048576 | tf_op jit(solution)/shard_map/all_to_all | solution.py:300
  54.6 3.4 %collective-permute-start.3 = (bf16[512,512]{1,0:T(8,128)(2,1)S(1)}, bf16[512,512]{1,0:T(8,128)(2,1)S(1)}, u32[]{:S(2)}, u32[]{:S(2)}) collective-permute-start(bf16[512,512]{1,0:T(8,128)(2,1)S(1)} %bitcast.16), channel_id=1, source_target_pairs={{0,16},{16,32},{32,48},{48,0},{64,80},{80,96},{96,112},{112,64},{1... | collective-permute-start | bytes 1572872 | tf_op jit(solution)/shard_map/ppermute | solution.py:29
  58.7 2.0 %collective-permute-start.1 = (bf16[256,512]{1,0:T(8,128)(2,1)}, bf16[256,512]{1,0:T(8,128)(2,1)}, u32[]{:S(2)}, u32[]{:S(2)}) collective-permute-start(bf16[256,512]{1,0:T(8,128)(2,1)} %bitcast.8), channel_id=1, source_target_pairs={{0,64},{16,80},{32,96},{48,112},{64,128},{80,144},{96,160},{112,17... | collective-permute-start | bytes 786440 | tf_op jit(solution)/shard_map/ppermute | solution.py:29
  60.7 4.5 %collective-permute-start.2 = (bf16[256,512]{1,0:T(8,128)(2,1)S(1)}, bf16[256,512]{1,0:T(8,128)(2,1)}, u32[]{:S(2)}, u32[]{:S(2)}) collective-permute-start(bf16[256,512]{1,0:T(8,128)(2,1)S(1)} %bitcast.19), channel_id=1, source_target_pairs={{0,448},{16,464},{32,480},{48,496},{64,0},{80,16},{96,32},{112,48}... | collective-permute-start | bytes 786440 | tf_op jit(solution)/shard_map/ppermute | solution.py:29
  66.4 3.7 %first.1.acc = f32[2,384,512]{2,1,0:T(8,128)} custom-call(bf16[384,2048]{1,0:T(8,128)(2,1)} %norm.1.own, bf16[384,2048]{1,0:T(8,128)(2,1)} %copy-done, bf16[512,512]{1,0:T(8,128)(2,1)} %bitcast.17), custom_call_target="tpu_custom_call" | custom-call | flops 402653184 | tf_op jit(solution)/shard_map/first/pallas_call | solution.py:310
  71.7 4.8 %sides.1.acc = f32[2,384,512]{2,1,0:T(8,128)} custom-call(bf16[384,2048]{1,0:T(8,128)(2,1)} %norm.1.own, bf16[384,2048]{1,0:T(8,128)(2,1)} %copy-done, bf16[512,512]{1,0:T(8,128)(2,1)} %copy-done.12, bf16[512,512]{1,0:T(8,128)(2,1)} %copy-done.11, f32[2,384,512]{2,1,0:T(8,128)} %first.1.acc), custom_call_target="tpu_custom_call", output_to_operand_aliasing={{}: (4, {})} | custom-call | flops 805306368 | tf_op jit(solution)/shard_map/sides/pallas_call | solution.py:318
  76.5 4.5 %last.1 = (bf16[768,128]{1,0:T(8,128)(2,1)}, bf16[768,128]{1,0:T(8,128)(2,1)}, bf16[768,128]{1,0:T(8,128)(2,1)}, bf16[768,128]{1,0:T(8,128)(2,1)}) custom-call(bf16[384,2048]{1,0:T(8,128)(2,1)} %norm.1.own, bf16[384,2048]{1,0:T(8,128)(2,1)} %copy-done, bf16[256,512]{1,0:T(8,128)(2,1)} %collective-permute-done.1.wu, ...), custom_call_target="tpu_custom_call" | custom-call | flops 402653184 | tf_op jit(solution)/shard_map/last/pallas_call | solution.py:327
  81.1 2.1 %collective-permute-start.6 = (bf16[768,128]{1,0:T(8,128)(2,1)}, bf16[768,128]{1,0:T(8,128)(2,1)S(1)}, u32[]{:S(2)}, u32[]{:S(2)}) collective-permute-start(bf16[768,128]{1,0:T(8,128)(2,1)} %get-tuple-element.17), channel_id=1, source_target_pairs={{0,14},{1,15},{2,4},{3,5},{4,2},{5,3},{6,8},{7,9},{8,6},{9,7},{10,... | collective-permute-start | bytes 589832 | tf_op jit(solution)/shard_map/ppermute | solution.py:34
  83.2 3.2 %collective-permute-start.7 = (bf16[768,128]{1,0:T(8,128)(2,1)}, bf16[768,128]{1,0:T(8,128)(2,1)S(1)}, u32[]{:S(2)}, u32[]{:S(2)}) collective-permute-start(bf16[768,128]{1,0:T(8,128)(2,1)} %get-tuple-element.18), channel_id=1, source_target_pairs={{0,4},{1,5},{2,14},{3,15},{4,8},{5,9},{6,2},{7,3},{8,12},{9,13},{1... | collective-permute-start | bytes 589832 | tf_op jit(solution)/shard_map/ppermute | solution.py:34
  86.5 5.9 %collective-permute-start.8 = (bf16[768,128]{1,0:T(8,128)(2,1)}, bf16[768,128]{1,0:T(8,128)(2,1)S(1)}, u32[]{:S(2)}, u32[]{:S(2)}) collective-permute-start(bf16[768,128]{1,0:T(8,128)(2,1)} %get-tuple-element.19), channel_id=1, source_target_pairs={{0,10},{1,11},{2,8},{3,9},{4,14},{5,15},{6,12},{7,13},{8,2},{9,3},... | collective-permute-start | bytes 589832 | tf_op jit(solution)/shard_map/ppermute | solution.py:34
  94.4 3.4 %collective-permute-start.10 = (bf16[768,128]{1,0:T(8,128)(2,1)S(1)}, bf16[768,128]{1,0:T(8,128)(2,1)S(1)}, u32[]{:S(2)}, u32[]{:S(2)}) collective-permute-start(bf16[768,128]{1,0:T(8,128)(2,1)S(1)} %collective-permute-done.7.refs_7_), channel_id=1, source_target_pairs={{0,2},{1,3},{2,0},{3,1},{4,6},{5,7},{6,4},{7,5},{8,10},{9,11},{10,... | collective-permute-start | bytes 589832 | tf_op jit(solution)/shard_map/ppermute | solution.py:34
  99.7 2.5 %collective-permute-done.8.refs_8_ = bf16[768,128]{1,0:T(8,128)(2,1)S(1)} collective-permute-done((bf16[768,128]{1,0:T(8,128)(2,1)}, bf16[768,128]{1,0:T(8,128)(2,1)S(1)}, u32[]{:S(2)}, u32[]{:S(2)}) %collective-permute-start.8) | collective-permute-done | bytes 196640 | tf_op jit(solution)/shard_map/ppermute | solution.py:34
  102.2 2.4 %collective-permute-done.10.refs_10_ = bf16[768,128]{1,0:T(8,128)(2,1)S(1)} collective-permute-done((bf16[768,128]{1,0:T(8,128)(2,1)S(1)}, bf16[768,128]{1,0:T(8,128)(2,1)S(1)}, u32[]{:S(2)}, u32[]{:S(2)}) %collective-permute-start.10) | collective-permute-done | bytes 196640 | tf_op jit(solution)/shard_map/ppermute | solution.py:34
  104.6 8.3 %collective-permute-start.13 = (bf16[3072,128]{1,0:T(8,128)(2,1)S(1)}, bf16[3072,128]{1,0:T(8,128)(2,1)S(1)}, u32[]{:S(2)}, u32[]{:S(2)}) collective-permute-start(bf16[3072,128]{1,0:T(8,128)(2,1)S(1)} %pad_maximum_fusion), channel_id=1, source_target_pairs={{0,1},{1,0},{2,3},{3,2},{4,5},{5,4},{6,7},{7,6},{8,9},{9,8},{10,11... | collective-permute-start | bytes 2359304 | tf_op jit(solution)/shard_map/ppermute | solution.py:40
  113.0 3.9 %collective-permute-start.12 = (bf16[2304,128]{1,0:T(8,128)(2,1)S(1)}, bf16[2304,128]{1,0:T(8,128)(2,1)S(1)}, u32[]{:S(2)}, u32[]{:S(2)}) collective-permute-start(bf16[2304,128]{1,0:T(8,128)(2,1)S(1)} %pad_maximum_fusion.1), channel_id=1, source_target_pairs={{0,1},{1,0},{2,3},{3,2},{4,5},{5,4},{6,7},{7,6},{8,9},{9,8},{10,11... | collective-permute-start | bytes 1769480 | tf_op jit(solution)/shard_map/ppermute | solution.py:40
  116.9 2.2 %collective-permute-start.11 = (bf16[768,128]{1,0:T(8,128)(2,1)S(1)}, bf16[768,128]{1,0:T(8,128)(2,1)S(1)}, u32[]{:S(2)}, u32[]{:S(2)}) collective-permute-start(bf16[768,128]{1,0:T(8,128)(2,1)S(1)} %collective-permute-done.8.refs_8_), channel_id=1, source_target_pairs={{0,2},{1,3},{2,0},{3,1},{4,6},{5,7},{6,4},{7,5},{8,10},{9,11},{10,... | collective-permute-start | bytes 589832 | tf_op jit(solution)/shard_map/ppermute | solution.py:34
  119.1 6.1 %collective-permute-done.11.refs_11_ = bf16[768,128]{1,0:T(8,128)(2,1)S(1)} collective-permute-done((bf16[768,128]{1,0:T(8,128)(2,1)S(1)}, bf16[768,128]{1,0:T(8,128)(2,1)S(1)}, u32[]{:S(2)}, u32[]{:S(2)}) %collective-permute-start.11) | collective-permute-done | bytes 196640 | tf_op jit(solution)/shard_map/ppermute | solution.py:34
  125.2 2.8 %collective-permute-start.14 = (bf16[768,128]{1,0:T(8,128)(2,1)S(1)}, bf16[768,128]{1,0:T(8,128)(2,1)S(1)}, u32[]{:S(2)}, u32[]{:S(2)}) collective-permute-start(bf16[768,128]{1,0:T(8,128)(2,1)S(1)} %collective-permute-done.11.refs_11_), channel_id=1, source_target_pairs={{0,1},{1,0},{2,3},{3,2},{4,5},{5,4},{6,7},{7,6},{8,9},{9,8},{10,11... | collective-permute-start | bytes 589832 | tf_op jit(solution)/shard_map/ppermute | solution.py:40
  130.2 5.5 %read.1 = (bf16[6144,128]{1,0:T(8,128)(2,1)}, bf16[6144,128]{1,0:T(8,128)(2,1)}, bf16[1,128]{1,0:T(2,128)(2,1)}) custom-call(bf16[1,128]{1,0:T(2,128)(2,1)} %bitcast.24, f32[1,128]{1,0:T(1,128)} %bitcast.25, f32[1,128]{1,0:T(1,128)} %bitcast.26, f32[48,128]{1,0:T(8,128)} %get-tuple-element.14.refs_3_, bf16[768,128]{1,0:T(8,128)(2,1)} %get-tuple-element.16.refs_4_, ...), custom_call_target="tpu_custom_call" | custom-call | tf_op jit(solution)/shard_map/read/pallas_call | solution.py:351
  (51 shorter events, 13.6 us)
Async XLA Ops:
  2.1 19.3 %all-to-all-start = ((bf16[16,32,128]{2,1,0:T(8,128)(2,1)}), bf16[16,32,128]{2,1,0:T(8,128)(2,1)S(1)}, u32[]{:S(2)}, u32[]{:S(2)}) async-start(bf16[16,32,128]{2,1,0:T(8,128)(2,1)} %pack.1), calls=%async_computation | async-start | bytes 262144 | tf_op jit(solution)/shard_map/all_to_all | solution.py:270
  16.4 48.8 %collective-permute-start = (bf16[384,2048]{1,0:T(8,128)(2,1)}, bf16[384,2048]{1,0:T(8,128)(2,1)S(1)}, u32[]{:S(2)}, u32[]{:S(2)}) collective-permute-start(bf16[384,2048]{1,0:T(8,128)(2,1)} %norm.1.own), channel_id=1, source_target_pairs={{0,1},{1,0},{2,3},{3,2},{4,5},{5,4},{6,7},{7,6},{8,9},{9,8},{10,11... | collective-permute-start | bytes 4718600 | tf_op jit(solution)/shard_map/ppermute | solution.py:40
  52.7 12.5 %copy-start.1 = (bf16[8,64,512]{2,1,0:T(8,128)(2,1)}, bf16[8,64,512]{2,1,0:T(8,128)(2,1)S(1)}, u32[]{:S(2)}) copy-start(bf16[8,64,512]{2,1,0:T(8,128)(2,1)S(1)} %all_to_all.10) | copy-start | bytes 1572868
  52.7 17.4 %collective-permute-start.4 = (bf16[512,512]{1,0:T(8,128)(2,1)S(1)}, bf16[512,512]{1,0:T(8,128)(2,1)S(1)}, u32[]{:S(2)}, u32[]{:S(2)}) collective-permute-start(bf16[512,512]{1,0:T(8,128)(2,1)S(1)} %bitcast.15), channel_id=1, source_target_pairs={{0,48},{16,0},{32,16},{48,32},{64,112},{80,64},{96,80},{112,96},{1... | collective-permute-start | bytes 1572872 | tf_op jit(solution)/shard_map/ppermute | solution.py:29
  54.6 15.5 %collective-permute-start.3 = (bf16[512,512]{1,0:T(8,128)(2,1)S(1)}, bf16[512,512]{1,0:T(8,128)(2,1)S(1)}, u32[]{:S(2)}, u32[]{:S(2)}) collective-permute-start(bf16[512,512]{1,0:T(8,128)(2,1)S(1)} %bitcast.16), channel_id=1, source_target_pairs={{0,16},{16,32},{32,48},{48,0},{64,80},{80,96},{96,112},{112,64},{1... | collective-permute-start | bytes 1572872 | tf_op jit(solution)/shard_map/ppermute | solution.py:29
  58.7 17.8 %collective-permute-start.1 = (bf16[256,512]{1,0:T(8,128)(2,1)}, bf16[256,512]{1,0:T(8,128)(2,1)}, u32[]{:S(2)}, u32[]{:S(2)}) collective-permute-start(bf16[256,512]{1,0:T(8,128)(2,1)} %bitcast.8), channel_id=1, source_target_pairs={{0,64},{16,80},{32,96},{48,112},{64,128},{80,144},{96,160},{112,17... | collective-permute-start | bytes 786440 | tf_op jit(solution)/shard_map/ppermute | solution.py:29
  60.7 15.9 %collective-permute-start.2 = (bf16[256,512]{1,0:T(8,128)(2,1)S(1)}, bf16[256,512]{1,0:T(8,128)(2,1)}, u32[]{:S(2)}, u32[]{:S(2)}) collective-permute-start(bf16[256,512]{1,0:T(8,128)(2,1)S(1)} %bitcast.19), channel_id=1, source_target_pairs={{0,448},{16,464},{32,480},{48,496},{64,0},{80,16},{96,32},{112,48}... | collective-permute-start | bytes 786440 | tf_op jit(solution)/shard_map/ppermute | solution.py:29
  81.1 31.8 %copy-start.2 = (bf16[768,128]{1,0:T(8,128)(2,1)S(1)}, bf16[768,128]{1,0:T(8,128)(2,1)}, u32[]{:S(2)}) copy-start(bf16[768,128]{1,0:T(8,128)(2,1)} %get-tuple-element.16.refs_4_) | copy-start | bytes 589828
  81.1 11.3 %collective-permute-start.6 = (bf16[768,128]{1,0:T(8,128)(2,1)}, bf16[768,128]{1,0:T(8,128)(2,1)S(1)}, u32[]{:S(2)}, u32[]{:S(2)}) collective-permute-start(bf16[768,128]{1,0:T(8,128)(2,1)} %get-tuple-element.17), channel_id=1, source_target_pairs={{0,14},{1,15},{2,4},{3,5},{4,2},{5,3},{6,8},{7,9},{8,6},{9,7},{10,... | collective-permute-start | bytes 589832 | tf_op jit(solution)/shard_map/ppermute | solution.py:34
  83.2 11.1 %collective-permute-start.7 = (bf16[768,128]{1,0:T(8,128)(2,1)}, bf16[768,128]{1,0:T(8,128)(2,1)S(1)}, u32[]{:S(2)}, u32[]{:S(2)}) collective-permute-start(bf16[768,128]{1,0:T(8,128)(2,1)} %get-tuple-element.18), channel_id=1, source_target_pairs={{0,4},{1,5},{2,14},{3,15},{4,8},{5,9},{6,2},{7,3},{8,12},{9,13},{1... | collective-permute-start | bytes 589832 | tf_op jit(solution)/shard_map/ppermute | solution.py:34
  86.5 15.7 %collective-permute-start.8 = (bf16[768,128]{1,0:T(8,128)(2,1)}, bf16[768,128]{1,0:T(8,128)(2,1)S(1)}, u32[]{:S(2)}, u32[]{:S(2)}) collective-permute-start(bf16[768,128]{1,0:T(8,128)(2,1)} %get-tuple-element.19), channel_id=1, source_target_pairs={{0,10},{1,11},{2,8},{3,9},{4,14},{5,15},{6,12},{7,13},{8,2},{9,3},... | collective-permute-start | bytes 589832 | tf_op jit(solution)/shard_map/ppermute | solution.py:34
  92.4 36.6 %copy-start.3 = (bf16[768,128]{1,0:T(8,128)(2,1)}, bf16[768,128]{1,0:T(8,128)(2,1)S(1)}, u32[]{:S(2)}) copy-start(bf16[768,128]{1,0:T(8,128)(2,1)S(1)} %collective-permute-done.6.refs_6_) | copy-start | bytes 589828
  92.4 9.8 %collective-permute-start.9 = (bf16[768,128]{1,0:T(8,128)(2,1)S(1)}, bf16[768,128]{1,0:T(8,128)(2,1)S(1)}, u32[]{:S(2)}, u32[]{:S(2)}) collective-permute-start(bf16[768,128]{1,0:T(8,128)(2,1)S(1)} %collective-permute-done.6.refs_6_), channel_id=1, source_target_pairs={{0,2},{1,3},{2,0},{3,1},{4,6},{5,7},{6,4},{7,5},{8,10},{9,11},{10,... | collective-permute-start | bytes 589832 | tf_op jit(solution)/shard_map/ppermute | solution.py:34
  94.4 34.7 %copy-start.4 = (bf16[768,128]{1,0:T(8,128)(2,1)}, bf16[768,128]{1,0:T(8,128)(2,1)S(1)}, u32[]{:S(2)}) copy-start(bf16[768,128]{1,0:T(8,128)(2,1)S(1)} %collective-permute-done.7.refs_7_) | copy-start | bytes 589828
  94.4 10.2 %collective-permute-start.10 = (bf16[768,128]{1,0:T(8,128)(2,1)S(1)}, bf16[768,128]{1,0:T(8,128)(2,1)S(1)}, u32[]{:S(2)}, u32[]{:S(2)}) collective-permute-start(bf16[768,128]{1,0:T(8,128)(2,1)S(1)} %collective-permute-done.7.refs_7_), channel_id=1, source_target_pairs={{0,2},{1,3},{2,0},{3,1},{4,6},{5,7},{6,4},{7,5},{8,10},{9,11},{10,... | collective-permute-start | bytes 589832 | tf_op jit(solution)/shard_map/ppermute | solution.py:34
  97.8 15.1 %collective-permute-start.5 = (bf16[768,128]{1,0:T(8,128)(2,1)}, bf16[768,128]{1,0:T(8,128)(2,1)S(1)}, u32[]{:S(2)}, u32[]{:S(2)}) collective-permute-start(bf16[768,128]{1,0:T(8,128)(2,1)} %get-tuple-element.16.refs_4_), channel_id=1, source_target_pairs={{0,2},{1,3},{2,0},{3,1},{4,6},{5,7},{6,4},{7,5},{8,10},{9,11},{10,... | collective-permute-start | bytes 589832 | tf_op jit(solution)/shard_map/ppermute | solution.py:34
  102.2 26.9 %copy-start.5 = (bf16[768,128]{1,0:T(8,128)(2,1)}, bf16[768,128]{1,0:T(8,128)(2,1)S(1)}, u32[]{:S(2)}) copy-start(bf16[768,128]{1,0:T(8,128)(2,1)S(1)} %collective-permute-done.8.refs_8_) | copy-start | bytes 589828
  102.2 26.9 %copy-start.6 = (bf16[768,128]{1,0:T(8,128)(2,1)}, bf16[768,128]{1,0:T(8,128)(2,1)S(1)}, u32[]{:S(2)}) copy-start(bf16[768,128]{1,0:T(8,128)(2,1)S(1)} %collective-permute-done.9.refs_9_) | copy-start | bytes 589828
  104.6 24.5 %copy-start.7 = (bf16[768,128]{1,0:T(8,128)(2,1)}, bf16[768,128]{1,0:T(8,128)(2,1)S(1)}, u32[]{:S(2)}) copy-start(bf16[768,128]{1,0:T(8,128)(2,1)S(1)} %collective-permute-done.10.refs_10_) | copy-start | bytes 589828
  104.6 24.4 %collective-permute-start.13 = (bf16[3072,128]{1,0:T(8,128)(2,1)S(1)}, bf16[3072,128]{1,0:T(8,128)(2,1)S(1)}, u32[]{:S(2)}, u32[]{:S(2)}) collective-permute-start(bf16[3072,128]{1,0:T(8,128)(2,1)S(1)} %pad_maximum_fusion), channel_id=1, source_target_pairs={{0,1},{1,0},{2,3},{3,2},{4,5},{5,4},{6,7},{7,6},{8,9},{9,8},{10,11... | collective-permute-start | bytes 2359304 | tf_op jit(solution)/shard_map/ppermute | solution.py:40
  112.9 16.2 %copy-start.8 = (bf16[768,128]{1,0:T(8,128)(2,1)}, bf16[768,128]{1,0:T(8,128)(2,1)S(1)}, u32[]{:S(2)}) copy-start(bf16[768,128]{1,0:T(8,128)(2,1)S(1)} %collective-permute-done.5.refs_5_) | copy-start | bytes 589828
  113.0 16.1 %collective-permute-start.12 = (bf16[2304,128]{1,0:T(8,128)(2,1)S(1)}, bf16[2304,128]{1,0:T(8,128)(2,1)S(1)}, u32[]{:S(2)}, u32[]{:S(2)}) collective-permute-start(bf16[2304,128]{1,0:T(8,128)(2,1)S(1)} %pad_maximum_fusion.1), channel_id=1, source_target_pairs={{0,1},{1,0},{2,3},{3,2},{4,5},{5,4},{6,7},{7,6},{8,9},{9,8},{10,11... | collective-permute-start | bytes 1769480 | tf_op jit(solution)/shard_map/ppermute | solution.py:40
  116.9 8.3 %collective-permute-start.11 = (bf16[768,128]{1,0:T(8,128)(2,1)S(1)}, bf16[768,128]{1,0:T(8,128)(2,1)S(1)}, u32[]{:S(2)}, u32[]{:S(2)}) collective-permute-start(bf16[768,128]{1,0:T(8,128)(2,1)S(1)} %collective-permute-done.8.refs_8_), channel_id=1, source_target_pairs={{0,2},{1,3},{2,0},{3,1},{4,6},{5,7},{6,4},{7,5},{8,10},{9,11},{10,... | collective-permute-start | bytes 589832 | tf_op jit(solution)/shard_map/ppermute | solution.py:34
  125.2 3.8 %collective-permute-start.14 = (bf16[768,128]{1,0:T(8,128)(2,1)S(1)}, bf16[768,128]{1,0:T(8,128)(2,1)S(1)}, u32[]{:S(2)}, u32[]{:S(2)}) collective-permute-start(bf16[768,128]{1,0:T(8,128)(2,1)S(1)} %collective-permute-done.11.refs_11_), channel_id=1, source_target_pairs={{0,1},{1,0},{2,3},{3,2},{4,5},{5,4},{6,7},{7,6},{8,9},{9,8},{10,11... | collective-permute-start | bytes 589832 | tf_op jit(solution)/shard_map/ppermute | solution.py:40
  (8 other events, 10.0 us)

commit v3 on v2

--- a/solution.py
+++ b/solution.py
@@ -9,6 +9,7 @@
 NX = 4
 CLASSES = 4
 epsilon = 1e-06
+MIB = 1 << 20
 
 
 def row_norm(value_entries, scaling):
@@ -150,10 +151,9 @@
 
 
 def read_body(query, query_gain, out_gain, shift, *rest, size, scale, chips):
-    mine, theirs = rest[:8], rest[8:11]
-    keys, values, first = rest[11:14]
-    score_ref, weight_ref, sems = rest[14:]
-    theirs_of = [(0, 0), (0, 1), (0, 2), (1, 0), (1, 3), (1, 1), (1, 2), (2, 0)]
+    mine, theirs = rest[:8], rest[8:10]
+    keys, values, first = rest[10:13]
+    score_ref, weight_ref, sems = rest[13:]
     per = size // 128
     blocks = chips * per
     y, core = chip_and_core()
@@ -163,8 +163,7 @@
     sources = [lax.rem(s + chips, chips) for s in sources]
 
     def their(j):
-        part, at = theirs_of[j]
-        return theirs[part].at[pl.ds(at * size, size), :]
+        return theirs[0].at[pl.ds(j * size, size), :] if j < 7 else theirs[1]
 
     q = row_norm(query[...].astype(jnp.float32), query_gain[...]).astype(jnp.bfloat16)
     rows = lax.broadcasted_iota(jnp.int32, (128, 128), 0)
@@ -265,21 +264,10 @@
         out_shape=shape(groups, 32, 128),
         in_specs=in_vmem(3),
         out_specs=in_vmem(1)[0],
+        compiler_params=pltpu.CompilerParams(vmem_limit_bytes=4 * MIB),
         name="pack",
     )(key_weight.T, value_weight.T, stop_shift[0])
     recv = lax.all_to_all(sent, "tp", split_axis=0, concat_axis=0, tiled=True)
-    own = pl.pallas_call(
-        norm_body,
-        grid=(4,),
-        out_shape=shape(rows, width),
-        in_specs=[
-            pl.BlockSpec((rows // 4, width), lambda i: (i, 0)),
-            pl.BlockSpec((1, width), lambda i: (0, 0)),
-        ],
-        out_specs=pl.BlockSpec((rows // 4, width), lambda i: (i, 0)),
-        name="norm",
-    )(layer_input[0], input_gain.reshape(1, width))
-    other = swapped(own)
     blocks, shift48, shift_line = pl.pallas_call(
         build_body,
         out_shape=(
@@ -293,8 +281,23 @@
             pltpu.VMEM((cols, deep), jnp.bfloat16),
             pltpu.VMEM((length // 128, 128), jnp.float32),
         ],
+        compiler_params=pltpu.CompilerParams(vmem_limit_bytes=8 * MIB),
         name="build",
     )(recv)
+
+    own = pl.pallas_call(
+        norm_body,
+        grid=(4,),
+        out_shape=shape(rows, width),
+        in_specs=[
+            pl.BlockSpec((rows // 4, width), lambda i: (i, 0)),
+            pl.BlockSpec((1, width), lambda i: (0, 0)),
+        ],
+        out_specs=pl.BlockSpec((rows // 4, width), lambda i: (i, 0)),
+        compiler_params=pltpu.CompilerParams(vmem_limit_bytes=16 * MIB),
+        name="norm",
+    )(layer_input[0], input_gain.reshape(1, width))
+    other = swapped(own)
 
     classes = [[z * NX + (c + 2 * z) % NX for z in range(nz)] for c in range(CLASSES)]
     got = lax.all_to_all(
@@ -313,6 +316,7 @@
         in_specs=in_vmem(3),
         out_specs=in_vmem(1)[0],
         cost_estimate=pl.CostEstimate(flops=4 * rows * half * cols * 2, bytes_accessed=0, transcendentals=0),
+        compiler_params=pltpu.CompilerParams(vmem_limit_bytes=16 * MIB),
         name="first",
     )(own, other, w0)
     acc = pl.pallas_call(
@@ -322,6 +326,7 @@
         out_specs=in_vmem(1)[0],
         input_output_aliases={4: 0},
         cost_estimate=pl.CostEstimate(flops=8 * rows * half * cols * 2, bytes_accessed=0, transcendentals=0),
+        compiler_params=pltpu.CompilerParams(vmem_limit_bytes=16 * MIB),
         name="sides",
     )(own, other, wl, wr, acc)
     slots = pl.pallas_call(
@@ -331,6 +336,7 @@
         out_specs=tuple(in_vmem(4)),
         scratch_shapes=[pltpu.VMEM((size, cols), jnp.bfloat16)],
         cost_estimate=pl.CostEstimate(flops=4 * rows * half * cols * 2, bytes_accessed=0, transcendentals=0),
+        compiler_params=pltpu.CompilerParams(vmem_limit_bytes=20 * MIB),
         name="last",
     )(own, other, wu, wd, acc, key_gain.reshape(1, head_size))
 
@@ -345,9 +351,8 @@
     f1 = moved_y(p1, across)
     f2 = moved_y(p2, across)
     f3 = moved_y(p3, across)
-    t1 = swapped(jnp.concatenate((mine, f0, p1), 0))
-    t2 = swapped(jnp.concatenate((p2, f1, f2, p3), 0))
-    t3 = swapped(f3)
+    t1 = swapped(jnp.concatenate((mine, f0, p1, p2, p3, f1, f2), 0))
+    t2 = swapped(f3)
     key_line, value_line, first_out = pl.pallas_call(
         lambda *refs: read_body(*refs, size=size, scale=1.0 / head_size**0.5, chips=ny),
         out_shape=(
@@ -355,7 +360,7 @@
             shape(length, head_size),
             shape(1, head_size),
         ),
-        in_specs=in_vmem(15),
+        in_specs=in_vmem(14),
         out_specs=(
             pl.BlockSpec(memory_space=pl.ANY),
             pl.BlockSpec(memory_space=pl.ANY),
@@ -366,6 +371,7 @@
             pltpu.VMEM((length // 128, 128), jnp.float32),
             pltpu.SemaphoreType.DMA((16,)),
         ],
+        compiler_params=pltpu.CompilerParams(vmem_limit_bytes=24 * MIB),
         name="read",
     )(
         new_query[0],
@@ -382,7 +388,6 @@
         f3,
         t1,
         t2,
-        t3,
     )
     return (
         key_line.reshape(1, 1, length, head_size),

time: 137 us -> 120 us (0.88)
  Pallas kernels: 26.3 us -> 9.48 us
  waiting for transfers between devices: 14.9 us -> 24.7 us
  starting transfers between devices: 59.7 us -> 51.5 us
    ppermute x4 -> x3, starting transfers between devices: 17 us -> 9.42 us  [swapped(): lax.ppermute(x, 'tp', [(i, i ^ 1) for i in range(lax.axis_size('tp'))])]
    ppermute x7, waiting for transfers between devices: 11 us -> 15.7 us  [moved_y(): lax.ppermute(x, 'tp', [(i, target(i // 2) % (n // 2) * 2 + i % 2) for i i...]
    ppermute x4, waiting for transfers between devices: 0.01 us -> 4.48 us  [moved_sp(): return lax.ppermute(x, 'sp', pairs)]
    pallas_call x1, Pallas kernels: 4.83 us -> 1.03 us  [shards(): pl.pallas_call(sides_body, out_shape=acc_shape, in_specs=in_vmem(5), out_...]
    pallas_call x1, Pallas kernels: 4.55 us -> 1.11 us  [shards(): pl.pallas_call(last_body, out_shape=tuple((shape(size, head_size) for _ i...]
    pallas_call x1, Pallas kernels: 3.73 us -> 0.56 us  [shards(): pl.pallas_call(first_body, out_shape=acc_shape, in_specs=in_vmem(3), out_...]
    pallas_call x1, Pallas kernels: 4.2 us -> 1.39 us  [shards(): pl.pallas_call(norm_body, grid=(4,), out_shape=shape(rows, width), in_spe...]
    pallas_call x1, Pallas kernels: 5.52 us -> 3.87 us  [shards(): pl.pallas_call(lambda *refs: read_body(*refs, size=size, scale=1.0 / head...]
  transfers between devices with their start and end apart: 16 -> 15, of which waited for: 5 -> 7; matrix products, arithmetic and copies ran while one was open for 1% -> 0% of each run, Pallas kernels for 11% -> 3%
where the time goes in v3:
time: 120 us; the launch traced here: 119 us
  starting transfers between devices  51.5 us (43%)
  blocking collectives  28.4 us (24%)
  waiting for transfers between devices  24.7 us (21%)
  Pallas kernels  9.48 us (8%)
  local copies, waits for them, and re-layouts  4.41 us (4%)
    all_to_all x1, blocking collectives, shards(): lax.all_to_all(blocks, 'sp', split_axis=0, concat_axis=0, tiled=True, axi...  28.4 us
    ppermute x7, starting transfers between devices, moved_y(): lax.ppermute(x, 'tp', [(i, target(i // 2) % (n // 2) * 2 + i % 2) for i i...  20.2 us
    ppermute x7, waiting for transfers between devices, moved_y(): lax.ppermute(x, 'tp', [(i, target(i // 2) % (n // 2) * 2 + i % 2) for i i...  15.7 us
    ppermute x4, starting transfers between devices, moved_sp(): return lax.ppermute(x, 'sp', pairs)  11.8 us
    all_to_all x1, starting transfers between devices, shards(): recv = lax.all_to_all(sent, 'tp', split_axis=0, concat_axis=0, tiled=True)  10.1 us
    ppermute x3, starting transfers between devices, swapped(): lax.ppermute(x, 'tp', [(i, i ^ 1) for i in range(lax.axis_size('tp'))])  9.42 us
    ppermute x4, waiting for transfers between devices, moved_sp(): return lax.ppermute(x, 'sp', pairs)  4.48 us
    unnamed x24, local copies, waits for them, and re-layouts  4.35 us
  transfers between devices with their start and end apart: 15, of which 7 were waited for; matrix products, arithmetic and copies ran while one was open for 0% of the time, Pallas kernels for 3%

profile of v3, /device:TPU:1, one launch (start us, length us, event | category | flops | bytes accessed | tf_op | source)
XLA Modules:
  0.0 119.5 jit_solution(14786028124790865002)
XLA Ops:
  3.4 10.1 %all-to-all-start = ((bf16[16,32,128]{2,1,0:T(8,128)(2,1)}), bf16[16,32,128]{2,1,0:T(8,128)(2,1)S(1)}, u32[]{:S(2)}, u32[]{:S(2)}) async-start(bf16[16,32,128]{2,1,0:T(8,128)(2,1)} %pack.1), calls=%async_computation | async-start | bytes 262144 | tf_op jit(solution)/shard_map/all_to_all | solution.py:270
  13.6 1.4 %copy-done = bf16[1,384,2048]{2,1,0:T(8,128)(2,1)S(1)} copy-done((bf16[1,384,2048]{2,1,0:T(8,128)(2,1)S(1)}, bf16[1,384,2048]{2,1,0:T(8,128)(2,1)}, u32[]{:S(2)}) %copy-start) | copy-done | bytes 1572888
  17.1 2.1 %collective-permute-start = (bf16[384,2048]{1,0:T(8,128)(2,1)S(1)}, bf16[384,2048]{1,0:T(8,128)(2,1)S(1)}, u32[]{:S(2)}, u32[]{:S(2)}) collective-permute-start(bf16[384,2048]{1,0:T(8,128)(2,1)S(1)} %norm.1.own), channel_id=1, source_target_pairs={{0,1},{1,0},{2,3},{3,2},{4,5},{5,4},{6,7},{7,6},{8,9},{9,8},{10,11... | collective-permute-start | bytes 4718600 | tf_op jit(solution)/shard_map/ppermute | solution.py:41
  19.2 3.5 %all-to-all-done.recv = bf16[16,32,128]{2,1,0:T(8,128)(2,1)S(1)} async-done(((bf16[16,32,128]{2,1,0:T(8,128)(2,1)}), bf16[16,32,128]{2,1,0:T(8,128)(2,1)S(1)}, u32[]{:S(2)}, u32[]{:S(2)}) %all-to-all-start) | async-done | bytes 131104 | tf_op jit(solution)/shard_map/all_to_all | solution.py:270
  23.5 28.4 %all_to_all.10 = bf16[8,64,512]{2,1,0:T(8,128)(2,1)S(1)} all-to-all(bf16[8,64,512]{2,1,0:T(8,128)(2,1)S(1)} %get-tuple-element.15), channel_id=1, replica_groups={{0,96,128,224,256,352,384,480},{16,112,144,240,272,368,400,496},{32,64,..., dimensions={0} | all-to-all | bytes 1048576 | tf_op jit(solution)/shard_map/all_to_all | solution.py:303
  52.0 1.9 %collective-permute-start.4 = (bf16[512,512]{1,0:T(8,128)(2,1)S(1)}, bf16[512,512]{1,0:T(8,128)(2,1)S(1)}, u32[]{:S(2)}, u32[]{:S(2)}) collective-permute-start(bf16[512,512]{1,0:T(8,128)(2,1)S(1)} %bitcast.15), channel_id=1, source_target_pairs={{0,48},{16,0},{32,16},{48,32},{64,112},{80,64},{96,80},{112,96},{1... | collective-permute-start | bytes 1572872 | tf_op jit(solution)/shard_map/ppermute | solution.py:30
  53.9 3.4 %collective-permute-start.3 = (bf16[512,512]{1,0:T(8,128)(2,1)S(1)}, bf16[512,512]{1,0:T(8,128)(2,1)S(1)}, u32[]{:S(2)}, u32[]{:S(2)}) collective-permute-start(bf16[512,512]{1,0:T(8,128)(2,1)S(1)} %bitcast.16), channel_id=1, source_target_pairs={{0,16},{16,32},{32,48},{48,0},{64,80},{80,96},{96,112},{112,64},{1... | collective-permute-start | bytes 1572872 | tf_op jit(solution)/shard_map/ppermute | solution.py:30
  57.3 2.0 %collective-permute-start.1 = (bf16[256,512]{1,0:T(8,128)(2,1)S(1)}, bf16[256,512]{1,0:T(8,128)(2,1)S(1)}, u32[]{:S(2)}, u32[]{:S(2)}) collective-permute-start(bf16[256,512]{1,0:T(8,128)(2,1)S(1)} %bitcast.28), channel_id=1, source_target_pairs={{0,64},{16,80},{32,96},{48,112},{64,128},{80,144},{96,160},{112,17... | collective-permute-start | bytes 786440 | tf_op jit(solution)/shard_map/ppermute | solution.py:30
  59.3 4.5 %collective-permute-start.2 = (bf16[256,512]{1,0:T(8,128)(2,1)S(1)}, bf16[256,512]{1,0:T(8,128)(2,1)S(1)}, u32[]{:S(2)}, u32[]{:S(2)}) collective-permute-start(bf16[256,512]{1,0:T(8,128)(2,1)S(1)} %bitcast.27), channel_id=1, source_target_pairs={{0,448},{16,464},{32,480},{48,496},{64,0},{80,16},{96,32},{112,48}... | collective-permute-start | bytes 786440 | tf_op jit(solution)/shard_map/ppermute | solution.py:30
  64.4 2.5 %collective-permute-done.4.wr = bf16[512,512]{1,0:T(8,128)(2,1)S(1)} collective-permute-done((bf16[512,512]{1,0:T(8,128)(2,1)S(1)}, bf16[512,512]{1,0:T(8,128)(2,1)S(1)}, u32[]{:S(2)}, u32[]{:S(2)}) %collective-permute-start.4) | collective-permute-done | bytes 524320 | tf_op jit(solution)/shard_map/ppermute | solution.py:30
  66.9 2.0 %collective-permute-done.3.wl = bf16[512,512]{1,0:T(8,128)(2,1)S(1)} collective-permute-done((bf16[512,512]{1,0:T(8,128)(2,1)S(1)}, bf16[512,512]{1,0:T(8,128)(2,1)S(1)}, u32[]{:S(2)}, u32[]{:S(2)}) %collective-permute-start.3) | collective-permute-done | bytes 524320 | tf_op jit(solution)/shard_map/ppermute | solution.py:30
  71.1 1.9 %collective-permute-start.6 = (bf16[768,128]{1,0:T(8,128)(2,1)S(1)}, bf16[768,128]{1,0:T(8,128)(2,1)S(1)}, u32[]{:S(2)}, u32[]{:S(2)}) collective-permute-start(bf16[768,128]{1,0:T(8,128)(2,1)S(1)} %get-tuple-element.17), channel_id=1, source_target_pairs={{0,14},{1,15},{2,4},{3,5},{4,2},{5,3},{6,8},{7,9},{8,6},{9,7},{10,... | collective-permute-start | bytes 589832 | tf_op jit(solution)/shard_map/ppermute | solution.py:35
  73.0 3.3 %collective-permute-start.7 = (bf16[768,128]{1,0:T(8,128)(2,1)S(1)}, bf16[768,128]{1,0:T(8,128)(2,1)S(1)}, u32[]{:S(2)}, u32[]{:S(2)}) collective-permute-start(bf16[768,128]{1,0:T(8,128)(2,1)S(1)} %get-tuple-element.18), channel_id=1, source_target_pairs={{0,4},{1,5},{2,14},{3,15},{4,8},{5,9},{6,2},{7,3},{8,12},{9,13},{1... | collective-permute-start | bytes 589832 | tf_op jit(solution)/shard_map/ppermute | solution.py:35
  76.3 4.3 %collective-permute-start.5 = (bf16[768,128]{1,0:T(8,128)(2,1)S(1)}, bf16[768,128]{1,0:T(8,128)(2,1)S(1)}, u32[]{:S(2)}, u32[]{:S(2)}) collective-permute-start(bf16[768,128]{1,0:T(8,128)(2,1)S(1)} %get-tuple-element.16.refs_4_), channel_id=1, source_target_pairs={{0,2},{1,3},{2,0},{3,1},{4,6},{5,7},{6,4},{7,5},{8,10},{9,11},{10,... | collective-permute-start | bytes 589832 | tf_op jit(solution)/shard_map/ppermute | solution.py:35
  80.7 2.9 %collective-permute-start.8 = (bf16[768,128]{1,0:T(8,128)(2,1)S(1)}, bf16[768,128]{1,0:T(8,128)(2,1)S(1)}, u32[]{:S(2)}, u32[]{:S(2)}) collective-permute-start(bf16[768,128]{1,0:T(8,128)(2,1)S(1)} %get-tuple-element.19), channel_id=1, source_target_pairs={{0,10},{1,11},{2,8},{3,9},{4,14},{5,15},{6,12},{7,13},{8,2},{9,3},... | collective-permute-start | bytes 589832 | tf_op jit(solution)/shard_map/ppermute | solution.py:35
  83.7 3.4 %collective-permute-start.9 = (bf16[768,128]{1,0:T(8,128)(2,1)S(1)}, bf16[768,128]{1,0:T(8,128)(2,1)S(1)}, u32[]{:S(2)}, u32[]{:S(2)}) collective-permute-start(bf16[768,128]{1,0:T(8,128)(2,1)S(1)} %collective-permute-done.6.refs_6_), channel_id=1, source_target_pairs={{0,2},{1,3},{2,0},{3,1},{4,6},{5,7},{6,4},{7,5},{8,10},{9,11},{10,... | collective-permute-start | bytes 589832 | tf_op jit(solution)/shard_map/ppermute | solution.py:35
  87.0 1.9 %collective-permute-start.10 = (bf16[768,128]{1,0:T(8,128)(2,1)S(1)}, bf16[768,128]{1,0:T(8,128)(2,1)S(1)}, u32[]{:S(2)}, u32[]{:S(2)}) collective-permute-start(bf16[768,128]{1,0:T(8,128)(2,1)S(1)} %collective-permute-done.7.refs_7_), channel_id=1, source_target_pairs={{0,2},{1,3},{2,0},{3,1},{4,6},{5,7},{6,4},{7,5},{8,10},{9,11},{10,... | collective-permute-start | bytes 589832 | tf_op jit(solution)/shard_map/ppermute | solution.py:35
  89.1 6.7 %collective-permute-done.8.refs_8_ = bf16[768,128]{1,0:T(8,128)(2,1)S(1)} collective-permute-done((bf16[768,128]{1,0:T(8,128)(2,1)S(1)}, bf16[768,128]{1,0:T(8,128)(2,1)S(1)}, u32[]{:S(2)}, u32[]{:S(2)}) %collective-permute-start.8) | collective-permute-done | bytes 196640 | tf_op jit(solution)/shard_map/ppermute | solution.py:35
  95.9 3.0 %collective-permute-done.10.refs_10_ = bf16[768,128]{1,0:T(8,128)(2,1)S(1)} collective-permute-done((bf16[768,128]{1,0:T(8,128)(2,1)S(1)}, bf16[768,128]{1,0:T(8,128)(2,1)S(1)}, u32[]{:S(2)}, u32[]{:S(2)}) %collective-permute-start.10) | collective-permute-done | bytes 196640 | tf_op jit(solution)/shard_map/ppermute | solution.py:35
  98.9 4.5 %collective-permute-start.12 = (bf16[5376,128]{1,0:T(8,128)(2,1)S(1)}, bf16[5376,128]{1,0:T(8,128)(2,1)S(1)}, u32[]{:S(2)}, u32[]{:S(2)}) collective-permute-start(bf16[5376,128]{1,0:T(8,128)(2,1)S(1)} %constant_dynamic-update-slice_fusion), channel_id=1, source_target_pairs={{0,1},{1,0},{2,3},{3,2},{4,5},{5,4},{6,7},{7,6},{8,9},{9,8},{10,11... | collective-permute-start | bytes 4128776 | tf_op jit(solution)/shard_map/ppermute | solution.py:41
  103.4 2.4 %collective-permute-start.11 = (bf16[768,128]{1,0:T(8,128)(2,1)S(1)}, bf16[768,128]{1,0:T(8,128)(2,1)S(1)}, u32[]{:S(2)}, u32[]{:S(2)}) collective-permute-start(bf16[768,128]{1,0:T(8,128)(2,1)S(1)} %collective-permute-done.8.refs_8_), channel_id=1, source_target_pairs={{0,2},{1,3},{2,0},{3,1},{4,6},{5,7},{6,4},{7,5},{8,10},{9,11},{10,... | collective-permute-start | bytes 589832 | tf_op jit(solution)/shard_map/ppermute | solution.py:35
  105.8 5.9 %collective-permute-done.11.refs_11_ = bf16[768,128]{1,0:T(8,128)(2,1)S(1)} collective-permute-done((bf16[768,128]{1,0:T(8,128)(2,1)S(1)}, bf16[768,128]{1,0:T(8,128)(2,1)S(1)}, u32[]{:S(2)}, u32[]{:S(2)}) %collective-permute-start.11) | collective-permute-done | bytes 196640 | tf_op jit(solution)/shard_map/ppermute | solution.py:35
  111.8 2.8 %collective-permute-start.13 = (bf16[768,128]{1,0:T(8,128)(2,1)S(1)}, bf16[768,128]{1,0:T(8,128)(2,1)S(1)}, u32[]{:S(2)}, u32[]{:S(2)}) collective-permute-start(bf16[768,128]{1,0:T(8,128)(2,1)S(1)} %collective-permute-done.11.refs_11_), channel_id=1, source_target_pairs={{0,1},{1,0},{2,3},{3,2},{4,5},{5,4},{6,7},{7,6},{8,9},{9,8},{10,11... | collective-permute-start | bytes 589832 | tf_op jit(solution)/shard_map/ppermute | solution.py:41
  115.6 3.9 %read.1 = (bf16[6144,128]{1,0:T(8,128)(2,1)}, bf16[6144,128]{1,0:T(8,128)(2,1)}, bf16[1,128]{1,0:T(2,128)(2,1)}) custom-call(bf16[1,128]{1,0:T(2,128)(2,1)S(1)} %bitcast.23, f32[1,128]{1,0:T(1,128)S(1)} %bitcast.24, f32[1,128]{1,0:T(1,128)S(1)} %bitcast.25, f32[48,128]{1,0:T(8,128)S(1)} %get-tuple-element.14.refs_3_, ...), custom_call_target="tpu_custom_call" | custom-call | tf_op jit(solution)/shard_map/read/pallas_call | solution.py:356
  (40 shorter events, 9.7 us)
Async XLA Ops:
  0.6 0.7 copy-start.2
  1.3 0.7 copy-start.3
  2.0 0.7 copy-start.4
  3.4 19.3 %all-to-all-start = ((bf16[16,32,128]{2,1,0:T(8,128)(2,1)}), bf16[16,32,128]{2,1,0:T(8,128)(2,1)S(1)}, u32[]{:S(2)}, u32[]{:S(2)}) async-start(bf16[16,32,128]{2,1,0:T(8,128)(2,1)} %pack.1), calls=%async_computation | async-start | bytes 262144 | tf_op jit(solution)/shard_map/all_to_all | solution.py:270
  13.6 1.4 %copy-start = (bf16[1,384,2048]{2,1,0:T(8,128)(2,1)S(1)}, bf16[1,384,2048]{2,1,0:T(8,128)(2,1)}, u32[]{:S(2)}) copy-start(bf16[1,384,2048]{2,1,0:T(8,128)(2,1)} %param.9) | copy-start | bytes 4718596
  15.0 0.7 copy-start.1
  17.1 46.7 %collective-permute-start = (bf16[384,2048]{1,0:T(8,128)(2,1)S(1)}, bf16[384,2048]{1,0:T(8,128)(2,1)S(1)}, u32[]{:S(2)}, u32[]{:S(2)}) collective-permute-start(bf16[384,2048]{1,0:T(8,128)(2,1)S(1)} %norm.1.own), channel_id=1, source_target_pairs={{0,1},{1,0},{2,3},{3,2},{4,5},{5,4},{6,7},{7,6},{8,9},{9,8},{10,11... | collective-permute-start | bytes 4718600 | tf_op jit(solution)/shard_map/ppermute | solution.py:41
  52.0 14.9 %collective-permute-start.4 = (bf16[512,512]{1,0:T(8,128)(2,1)S(1)}, bf16[512,512]{1,0:T(8,128)(2,1)S(1)}, u32[]{:S(2)}, u32[]{:S(2)}) collective-permute-start(bf16[512,512]{1,0:T(8,128)(2,1)S(1)} %bitcast.15), channel_id=1, source_target_pairs={{0,48},{16,0},{32,16},{48,32},{64,112},{80,64},{96,80},{112,96},{1... | collective-permute-start | bytes 1572872 | tf_op jit(solution)/shard_map/ppermute | solution.py:30
  53.9 15.0 %collective-permute-start.3 = (bf16[512,512]{1,0:T(8,128)(2,1)S(1)}, bf16[512,512]{1,0:T(8,128)(2,1)S(1)}, u32[]{:S(2)}, u32[]{:S(2)}) collective-permute-start(bf16[512,512]{1,0:T(8,128)(2,1)S(1)} %bitcast.16), channel_id=1, source_target_pairs={{0,16},{16,32},{32,48},{48,0},{64,80},{80,96},{96,112},{112,64},{1... | collective-permute-start | bytes 1572872 | tf_op jit(solution)/shard_map/ppermute | solution.py:30
  57.3 12.6 %collective-permute-start.1 = (bf16[256,512]{1,0:T(8,128)(2,1)S(1)}, bf16[256,512]{1,0:T(8,128)(2,1)S(1)}, u32[]{:S(2)}, u32[]{:S(2)}) collective-permute-start(bf16[256,512]{1,0:T(8,128)(2,1)S(1)} %bitcast.28), channel_id=1, source_target_pairs={{0,64},{16,80},{32,96},{48,112},{64,128},{80,144},{96,160},{112,17... | collective-permute-start | bytes 786440 | tf_op jit(solution)/shard_map/ppermute | solution.py:30
  59.3 10.7 %collective-permute-start.2 = (bf16[256,512]{1,0:T(8,128)(2,1)S(1)}, bf16[256,512]{1,0:T(8,128)(2,1)S(1)}, u32[]{:S(2)}, u32[]{:S(2)}) collective-permute-start(bf16[256,512]{1,0:T(8,128)(2,1)S(1)} %bitcast.27), channel_id=1, source_target_pairs={{0,448},{16,464},{32,480},{48,496},{64,0},{80,16},{96,32},{112,48}... | collective-permute-start | bytes 786440 | tf_op jit(solution)/shard_map/ppermute | solution.py:30
  64.4 5.5 %copy-start.8 = (f32[128]{0:T(128)S(1)}, f32[128]{0:T(128)}, u32[]{:S(2)}) copy-start(f32[128]{0:T(128)} %param.13) | copy-start | bytes 1540
  71.1 12.6 %collective-permute-start.6 = (bf16[768,128]{1,0:T(8,128)(2,1)S(1)}, bf16[768,128]{1,0:T(8,128)(2,1)S(1)}, u32[]{:S(2)}, u32[]{:S(2)}) collective-permute-start(bf16[768,128]{1,0:T(8,128)(2,1)S(1)} %get-tuple-element.17), channel_id=1, source_target_pairs={{0,14},{1,15},{2,4},{3,5},{4,2},{5,3},{6,8},{7,9},{8,6},{9,7},{10,... | collective-permute-start | bytes 589832 | tf_op jit(solution)/shard_map/ppermute | solution.py:35
  73.0 14.0 %collective-permute-start.7 = (bf16[768,128]{1,0:T(8,128)(2,1)S(1)}, bf16[768,128]{1,0:T(8,128)(2,1)S(1)}, u32[]{:S(2)}, u32[]{:S(2)}) collective-permute-start(bf16[768,128]{1,0:T(8,128)(2,1)S(1)} %get-tuple-element.18), channel_id=1, source_target_pairs={{0,4},{1,5},{2,14},{3,15},{4,8},{5,9},{6,2},{7,3},{8,12},{9,13},{1... | collective-permute-start | bytes 589832 | tf_op jit(solution)/shard_map/ppermute | solution.py:35
  76.3 12.6 %collective-permute-start.5 = (bf16[768,128]{1,0:T(8,128)(2,1)S(1)}, bf16[768,128]{1,0:T(8,128)(2,1)S(1)}, u32[]{:S(2)}, u32[]{:S(2)}) collective-permute-start(bf16[768,128]{1,0:T(8,128)(2,1)S(1)} %get-tuple-element.16.refs_4_), channel_id=1, source_target_pairs={{0,2},{1,3},{2,0},{3,1},{4,6},{5,7},{6,4},{7,5},{8,10},{9,11},{10,... | collective-permute-start | bytes 589832 | tf_op jit(solution)/shard_map/ppermute | solution.py:35
  80.7 34.9 %copy-start.5 = (bf16[1,1,128]{2,1,0:T(2,128)(2,1)S(1)}, bf16[1,1,128]{2,1,0:T(2,128)(2,1)}, u32[]{:S(2)}) copy-start(bf16[1,1,128]{2,1,0:T(2,128)(2,1)} %param.15) | copy-start | bytes 772
  80.7 34.9 %copy-start.6 = (f32[128]{0:T(128)S(1)}, f32[128]{0:T(128)}, u32[]{:S(2)}) copy-start(f32[128]{0:T(128)} %param.16) | copy-start | bytes 1540
  80.7 34.9 %copy-start.7 = (f32[128]{0:T(128)S(1)}, f32[128]{0:T(128)}, u32[]{:S(2)}) copy-start(f32[128]{0:T(128)} %param.17) | copy-start | bytes 1540
  80.7 15.1 %collective-permute-start.8 = (bf16[768,128]{1,0:T(8,128)(2,1)S(1)}, bf16[768,128]{1,0:T(8,128)(2,1)S(1)}, u32[]{:S(2)}, u32[]{:S(2)}) collective-permute-start(bf16[768,128]{1,0:T(8,128)(2,1)S(1)} %get-tuple-element.19), channel_id=1, source_target_pairs={{0,10},{1,11},{2,8},{3,9},{4,14},{5,15},{6,12},{7,13},{8,2},{9,3},... | collective-permute-start | bytes 589832 | tf_op jit(solution)/shard_map/ppermute | solution.py:35
  83.7 12.2 %collective-permute-start.9 = (bf16[768,128]{1,0:T(8,128)(2,1)S(1)}, bf16[768,128]{1,0:T(8,128)(2,1)S(1)}, u32[]{:S(2)}, u32[]{:S(2)}) collective-permute-start(bf16[768,128]{1,0:T(8,128)(2,1)S(1)} %collective-permute-done.6.refs_6_), channel_id=1, source_target_pairs={{0,2},{1,3},{2,0},{3,1},{4,6},{5,7},{6,4},{7,5},{8,10},{9,11},{10,... | collective-permute-start | bytes 589832 | tf_op jit(solution)/shard_map/ppermute | solution.py:35
  87.0 11.8 %collective-permute-start.10 = (bf16[768,128]{1,0:T(8,128)(2,1)S(1)}, bf16[768,128]{1,0:T(8,128)(2,1)S(1)}, u32[]{:S(2)}, u32[]{:S(2)}) collective-permute-start(bf16[768,128]{1,0:T(8,128)(2,1)S(1)} %collective-permute-done.7.refs_7_), channel_id=1, source_target_pairs={{0,2},{1,3},{2,0},{3,1},{4,6},{5,7},{6,4},{7,5},{8,10},{9,11},{10,... | collective-permute-start | bytes 589832 | tf_op jit(solution)/shard_map/ppermute | solution.py:35
  98.9 16.7 %collective-permute-start.12 = (bf16[5376,128]{1,0:T(8,128)(2,1)S(1)}, bf16[5376,128]{1,0:T(8,128)(2,1)S(1)}, u32[]{:S(2)}, u32[]{:S(2)}) collective-permute-start(bf16[5376,128]{1,0:T(8,128)(2,1)S(1)} %constant_dynamic-update-slice_fusion), channel_id=1, source_target_pairs={{0,1},{1,0},{2,3},{3,2},{4,5},{5,4},{6,7},{7,6},{8,9},{9,8},{10,11... | collective-permute-start | bytes 4128776 | tf_op jit(solution)/shard_map/ppermute | solution.py:41
  103.4 8.3 %collective-permute-start.11 = (bf16[768,128]{1,0:T(8,128)(2,1)S(1)}, bf16[768,128]{1,0:T(8,128)(2,1)S(1)}, u32[]{:S(2)}, u32[]{:S(2)}) collective-permute-start(bf16[768,128]{1,0:T(8,128)(2,1)S(1)} %collective-permute-done.8.refs_8_), channel_id=1, source_target_pairs={{0,2},{1,3},{2,0},{3,1},{4,6},{5,7},{6,4},{7,5},{8,10},{9,11},{10,... | collective-permute-start | bytes 589832 | tf_op jit(solution)/shard_map/ppermute | solution.py:35
  111.8 3.8 %collective-permute-start.13 = (bf16[768,128]{1,0:T(8,128)(2,1)S(1)}, bf16[768,128]{1,0:T(8,128)(2,1)S(1)}, u32[]{:S(2)}, u32[]{:S(2)}) collective-permute-start(bf16[768,128]{1,0:T(8,128)(2,1)S(1)} %collective-permute-done.11.refs_11_), channel_id=1, source_target_pairs={{0,1},{1,0},{2,3},{3,2},{4,5},{5,4},{6,7},{7,6},{8,9},{9,8},{10,11... | collective-permute-start | bytes 589832 | tf_op jit(solution)/shard_map/ppermute | solution.py:41

commit v4 on v3

--- a/solution.py
+++ b/solution.py
@@ -56,8 +56,18 @@
     return lax.rem(lax.rem(at, NX) + 2 * lax.div(at, NX), CLASSES)
 
 
-def pack_body(key_t, value_t, shift, out):
+def pack_body(key_hbm, value_hbm, shift_hbm, out, key_t, value_t, shift, sems):
     groups = out.shape[0]
+    copies = [
+        pltpu.make_async_copy(src, dst, sems.at[i])
+        for i, (src, dst) in enumerate(
+            ((key_hbm, key_t), (value_hbm, value_t), (shift_hbm, shift))
+        )
+    ]
+    for c in copies:
+        c.start()
+    for c in copies:
+        c.wait()
     zeros = jnp.zeros((13, 128), jnp.float32)
     rows = []
     for ref in (key_t, value_t):
@@ -150,50 +160,49 @@
         outs[slot][...] = line[:, pl.ds(at, 128)]
 
 
-def read_body(query, query_gain, out_gain, shift, *rest, size, scale, chips):
-    mine, theirs = rest[:8], rest[8:10]
-    keys, values, first = rest[10:13]
-    score_ref, weight_ref, sems = rest[13:]
-    per = size // 128
-    blocks = chips * per
-    y, core = chip_and_core()
-    sign = 2 * lax.rem(y, 2) - 1
-    beside = y - sign
-    sources = [y, beside] + [y + sign * d for d in (1, 2, 3)] + [beside - sign * d for d in (1, 2, 3)]
-    sources = [lax.rem(s + chips, chips) for s in sources]
-
-    def their(j):
-        return theirs[0].at[pl.ds(j * size, size), :] if j < 7 else theirs[1]
-
+def read_pieces(pieces, query, query_gain, shift, lines, keys, values, sems, finish, scale):
+    size = pieces[0][1].shape[0]
+    per, n = size // 128, len(pieces)
+    score_ref, weight_ref = lines
     q = row_norm(query[...].astype(jnp.float32), query_gain[...]).astype(jnp.bfloat16)
     rows = lax.broadcasted_iota(jnp.int32, (128, 128), 0)
     lanes = lax.broadcasted_iota(jnp.int32, (128, 128), 1)
     on = rows == lanes
     q_all = jnp.broadcast_to(q, (128, 128))
     ones = jnp.ones((128, 128), jnp.bfloat16)
+    n_rows = n * per
+    at_row = lax.broadcasted_iota(jnp.int32, (n_rows, n_rows), 0)
+    at_col = lax.broadcasted_iota(jnp.int32, (n_rows, n_rows), 1)
+    up = ((at_col > at_row) & (at_col // per == at_row // per)).astype(jnp.float32)
 
     def run(key_of, value_of):
         copies = []
-        for j in range(8):
-            at = pl.multiple_of(sources[j] * size, 128)
+        for j, piece in enumerate(pieces):
+            to = pl.multiple_of(piece[0] * size, 128)
             copies.append(
-                pltpu.make_async_copy(key_of(j), keys.at[pl.ds(at, size), :], sems.at[j])
+                pltpu.make_async_copy(key_of(piece), keys.at[pl.ds(to, size), :], sems.at[j])
             )
             copies.append(
-                pltpu.make_async_copy(value_of(j), values.at[pl.ds(at, size), :], sems.at[8 + j])
+                pltpu.make_async_copy(
+                    value_of(piece), values.at[pl.ds(to, size), :], sems.at[n + j]
+                )
             )
         for c in copies:
             c.start()
-        for j in range(8):
+        for j, piece in enumerate(pieces):
             s = lax.dot_general(
-                key_of(j)[...], q_all, (((1,), (1,)), ((), ())), preferred_element_type=jnp.float32
+                key_of(piece)[...],
+                q_all,
+                (((1,), (1,)), ((), ())),
+                preferred_element_type=jnp.float32,
             )
             for i in range(per):
                 line = jnp.sum(
                     jnp.where(on, s[128 * i : 128 * i + 128], 0.0), axis=0, keepdims=True
                 )
-                score_ref[pl.ds(sources[j] * per + i, 1), :] = line
-        s = score_ref[...] * scale + shift[...]
+                at = piece[0] * per + i
+                score_ref[per * j + i : per * j + i + 1, :] = line * scale + shift[pl.ds(at, 1), :]
+        s = score_ref[...]
         keep = jax.nn.log_sigmoid(-s)
         inside = jnp.dot(
             keep,
@@ -201,33 +210,97 @@
             precision=lax.Precision.HIGHEST,
             preferred_element_type=jnp.float32,
         )
-        at_row = lax.broadcasted_iota(jnp.int32, (blocks, blocks), 0)
-        up = (lax.broadcasted_iota(jnp.int32, (blocks, blocks), 1) > at_row).astype(jnp.float32)
         later = jnp.dot(
             up, keep, precision=lax.Precision.HIGHEST, preferred_element_type=jnp.float32
         )
         inside = inside + jnp.sum(later, axis=1, keepdims=True)
         weight_ref[...] = jnp.exp(jax.nn.log_sigmoid(s) + inside)
-        total = jnp.zeros((128, 128), jnp.float32)
-        for j in range(8):
-            ref = value_of(j)
+        found = []
+        for j, piece in enumerate(pieces):
+            ref = value_of(piece)
+            total = jnp.zeros((128, 128), jnp.float32)
             for i in range(per):
-                w = weight_ref[pl.ds(sources[j] * per + i, 1), :]
+                w = weight_ref[per * j + i : per * j + i + 1, :]
                 spread = jnp.where(on, w, 0.0).astype(jnp.bfloat16)
                 spread = jnp.dot(spread, ones, preferred_element_type=jnp.float32)
                 total = total + spread * ref[128 * i : 128 * i + 128, :].astype(jnp.float32)
+            kept = jnp.sum(keep[per * j : per * j + per], axis=0, keepdims=True)
+            found.append((piece[0], jnp.sum(total, axis=0, keepdims=True), kept))
+        finish(found)
+        for c in copies:
+            c.wait()
+
+    _, core = chip_and_core()
+
+    @pl.when(core == 0)
+    def _():
+        run(lambda p: p[1], lambda p: p[2])
+
+    @pl.when(core == 1)
+    def _():
+        run(lambda p: p[2], lambda p: p[1])
+
+
+def positions(chips):
+    y, _ = chip_and_core()
+    sign = 2 * lax.rem(y, 2) - 1
+    near = [lax.rem(y + sign * d + chips, chips) for d in range(4)]
+    beside = y - sign
+    return near, [lax.rem(beside - sign * d + chips, chips) for d in range(4)]
+
+
+def early_body(query, query_gain, shift, own, f0, p3, p2, theirs, *rest, scale, chips):
+    keys, values, parts, kept, score_ref, weight_ref, sems = rest
+    near, far = positions(chips)
+    size = own.shape[0]
+    pieces = [
+        (at, ref, theirs.at[pl.ds(j * size, size), :])
+        for j, (at, ref) in enumerate(
+            ((near[0], own), (far[0], f0), (near[3], p3), (near[2], p2))
+        )
+    ]
+
+    def finish(found):
+        for at, total, keep in found:
+            parts[pl.ds(at, 1), :] = total
+            kept[pl.ds(at, 1), :] = keep
+
+    read_pieces(
+        pieces, query, query_gain, shift, (score_ref, weight_ref), keys, values, sems, finish, scale
+    )
+
+
+def late_body(
+    query, query_gain, out_gain, shift, p1, f3, f2, f1, theirs, last, parts, kept, *rest, scale, chips
+):
+    keys, values, first, part_ref, kept_ref, score_ref, weight_ref, sems = rest[2:]
+    near, far = positions(chips)
+    size = p1.shape[0]
+    pieces = [
+        (near[1], p1, theirs.at[pl.ds(0, size), :]),
+        (far[3], f3, theirs.at[pl.ds(size, size), :]),
+        (far[2], f2, theirs.at[pl.ds(2 * size, size), :]),
+        (far[1], f1, last),
+    ]
+    part_ref[...] = parts[...]
+    kept_ref[...] = kept[...]
+
+    def finish(found):
+        for at, total, keep in found:
+            part_ref[pl.ds(at, 1), :] = total
+            kept_ref[pl.ds(at, 1), :] = keep
+        row = lax.broadcasted_iota(jnp.int32, (chips, chips), 0)
+        up = (lax.broadcasted_iota(jnp.int32, (chips, chips), 1) > row).astype(jnp.float32)
+        later = jnp.dot(
+            up, kept_ref[...], precision=lax.Precision.HIGHEST, preferred_element_type=jnp.float32
+        )
+        total = jnp.exp(jnp.sum(later, axis=1, keepdims=True)) * part_ref[...]
         total = jnp.sum(total, axis=0, keepdims=True)
         first[...] = row_norm(total, out_gain[...]).astype(jnp.bfloat16)
-        for c in copies:
-            c.wait()
-
-    @pl.when(core == 0)
-    def _():
-        run(lambda j: mine[j], their)
-
-    @pl.when(core == 1)
-    def _():
-        run(their, lambda j: mine[j])
+
+    read_pieces(
+        pieces, query, query_gain, shift, (score_ref, weight_ref), keys, values, sems, finish, scale
+    )
 
 
 def in_vmem(n):
@@ -262,11 +335,22 @@
     sent = pl.pallas_call(
         pack_body,
         out_shape=shape(groups, 32, 128),
-        in_specs=in_vmem(3),
+        in_specs=[pl.BlockSpec(memory_space=pltpu.HBM)] * 3,
         out_specs=in_vmem(1)[0],
+        scratch_shapes=[
+            pltpu.VMEM(key_weight.shape[::-1], jnp.bfloat16),
+            pltpu.VMEM(key_weight.shape[::-1], jnp.bfloat16),
+            pltpu.VMEM(stop_shift.shape[1:], jnp.bfloat16),
+            pltpu.SemaphoreType.DMA((3,)),
+        ],
         compiler_params=pltpu.CompilerParams(vmem_limit_bytes=4 * MIB),
         name="pack",
-    )(key_weight.T, value_weight.T, stop_shift[0])
+    )(
+        *(
+            pltpu.with_memory_space_constraint(a, pltpu.HBM)
+            for a in (key_weight.T, value_weight.T, stop_shift[0])
+        )
+    )
     recv = lax.all_to_all(sent, "tp", split_axis=0, concat_axis=0, tiled=True)
     blocks, shift48, shift_line = pl.pallas_call(
         build_body,
@@ -296,7 +380,10 @@
         out_specs=pl.BlockSpec((rows // 4, width), lambda i: (i, 0)),
         compiler_params=pltpu.CompilerParams(vmem_limit_bytes=16 * MIB),
         name="norm",
-    )(layer_input[0], input_gain.reshape(1, width))
+    )(
+        pltpu.with_memory_space_constraint(layer_input[0], pltpu.HBM),
+        pltpu.with_memory_space_constraint(input_gain.reshape(1, width), pltpu.HBM),
+    )
     other = swapped(own)
 
     classes = [[z * NX + (c + 2 * z) % NX for z in range(nz)] for c in range(CLASSES)]
@@ -351,44 +438,44 @@
     f1 = moved_y(p1, across)
     f2 = moved_y(p2, across)
     f3 = moved_y(p3, across)
-    t1 = swapped(jnp.concatenate((mine, f0, p1, p2, p3, f1, f2), 0))
-    t2 = swapped(f3)
+    t1 = swapped(jnp.concatenate((mine, f0, p3, p2), 0))
+    t2 = swapped(jnp.concatenate((p1, f3, f2), 0))
+    t3 = swapped(f1)
+    in_hbm = pl.BlockSpec(memory_space=pltpu.HBM)
+    scale = 1.0 / head_size**0.5
+    half = length // 256
+    line_shape = shape(length, head_size)
+    part_shape = shape(ny, head_size, dtype=jnp.float32)
+    scratch = [
+        pltpu.VMEM((half, 128), jnp.float32),
+        pltpu.VMEM((half, 128), jnp.float32),
+        pltpu.SemaphoreType.DMA((8,)),
+    ]
+    query, gain_q, gain_o = new_query[0], query_gain.reshape(1, -1), out_gain.reshape(1, -1)
+    early = pl.pallas_call(
+        lambda *refs: early_body(*refs, scale=scale, chips=ny),
+        out_shape=(line_shape, line_shape, part_shape, part_shape),
+        in_specs=in_vmem(8),
+        out_specs=(in_hbm, in_hbm, *in_vmem(2)),
+        scratch_shapes=scratch,
+        compiler_params=pltpu.CompilerParams(vmem_limit_bytes=16 * MIB),
+        name="early",
+    )
+    key_line, value_line, parts, kept = early(query, gain_q, shift48, mine, f0, p3, p2, t1)
     key_line, value_line, first_out = pl.pallas_call(
-        lambda *refs: read_body(*refs, size=size, scale=1.0 / head_size**0.5, chips=ny),
-        out_shape=(
-            shape(length, head_size),
-            shape(length, head_size),
-            shape(1, head_size),
-        ),
-        in_specs=in_vmem(14),
-        out_specs=(
-            pl.BlockSpec(memory_space=pl.ANY),
-            pl.BlockSpec(memory_space=pl.ANY),
-            pl.BlockSpec(memory_space=pltpu.VMEM),
-        ),
+        lambda *refs: late_body(*refs, scale=scale, chips=ny),
+        out_shape=(line_shape, line_shape, shape(1, head_size)),
+        in_specs=in_vmem(12) + [in_hbm] * 2,
+        out_specs=(in_hbm, in_hbm, in_vmem(1)[0]),
         scratch_shapes=[
-            pltpu.VMEM((length // 128, 128), jnp.float32),
-            pltpu.VMEM((length // 128, 128), jnp.float32),
-            pltpu.SemaphoreType.DMA((16,)),
+            pltpu.VMEM((ny, head_size), jnp.float32),
+            pltpu.VMEM((ny, head_size), jnp.float32),
+            *scratch,
         ],
-        compiler_params=pltpu.CompilerParams(vmem_limit_bytes=24 * MIB),
-        name="read",
-    )(
-        new_query[0],
-        query_gain.reshape(1, head_size),
-        out_gain.reshape(1, head_size),
-        shift48,
-        mine,
-        f0,
-        p1,
-        p2,
-        p3,
-        f1,
-        f2,
-        f3,
-        t1,
-        t2,
-    )
+        input_output_aliases={12: 0, 13: 1},
+        compiler_params=pltpu.CompilerParams(vmem_limit_bytes=16 * MIB),
+        name="late",
+    )(query, gain_q, gain_o, shift48, p1, f3, f2, f1, t2, t3, parts, kept, key_line, value_line)
     return (
         key_line.reshape(1, 1, length, head_size),
         value_line.reshape(1, 1, length, head_size),

time: 120 us -> 121 us (level)
  starting transfers between devices: 51.5 us -> 57.6 us
  waiting for transfers between devices: 24.7 us -> 20.2 us
  local copies, waits for them, and re-layouts: 4.41 us -> 0.06 us
  Pallas kernels: 9.48 us -> 12.6 us
    ppermute x3 -> x4, starting transfers between devices: 9.42 us -> 14.8 us  [swapped(): lax.ppermute(x, 'tp', [(i, i ^ 1) for i in range(lax.axis_size('tp'))])]
    unnamed x24 -> x8, local copies, waits for them, and re-layouts: 4.35 us -> 0.03 us
    ppermute x7, waiting for transfers between devices: 15.7 us -> 11.7 us  [moved_y(): lax.ppermute(x, 'tp', [(i, target(i // 2) % (n // 2) * 2 + i % 2) for i i...]
    pallas_call x1, Pallas kernels: 1.39 us -> 3.08 us  [shards(): pl.pallas_call(norm_body, grid=(4,), out_shape=shape(rows, width), in_spe...]
    pallas_call x2 -> x3, Pallas kernels: 4.6 us -> 6.06 us  [the longest x1 2.62 us: shards(): pl.pallas_call(lambda *refs: late_body(*refs, scale=scale, chips=ny), out...]
  transfers between devices with their start and end apart: 15 -> 16, of which waited for: 7 -> 5; matrix products, arithmetic and copies ran while one was open for 0% -> 0% of each run, Pallas kernels for 3% -> 6%
where the time goes in v4:
time: 121 us; the launch traced here: 120 us
  starting transfers between devices  57.6 us (48%)
  blocking collectives  28.4 us (23%)
  waiting for transfers between devices  20.2 us (17%)
  Pallas kernels  12.6 us (10%)
    all_to_all x1, blocking collectives, shards(): lax.all_to_all(blocks, 'sp', split_axis=0, concat_axis=0, tiled=True, axi...  28.4 us
    ppermute x7, starting transfers between devices, moved_y(): lax.ppermute(x, 'tp', [(i, target(i // 2) % (n // 2) * 2 + i % 2) for i i...  20.9 us
    ppermute x4, starting transfers between devices, swapped(): lax.ppermute(x, 'tp', [(i, i ^ 1) for i in range(lax.axis_size('tp'))])  14.8 us
    ppermute x4, starting transfers between devices, moved_sp(): return lax.ppermute(x, 'sp', pairs)  11.8 us
    ppermute x7, waiting for transfers between devices, moved_y(): lax.ppermute(x, 'tp', [(i, target(i // 2) % (n // 2) * 2 + i % 2) for i i...  11.7 us
    all_to_all x1, starting transfers between devices, shards(): recv = lax.all_to_all(sent, 'tp', split_axis=0, concat_axis=0, tiled=True)  10.2 us
    ppermute x4, waiting for transfers between devices, moved_sp(): return lax.ppermute(x, 'sp', pairs)  4.48 us
    all_to_all x1, waiting for transfers between devices, shards(): recv = lax.all_to_all(sent, 'tp', split_axis=0, concat_axis=0, tiled=True)  3.95 us
  transfers between devices with their start and end apart: 16, of which 5 were waited for; matrix products, arithmetic and copies ran while one was open for 0% of the time, Pallas kernels for 6%

profile of v4, /device:TPU:1, one launch (start us, length us, event | category | flops | bytes accessed | tf_op | source)
XLA Modules:
  0.0 119.9 jit_solution(3776895825364748245)
XLA Ops:
  2.1 10.2 %all-to-all-start = ((bf16[16,32,128]{2,1,0:T(8,128)(2,1)}), bf16[16,32,128]{2,1,0:T(8,128)(2,1)S(1)}, u32[]{:S(2)}, u32[]{:S(2)}) async-start(bf16[16,32,128]{2,1,0:T(8,128)(2,1)} %pack.1), calls=%async_computation | async-start | bytes 262144 | tf_op jit(solution)/shard_map/all_to_all | solution.py:354
  12.3 3.1 %norm.1.own = bf16[384,2048]{1,0:T(8,128)(2,1)S(1)} custom-call(bf16[384,2048]{1,0:T(8,128)(2,1)} %bitcast.24, f32[1,2048]{1,0:T(1,128)} %bitcast.29), custom_call_target="tpu_custom_call" | custom-call | tf_op jit(solution)/shard_map/norm/pallas_call | solution.py:372
  15.4 2.1 %collective-permute-start = (bf16[384,2048]{1,0:T(8,128)(2,1)S(1)}, bf16[384,2048]{1,0:T(8,128)(2,1)S(1)}, u32[]{:S(2)}, u32[]{:S(2)}) collective-permute-start(bf16[384,2048]{1,0:T(8,128)(2,1)S(1)} %norm.1.own), channel_id=1, source_target_pairs={{0,1},{1,0},{2,3},{3,2},{4,5},{5,4},{6,7},{7,6},{8,9},{9,8},{10,11... | collective-permute-start | bytes 4718600 | tf_op jit(solution)/shard_map/ppermute | solution.py:41
  17.5 4.0 %all-to-all-done.recv = bf16[16,32,128]{2,1,0:T(8,128)(2,1)S(1)} async-done(((bf16[16,32,128]{2,1,0:T(8,128)(2,1)}), bf16[16,32,128]{2,1,0:T(8,128)(2,1)S(1)}, u32[]{:S(2)}, u32[]{:S(2)}) %all-to-all-start) | async-done | bytes 131104 | tf_op jit(solution)/shard_map/all_to_all | solution.py:354
  22.2 28.4 %all_to_all.10 = bf16[8,64,512]{2,1,0:T(8,128)(2,1)S(1)} all-to-all(bf16[8,64,512]{2,1,0:T(8,128)(2,1)S(1)} %get-tuple-element.19), channel_id=1, replica_groups={{0,96,128,224,256,352,384,480},{16,112,144,240,272,368,400,496},{32,64,..., dimensions={0} | all-to-all | bytes 1048576 | tf_op jit(solution)/shard_map/all_to_all | solution.py:390
  50.7 1.9 %collective-permute-start.4 = (bf16[512,512]{1,0:T(8,128)(2,1)S(1)}, bf16[512,512]{1,0:T(8,128)(2,1)S(1)}, u32[]{:S(2)}, u32[]{:S(2)}) collective-permute-start(bf16[512,512]{1,0:T(8,128)(2,1)S(1)} %bitcast.15), channel_id=1, source_target_pairs={{0,48},{16,0},{32,16},{48,32},{64,112},{80,64},{96,80},{112,96},{1... | collective-permute-start | bytes 1572872 | tf_op jit(solution)/shard_map/ppermute | solution.py:30
  52.6 3.4 %collective-permute-start.3 = (bf16[512,512]{1,0:T(8,128)(2,1)S(1)}, bf16[512,512]{1,0:T(8,128)(2,1)S(1)}, u32[]{:S(2)}, u32[]{:S(2)}) collective-permute-start(bf16[512,512]{1,0:T(8,128)(2,1)S(1)} %bitcast.16), channel_id=1, source_target_pairs={{0,16},{16,32},{32,48},{48,0},{64,80},{80,96},{96,112},{112,64},{1... | collective-permute-start | bytes 1572872 | tf_op jit(solution)/shard_map/ppermute | solution.py:30
  56.0 2.0 %collective-permute-start.1 = (bf16[256,512]{1,0:T(8,128)(2,1)S(1)}, bf16[256,512]{1,0:T(8,128)(2,1)S(1)}, u32[]{:S(2)}, u32[]{:S(2)}) collective-permute-start(bf16[256,512]{1,0:T(8,128)(2,1)S(1)} %bitcast.28), channel_id=1, source_target_pairs={{0,64},{16,80},{32,96},{48,112},{64,128},{80,144},{96,160},{112,17... | collective-permute-start | bytes 786440 | tf_op jit(solution)/shard_map/ppermute | solution.py:30
  58.0 4.5 %collective-permute-start.2 = (bf16[256,512]{1,0:T(8,128)(2,1)S(1)}, bf16[256,512]{1,0:T(8,128)(2,1)S(1)}, u32[]{:S(2)}, u32[]{:S(2)}) collective-permute-start(bf16[256,512]{1,0:T(8,128)(2,1)S(1)} %bitcast.27), channel_id=1, source_target_pairs={{0,448},{16,464},{32,480},{48,496},{64,0},{80,16},{96,32},{112,48}... | collective-permute-start | bytes 786440 | tf_op jit(solution)/shard_map/ppermute | solution.py:30
  63.1 2.5 %collective-permute-done.4.wr = bf16[512,512]{1,0:T(8,128)(2,1)S(1)} collective-permute-done((bf16[512,512]{1,0:T(8,128)(2,1)S(1)}, bf16[512,512]{1,0:T(8,128)(2,1)S(1)}, u32[]{:S(2)}, u32[]{:S(2)}) %collective-permute-start.4) | collective-permute-done | bytes 524320 | tf_op jit(solution)/shard_map/ppermute | solution.py:30
  65.6 2.0 %collective-permute-done.3.wl = bf16[512,512]{1,0:T(8,128)(2,1)S(1)} collective-permute-done((bf16[512,512]{1,0:T(8,128)(2,1)S(1)}, bf16[512,512]{1,0:T(8,128)(2,1)S(1)}, u32[]{:S(2)}, u32[]{:S(2)}) %collective-permute-start.3) | collective-permute-done | bytes 524320 | tf_op jit(solution)/shard_map/ppermute | solution.py:30
  69.8 1.9 %collective-permute-start.6 = (bf16[768,128]{1,0:T(8,128)(2,1)S(1)}, bf16[768,128]{1,0:T(8,128)(2,1)S(1)}, u32[]{:S(2)}, u32[]{:S(2)}) collective-permute-start(bf16[768,128]{1,0:T(8,128)(2,1)S(1)} %get-tuple-element.21), channel_id=1, source_target_pairs={{0,10},{1,11},{2,8},{3,9},{4,14},{5,15},{6,12},{7,13},{8,2},{9,3},... | collective-permute-start | bytes 589832 | tf_op jit(solution)/shard_map/ppermute | solution.py:35
  71.7 4.0 %collective-permute-start.8 = (bf16[768,128]{1,0:T(8,128)(2,1)S(1)}, bf16[768,128]{1,0:T(8,128)(2,1)S(1)}, u32[]{:S(2)}, u32[]{:S(2)}) collective-permute-start(bf16[768,128]{1,0:T(8,128)(2,1)S(1)} %get-tuple-element.22), channel_id=1, source_target_pairs={{0,4},{1,5},{2,14},{3,15},{4,8},{5,9},{6,2},{7,3},{8,12},{9,13},{1... | collective-permute-start | bytes 589832 | tf_op jit(solution)/shard_map/ppermute | solution.py:35
  75.7 3.8 %collective-permute-start.13 = (bf16[768,128]{1,0:T(8,128)(2,1)S(1)}, bf16[768,128]{1,0:T(8,128)(2,1)S(1)}, u32[]{:S(2)}, u32[]{:S(2)}) collective-permute-start(bf16[768,128]{1,0:T(8,128)(2,1)S(1)} %get-tuple-element.23.refs_3_), channel_id=1, source_target_pairs={{0,2},{1,3},{2,0},{3,1},{4,6},{5,7},{6,4},{7,5},{8,10},{9,11},{10,... | collective-permute-start | bytes 589832 | tf_op jit(solution)/shard_map/ppermute | solution.py:35
  79.5 2.7 %collective-permute-start.5 = (bf16[768,128]{1,0:T(8,128)(2,1)S(1)}, bf16[768,128]{1,0:T(8,128)(2,1)S(1)}, u32[]{:S(2)}, u32[]{:S(2)}) collective-permute-start(bf16[768,128]{1,0:T(8,128)(2,1)S(1)} %get-tuple-element.20), channel_id=1, source_target_pairs={{0,14},{1,15},{2,4},{3,5},{4,2},{5,3},{6,8},{7,9},{8,6},{9,7},{10,... | collective-permute-start | bytes 589832 | tf_op jit(solution)/shard_map/ppermute | solution.py:35
  82.2 6.6 %collective-permute-done.6.refs_5_ = bf16[768,128]{1,0:T(8,128)(2,1)S(1)} collective-permute-done((bf16[768,128]{1,0:T(8,128)(2,1)S(1)}, bf16[768,128]{1,0:T(8,128)(2,1)S(1)}, u32[]{:S(2)}, u32[]{:S(2)}) %collective-permute-start.6) | collective-permute-done | bytes 196640 | tf_op jit(solution)/shard_map/ppermute | solution.py:35
  90.7 3.4 %collective-permute-start.9 = (bf16[768,128]{1,0:T(8,128)(2,1)S(1)}, bf16[768,128]{1,0:T(8,128)(2,1)S(1)}, u32[]{:S(2)}, u32[]{:S(2)}) collective-permute-start(bf16[768,128]{1,0:T(8,128)(2,1)S(1)} %collective-permute-done.8.refs_6_), channel_id=1, source_target_pairs={{0,2},{1,3},{2,0},{3,1},{4,6},{5,7},{6,4},{7,5},{8,10},{9,11},{10,... | collective-permute-start | bytes 589832 | tf_op jit(solution)/shard_map/ppermute | solution.py:35
  94.2 5.3 %collective-permute-start.14 = (bf16[3072,128]{1,0:T(8,128)(2,1)S(1)}, bf16[3072,128]{1,0:T(8,128)(2,1)S(1)}, u32[]{:S(2)}, u32[]{:S(2)}) collective-permute-start(bf16[3072,128]{1,0:T(8,128)(2,1)S(1)} %pad_maximum_fusion), channel_id=1, source_target_pairs={{0,1},{1,0},{2,3},{3,2},{4,5},{5,4},{6,7},{7,6},{8,9},{9,8},{10,11... | collective-permute-start | bytes 2359304 | tf_op jit(solution)/shard_map/ppermute | solution.py:41
  99.6 4.6 %collective-permute-start.11 = (bf16[2304,128]{1,0:T(8,128)(2,1)S(1)}, bf16[2304,128]{1,0:T(8,128)(2,1)S(1)}, u32[]{:S(2)}, u32[]{:S(2)}) collective-permute-start(bf16[2304,128]{1,0:T(8,128)(2,1)S(1)} %pad_maximum_fusion.1), channel_id=1, source_target_pairs={{0,1},{1,0},{2,3},{3,2},{4,5},{5,4},{6,7},{7,6},{8,9},{9,8},{10,11... | collective-permute-start | bytes 1769480 | tf_op jit(solution)/shard_map/ppermute | solution.py:41
  104.2 3.2 %collective-permute-start.10 = (bf16[768,128]{1,0:T(8,128)(2,1)S(1)}, bf16[768,128]{1,0:T(8,128)(2,1)S(1)}, u32[]{:S(2)}, u32[]{:S(2)}) collective-permute-start(bf16[768,128]{1,0:T(8,128)(2,1)S(1)} %collective-permute-done.5.refs_4_), channel_id=1, source_target_pairs={{0,2},{1,3},{2,0},{3,1},{4,6},{5,7},{6,4},{7,5},{8,10},{9,11},{10,... | collective-permute-start | bytes 589832 | tf_op jit(solution)/shard_map/ppermute | solution.py:35
  107.4 5.1 %collective-permute-done.10.refs_7_ = bf16[768,128]{1,0:T(8,128)(2,1)S(1)} collective-permute-done((bf16[768,128]{1,0:T(8,128)(2,1)S(1)}, bf16[768,128]{1,0:T(8,128)(2,1)S(1)}, u32[]{:S(2)}, u32[]{:S(2)}) %collective-permute-start.10) | collective-permute-done | bytes 196640 | tf_op jit(solution)/shard_map/ppermute | solution.py:35
  112.5 2.8 %collective-permute-start.12 = (bf16[768,128]{1,0:T(8,128)(2,1)S(1)}, bf16[768,128]{1,0:T(8,128)(2,1)S(1)}, u32[]{:S(2)}, u32[]{:S(2)}) collective-permute-start(bf16[768,128]{1,0:T(8,128)(2,1)S(1)} %collective-permute-done.10.refs_7_), channel_id=1, source_target_pairs={{0,1},{1,0},{2,3},{3,2},{4,5},{5,4},{6,7},{7,6},{8,9},{9,8},{10,11... | collective-permute-start | bytes 589832 | tf_op jit(solution)/shard_map/ppermute | solution.py:41
  115.3 2.0 %early.1 = (bf16[6144,128]{1,0:T(8,128)(2,1)}, bf16[6144,128]{1,0:T(8,128)(2,1)}, f32[8,128]{1,0:T(8,128)S(1)}, f32[8,128]{1,0:T(8,128)S(1)}) custom-call(bf16[1,128]{1,0:T(2,128)(2,1)S(1)} %bitcast.18, f32[1,128]{1,0:T(1,128)S(1)} %bitcast.20, f32[48,128]{1,0:T(8,128)S(1)} %get-tuple-element.18.refs_2_.refs_3_, ...), custom_call_target="tpu_custom_call" | custom-call | tf_op jit(solution)/shard_map/early/pallas_call | solution.py:464
  117.3 2.6 %late.1 = (bf16[6144,128]{1,0:T(8,128)(2,1)}, bf16[6144,128]{1,0:T(8,128)(2,1)}, bf16[1,128]{1,0:T(2,128)(2,1)}) custom-call(bf16[1,128]{1,0:T(2,128)(2,1)S(1)} %bitcast.19, f32[1,128]{1,0:T(1,128)S(1)} %bitcast.21, f32[1,128]{1,0:T(1,128)S(1)} %bitcast.22, ...), custom_call_target="tpu_custom_call", output_to_operand_aliasing={{0}: (12, {}), {1}: (13, {})} | custom-call | tf_op jit(solution)/shard_map/late/pallas_call | solution.py:465
  (28 shorter events, 7.1 us)
Async XLA Ops:
  2.1 19.3 %all-to-all-start = ((bf16[16,32,128]{2,1,0:T(8,128)(2,1)}), bf16[16,32,128]{2,1,0:T(8,128)(2,1)S(1)}, u32[]{:S(2)}, u32[]{:S(2)}) async-start(bf16[16,32,128]{2,1,0:T(8,128)(2,1)} %pack.1), calls=%async_computation | async-start | bytes 262144 | tf_op jit(solution)/shard_map/all_to_all | solution.py:354
  15.4 47.1 %collective-permute-start = (bf16[384,2048]{1,0:T(8,128)(2,1)S(1)}, bf16[384,2048]{1,0:T(8,128)(2,1)S(1)}, u32[]{:S(2)}, u32[]{:S(2)}) collective-permute-start(bf16[384,2048]{1,0:T(8,128)(2,1)S(1)} %norm.1.own), channel_id=1, source_target_pairs={{0,1},{1,0},{2,3},{3,2},{4,5},{5,4},{6,7},{7,6},{8,9},{9,8},{10,11... | collective-permute-start | bytes 4718600 | tf_op jit(solution)/shard_map/ppermute | solution.py:41
  50.7 14.9 %collective-permute-start.4 = (bf16[512,512]{1,0:T(8,128)(2,1)S(1)}, bf16[512,512]{1,0:T(8,128)(2,1)S(1)}, u32[]{:S(2)}, u32[]{:S(2)}) collective-permute-start(bf16[512,512]{1,0:T(8,128)(2,1)S(1)} %bitcast.15), channel_id=1, source_target_pairs={{0,48},{16,0},{32,16},{48,32},{64,112},{80,64},{96,80},{112,96},{1... | collective-permute-start | bytes 1572872 | tf_op jit(solution)/shard_map/ppermute | solution.py:30
  52.6 15.0 %collective-permute-start.3 = (bf16[512,512]{1,0:T(8,128)(2,1)S(1)}, bf16[512,512]{1,0:T(8,128)(2,1)S(1)}, u32[]{:S(2)}, u32[]{:S(2)}) collective-permute-start(bf16[512,512]{1,0:T(8,128)(2,1)S(1)} %bitcast.16), channel_id=1, source_target_pairs={{0,16},{16,32},{32,48},{48,0},{64,80},{80,96},{96,112},{112,64},{1... | collective-permute-start | bytes 1572872 | tf_op jit(solution)/shard_map/ppermute | solution.py:30
  56.0 12.6 %collective-permute-start.1 = (bf16[256,512]{1,0:T(8,128)(2,1)S(1)}, bf16[256,512]{1,0:T(8,128)(2,1)S(1)}, u32[]{:S(2)}, u32[]{:S(2)}) collective-permute-start(bf16[256,512]{1,0:T(8,128)(2,1)S(1)} %bitcast.28), channel_id=1, source_target_pairs={{0,64},{16,80},{32,96},{48,112},{64,128},{80,144},{96,160},{112,17... | collective-permute-start | bytes 786440 | tf_op jit(solution)/shard_map/ppermute | solution.py:30
  58.0 10.7 %collective-permute-start.2 = (bf16[256,512]{1,0:T(8,128)(2,1)S(1)}, bf16[256,512]{1,0:T(8,128)(2,1)S(1)}, u32[]{:S(2)}, u32[]{:S(2)}) collective-permute-start(bf16[256,512]{1,0:T(8,128)(2,1)S(1)} %bitcast.27), channel_id=1, source_target_pairs={{0,448},{16,464},{32,480},{48,496},{64,0},{80,16},{96,32},{112,48}... | collective-permute-start | bytes 786440 | tf_op jit(solution)/shard_map/ppermute | solution.py:30
  63.1 5.5 %copy-start.3 = (f32[128]{0:T(128)S(1)}, f32[128]{0:T(128)}, u32[]{:S(2)}) copy-start(f32[128]{0:T(128)} %param.13) | copy-start | bytes 1540
  69.8 45.5 %copy-start = (bf16[1,1,128]{2,1,0:T(2,128)(2,1)S(1)}, bf16[1,1,128]{2,1,0:T(2,128)(2,1)}, u32[]{:S(2)}) copy-start(bf16[1,1,128]{2,1,0:T(2,128)(2,1)} %param.15) | copy-start | bytes 772
  69.8 45.5 %copy-start.1 = (f32[128]{0:T(128)S(1)}, f32[128]{0:T(128)}, u32[]{:S(2)}) copy-start(f32[128]{0:T(128)} %param.16) | copy-start | bytes 1540
  69.8 19.0 %collective-permute-start.6 = (bf16[768,128]{1,0:T(8,128)(2,1)S(1)}, bf16[768,128]{1,0:T(8,128)(2,1)S(1)}, u32[]{:S(2)}, u32[]{:S(2)}) collective-permute-start(bf16[768,128]{1,0:T(8,128)(2,1)S(1)} %get-tuple-element.21), channel_id=1, source_target_pairs={{0,10},{1,11},{2,8},{3,9},{4,14},{5,15},{6,12},{7,13},{8,2},{9,3},... | collective-permute-start | bytes 589832 | tf_op jit(solution)/shard_map/ppermute | solution.py:35
  71.7 19.0 %collective-permute-start.8 = (bf16[768,128]{1,0:T(8,128)(2,1)S(1)}, bf16[768,128]{1,0:T(8,128)(2,1)S(1)}, u32[]{:S(2)}, u32[]{:S(2)}) collective-permute-start(bf16[768,128]{1,0:T(8,128)(2,1)S(1)} %get-tuple-element.22), channel_id=1, source_target_pairs={{0,4},{1,5},{2,14},{3,15},{4,8},{5,9},{6,2},{7,3},{8,12},{9,13},{1... | collective-permute-start | bytes 589832 | tf_op jit(solution)/shard_map/ppermute | solution.py:35
  75.7 18.4 %collective-permute-start.13 = (bf16[768,128]{1,0:T(8,128)(2,1)S(1)}, bf16[768,128]{1,0:T(8,128)(2,1)S(1)}, u32[]{:S(2)}, u32[]{:S(2)}) collective-permute-start(bf16[768,128]{1,0:T(8,128)(2,1)S(1)} %get-tuple-element.23.refs_3_), channel_id=1, source_target_pairs={{0,2},{1,3},{2,0},{3,1},{4,6},{5,7},{6,4},{7,5},{8,10},{9,11},{10,... | collective-permute-start | bytes 589832 | tf_op jit(solution)/shard_map/ppermute | solution.py:35
  79.5 20.0 %collective-permute-start.5 = (bf16[768,128]{1,0:T(8,128)(2,1)S(1)}, bf16[768,128]{1,0:T(8,128)(2,1)S(1)}, u32[]{:S(2)}, u32[]{:S(2)}) collective-permute-start(bf16[768,128]{1,0:T(8,128)(2,1)S(1)} %get-tuple-element.20), channel_id=1, source_target_pairs={{0,14},{1,15},{2,4},{3,5},{4,2},{5,3},{6,8},{7,9},{8,6},{9,7},{10,... | collective-permute-start | bytes 589832 | tf_op jit(solution)/shard_map/ppermute | solution.py:35
  88.8 10.7 %collective-permute-start.7 = (bf16[768,128]{1,0:T(8,128)(2,1)S(1)}, bf16[768,128]{1,0:T(8,128)(2,1)S(1)}, u32[]{:S(2)}, u32[]{:S(2)}) collective-permute-start(bf16[768,128]{1,0:T(8,128)(2,1)S(1)} %collective-permute-done.6.refs_5_), channel_id=1, source_target_pairs={{0,2},{1,3},{2,0},{3,1},{4,6},{5,7},{6,4},{7,5},{8,10},{9,11},{10,... | collective-permute-start | bytes 589832 | tf_op jit(solution)/shard_map/ppermute | solution.py:35
  90.7 8.8 %collective-permute-start.9 = (bf16[768,128]{1,0:T(8,128)(2,1)S(1)}, bf16[768,128]{1,0:T(8,128)(2,1)S(1)}, u32[]{:S(2)}, u32[]{:S(2)}) collective-permute-start(bf16[768,128]{1,0:T(8,128)(2,1)S(1)} %collective-permute-done.8.refs_6_), channel_id=1, source_target_pairs={{0,2},{1,3},{2,0},{3,1},{4,6},{5,7},{6,4},{7,5},{8,10},{9,11},{10,... | collective-permute-start | bytes 589832 | tf_op jit(solution)/shard_map/ppermute | solution.py:35
  94.2 23.1 %copy-start.2 = (f32[128]{0:T(128)S(1)}, f32[128]{0:T(128)}, u32[]{:S(2)}) copy-start(f32[128]{0:T(128)} %param.17) | copy-start | bytes 1540
  94.2 21.1 %collective-permute-start.14 = (bf16[3072,128]{1,0:T(8,128)(2,1)S(1)}, bf16[3072,128]{1,0:T(8,128)(2,1)S(1)}, u32[]{:S(2)}, u32[]{:S(2)}) collective-permute-start(bf16[3072,128]{1,0:T(8,128)(2,1)S(1)} %pad_maximum_fusion), channel_id=1, source_target_pairs={{0,1},{1,0},{2,3},{3,2},{4,5},{5,4},{6,7},{7,6},{8,9},{9,8},{10,11... | collective-permute-start | bytes 2359304 | tf_op jit(solution)/shard_map/ppermute | solution.py:41
  99.6 17.7 %collective-permute-start.11 = (bf16[2304,128]{1,0:T(8,128)(2,1)S(1)}, bf16[2304,128]{1,0:T(8,128)(2,1)S(1)}, u32[]{:S(2)}, u32[]{:S(2)}) collective-permute-start(bf16[2304,128]{1,0:T(8,128)(2,1)S(1)} %pad_maximum_fusion.1), channel_id=1, source_target_pairs={{0,1},{1,0},{2,3},{3,2},{4,5},{5,4},{6,7},{7,6},{8,9},{9,8},{10,11... | collective-permute-start | bytes 1769480 | tf_op jit(solution)/shard_map/ppermute | solution.py:41
  104.2 8.3 %collective-permute-start.10 = (bf16[768,128]{1,0:T(8,128)(2,1)S(1)}, bf16[768,128]{1,0:T(8,128)(2,1)S(1)}, u32[]{:S(2)}, u32[]{:S(2)}) collective-permute-start(bf16[768,128]{1,0:T(8,128)(2,1)S(1)} %collective-permute-done.5.refs_4_), channel_id=1, source_target_pairs={{0,2},{1,3},{2,0},{3,1},{4,6},{5,7},{6,4},{7,5},{8,10},{9,11},{10,... | collective-permute-start | bytes 589832 | tf_op jit(solution)/shard_map/ppermute | solution.py:35
  112.5 4.8 %collective-permute-start.12 = (bf16[768,128]{1,0:T(8,128)(2,1)S(1)}, bf16[768,128]{1,0:T(8,128)(2,1)S(1)}, u32[]{:S(2)}, u32[]{:S(2)}) collective-permute-start(bf16[768,128]{1,0:T(8,128)(2,1)S(1)} %collective-permute-done.10.refs_7_), channel_id=1, source_target_pairs={{0,1},{1,0},{2,3},{3,2},{4,5},{5,4},{6,7},{7,6},{8,9},{9,8},{10,11... | collective-permute-start | bytes 589832 | tf_op jit(solution)/shard_map/ppermute | solution.py:41

commit v5 on v3

--- a/solution.py
+++ b/solution.py
@@ -56,8 +56,18 @@
     return lax.rem(lax.rem(at, NX) + 2 * lax.div(at, NX), CLASSES)
 
 
-def pack_body(key_t, value_t, shift, out):
+def pack_body(key_hbm, value_hbm, shift_hbm, out, key_t, value_t, shift, sems):
     groups = out.shape[0]
+    copies = [
+        pltpu.make_async_copy(src, dst, sems.at[i])
+        for i, (src, dst) in enumerate(
+            ((key_hbm, key_t), (value_hbm, value_t), (shift_hbm, shift))
+        )
+    ]
+    for c in copies:
+        c.start()
+    for c in copies:
+        c.wait()
     zeros = jnp.zeros((13, 128), jnp.float32)
     rows = []
     for ref in (key_t, value_t):
@@ -151,9 +161,10 @@
 
 
 def read_body(query, query_gain, out_gain, shift, *rest, size, scale, chips):
-    mine, theirs = rest[:8], rest[8:10]
-    keys, values, first = rest[10:13]
-    score_ref, weight_ref, sems = rest[13:]
+    both, theirs = rest[5], rest[7:9]
+    mine = [*rest[:5], both.at[pl.ds(0, size), :], both.at[pl.ds(size, size), :], rest[6]]
+    keys, values, first = rest[9:12]
+    score_ref, weight_ref, sems = rest[12:]
     per = size // 128
     blocks = chips * per
     y, core = chip_and_core()
@@ -168,9 +179,7 @@
     q = row_norm(query[...].astype(jnp.float32), query_gain[...]).astype(jnp.bfloat16)
     rows = lax.broadcasted_iota(jnp.int32, (128, 128), 0)
     lanes = lax.broadcasted_iota(jnp.int32, (128, 128), 1)
-    on = rows == lanes
-    q_all = jnp.broadcast_to(q, (128, 128))
-    ones = jnp.ones((128, 128), jnp.bfloat16)
+    q_all = jnp.broadcast_to(q, (16, 128))
 
     def run(key_of, value_of):
         copies = []
@@ -186,13 +195,10 @@
             c.start()
         for j in range(8):
             s = lax.dot_general(
-                key_of(j)[...], q_all, (((1,), (1,)), ((), ())), preferred_element_type=jnp.float32
+                q_all, key_of(j)[...], (((1,), (1,)), ((), ())), preferred_element_type=jnp.float32
             )
             for i in range(per):
-                line = jnp.sum(
-                    jnp.where(on, s[128 * i : 128 * i + 128], 0.0), axis=0, keepdims=True
-                )
-                score_ref[pl.ds(sources[j] * per + i, 1), :] = line
+                score_ref[pl.ds(sources[j] * per + i, 1), :] = s[0:1, 128 * i : 128 * i + 128]
         s = score_ref[...] * scale + shift[...]
         keep = jax.nn.log_sigmoid(-s)
         inside = jnp.dot(
@@ -208,15 +214,17 @@
         )
         inside = inside + jnp.sum(later, axis=1, keepdims=True)
         weight_ref[...] = jnp.exp(jax.nn.log_sigmoid(s) + inside)
-        total = jnp.zeros((128, 128), jnp.float32)
+        total = jnp.zeros((16, 128), jnp.float32)
         for j in range(8):
-            ref = value_of(j)
-            for i in range(per):
-                w = weight_ref[pl.ds(sources[j] * per + i, 1), :]
-                spread = jnp.where(on, w, 0.0).astype(jnp.bfloat16)
-                spread = jnp.dot(spread, ones, preferred_element_type=jnp.float32)
-                total = total + spread * ref[128 * i : 128 * i + 128, :].astype(jnp.float32)
-        total = jnp.sum(total, axis=0, keepdims=True)
+            w = jnp.concatenate(
+                [weight_ref[pl.ds(sources[j] * per + i, 1), :] for i in range(per)], axis=1
+            )
+            total = total + jnp.dot(
+                jnp.broadcast_to(w, (16, size)).astype(jnp.bfloat16),
+                value_of(j)[...],
+                preferred_element_type=jnp.float32,
+            )
+        total = total[0:1]
         first[...] = row_norm(total, out_gain[...]).astype(jnp.bfloat16)
         for c in copies:
             c.wait()
@@ -262,11 +270,22 @@
     sent = pl.pallas_call(
         pack_body,
         out_shape=shape(groups, 32, 128),
-        in_specs=in_vmem(3),
+        in_specs=[pl.BlockSpec(memory_space=pltpu.HBM)] * 3,
         out_specs=in_vmem(1)[0],
+        scratch_shapes=[
+            pltpu.VMEM(key_weight.shape[::-1], jnp.bfloat16),
+            pltpu.VMEM(key_weight.shape[::-1], jnp.bfloat16),
+            pltpu.VMEM(stop_shift.shape[1:], jnp.bfloat16),
+            pltpu.SemaphoreType.DMA((3,)),
+        ],
         compiler_params=pltpu.CompilerParams(vmem_limit_bytes=4 * MIB),
         name="pack",
-    )(key_weight.T, value_weight.T, stop_shift[0])
+    )(
+        *(
+            pltpu.with_memory_space_constraint(a, pltpu.HBM)
+            for a in (key_weight.T, value_weight.T, stop_shift[0])
+        )
+    )
     recv = lax.all_to_all(sent, "tp", split_axis=0, concat_axis=0, tiled=True)
     blocks, shift48, shift_line = pl.pallas_call(
         build_body,
@@ -296,7 +315,10 @@
         out_specs=pl.BlockSpec((rows // 4, width), lambda i: (i, 0)),
         compiler_params=pltpu.CompilerParams(vmem_limit_bytes=16 * MIB),
         name="norm",
-    )(layer_input[0], input_gain.reshape(1, width))
+    )(
+        pltpu.with_memory_space_constraint(layer_input[0], pltpu.HBM),
+        pltpu.with_memory_space_constraint(input_gain.reshape(1, width), pltpu.HBM),
+    )
     other = swapped(own)
 
     classes = [[z * NX + (c + 2 * z) % NX for z in range(nz)] for c in range(CLASSES)]
@@ -348,10 +370,9 @@
     p2 = moved_y(slots[2], step_to(2))
     p3 = moved_y(slots[3], step_to(3))
     f0 = moved_y(mine, across)
-    f1 = moved_y(p1, across)
-    f2 = moved_y(p2, across)
+    f12 = moved_y(jnp.concatenate((p1, p2), 0), across)
     f3 = moved_y(p3, across)
-    t1 = swapped(jnp.concatenate((mine, f0, p1, p2, p3, f1, f2), 0))
+    t1 = swapped(jnp.concatenate((mine, f0, p1, p2, p3, f12), 0))
     t2 = swapped(f3)
     key_line, value_line, first_out = pl.pallas_call(
         lambda *refs: read_body(*refs, size=size, scale=1.0 / head_size**0.5, chips=ny),
@@ -360,7 +381,7 @@
             shape(length, head_size),
             shape(1, head_size),
         ),
-        in_specs=in_vmem(14),
+        in_specs=in_vmem(13),
         out_specs=(
             pl.BlockSpec(memory_space=pl.ANY),
             pl.BlockSpec(memory_space=pl.ANY),
@@ -383,8 +404,7 @@
         p1,
         p2,
         p3,
-        f1,
-        f2,
+        f12,
         f3,
         t1,
         t2,

time: 120 us -> 120 us (level)
  local copies, waits for them, and re-layouts: 4.41 us -> 0.24 us
  waiting for transfers between devices: 24.7 us -> 27.1 us
  Pallas kernels: 9.48 us -> 11.5 us
    unnamed x24 -> x13, local copies, waits for them, and re-layouts: 4.35 us -> 0.15 us
    ppermute x7 -> x6, waiting for transfers between devices: 15.7 us -> 17.7 us  [moved_y(): lax.ppermute(x, 'tp', [(i, target(i // 2) % (n // 2) * 2 + i % 2) for i i...]
    pallas_call x1, Pallas kernels: 1.39 us -> 3.08 us  [shards(): pl.pallas_call(norm_body, grid=(4,), out_shape=shape(rows, width), in_spe...]
    ppermute x7 -> x6, starting transfers between devices: 20.2 us -> 18.9 us  [moved_y(): lax.ppermute(x, 'tp', [(i, target(i // 2) % (n // 2) * 2 + i % 2) for i i...]
  transfers between devices with their start and end apart: 15 -> 14, of which waited for: 7 -> 7; matrix products, arithmetic and copies ran while one was open for 0% -> 0% of each run, Pallas kernels for 3% -> 5%
where the time goes in v5:
time: 120 us; the launch traced here: 119 us
  starting transfers between devices  50.7 us (42%)
  blocking collectives  28.4 us (24%)
  waiting for transfers between devices  27.1 us (23%)
  Pallas kernels  11.5 us (10%)
    all_to_all x1, blocking collectives, shards(): lax.all_to_all(blocks, 'sp', split_axis=0, concat_axis=0, tiled=True, axi...  28.4 us
    ppermute x6, starting transfers between devices, moved_y(): lax.ppermute(x, 'tp', [(i, target(i // 2) % (n // 2) * 2 + i % 2) for i i...  18.9 us
    ppermute x6, waiting for transfers between devices, moved_y(): lax.ppermute(x, 'tp', [(i, target(i // 2) % (n // 2) * 2 + i % 2) for i i...  17.7 us
    ppermute x4, starting transfers between devices, moved_sp(): return lax.ppermute(x, 'sp', pairs)  11.8 us
    all_to_all x1, starting transfers between devices, shards(): recv = lax.all_to_all(sent, 'tp', split_axis=0, concat_axis=0, tiled=True)  10.2 us
    ppermute x3, starting transfers between devices, swapped(): lax.ppermute(x, 'tp', [(i, i ^ 1) for i in range(lax.axis_size('tp'))])  9.87 us
    ppermute x4, waiting for transfers between devices, moved_sp(): return lax.ppermute(x, 'sp', pairs)  4.48 us
    all_to_all x1, waiting for transfers between devices, shards(): recv = lax.all_to_all(sent, 'tp', split_axis=0, concat_axis=0, tiled=True)  3.95 us
  transfers between devices with their start and end apart: 14, of which 7 were waited for; matrix products, arithmetic and copies ran while one was open for 0% of the time, Pallas kernels for 5%

profile of v5, /device:TPU:1, one launch (start us, length us, event | category | flops | bytes accessed | tf_op | source)
XLA Modules:
  0.0 118.9 jit_solution(15827737799377217116)
XLA Ops:
  0.6 1.5 %pack.1 = bf16[16,32,128]{2,1,0:T(8,128)(2,1)} custom-call(bf16[32,64]{1,0:T(8,128)(2,1)} %bitcast.26, bf16[32,64]{1,0:T(8,128)(2,1)} %bitcast.27, bf16[4,384]{1,0:T(4,128)(2,1)} %bitcast.28), custom_call_target="tpu_custom_call" | custom-call | tf_op jit(solution)/shard_map/pack/pallas_call | solution.py:270
  2.1 10.2 %all-to-all-start = ((bf16[16,32,128]{2,1,0:T(8,128)(2,1)}), bf16[16,32,128]{2,1,0:T(8,128)(2,1)S(1)}, u32[]{:S(2)}, u32[]{:S(2)}) async-start(bf16[16,32,128]{2,1,0:T(8,128)(2,1)} %pack.1), calls=%async_computation | async-start | bytes 262144 | tf_op jit(solution)/shard_map/all_to_all | solution.py:289
  12.3 3.1 %norm.1.own = bf16[384,2048]{1,0:T(8,128)(2,1)S(1)} custom-call(bf16[384,2048]{1,0:T(8,128)(2,1)} %bitcast.22, f32[1,2048]{1,0:T(1,128)} %bitcast.25), custom_call_target="tpu_custom_call" | custom-call | tf_op jit(solution)/shard_map/norm/pallas_call | solution.py:307
  15.4 2.1 %collective-permute-start = (bf16[384,2048]{1,0:T(8,128)(2,1)S(1)}, bf16[384,2048]{1,0:T(8,128)(2,1)S(1)}, u32[]{:S(2)}, u32[]{:S(2)}) collective-permute-start(bf16[384,2048]{1,0:T(8,128)(2,1)S(1)} %norm.1.own), channel_id=1, source_target_pairs={{0,1},{1,0},{2,3},{3,2},{4,5},{5,4},{6,7},{7,6},{8,9},{9,8},{10,11... | collective-permute-start | bytes 4718600 | tf_op jit(solution)/shard_map/ppermute | solution.py:41
  17.5 4.0 %all-to-all-done.recv = bf16[16,32,128]{2,1,0:T(8,128)(2,1)S(1)} async-done(((bf16[16,32,128]{2,1,0:T(8,128)(2,1)}), bf16[16,32,128]{2,1,0:T(8,128)(2,1)S(1)}, u32[]{:S(2)}, u32[]{:S(2)}) %all-to-all-start) | async-done | bytes 131104 | tf_op jit(solution)/shard_map/all_to_all | solution.py:289
  22.2 28.4 %all_to_all.10 = bf16[8,64,512]{2,1,0:T(8,128)(2,1)S(1)} all-to-all(bf16[8,64,512]{2,1,0:T(8,128)(2,1)S(1)} %get-tuple-element.15), channel_id=1, replica_groups={{0,96,128,224,256,352,384,480},{16,112,144,240,272,368,400,496},{32,64,..., dimensions={0} | all-to-all | bytes 1048576 | tf_op jit(solution)/shard_map/all_to_all | solution.py:325
  50.7 1.9 %collective-permute-start.4 = (bf16[512,512]{1,0:T(8,128)(2,1)S(1)}, bf16[512,512]{1,0:T(8,128)(2,1)S(1)}, u32[]{:S(2)}, u32[]{:S(2)}) collective-permute-start(bf16[512,512]{1,0:T(8,128)(2,1)S(1)} %bitcast.15), channel_id=1, source_target_pairs={{0,48},{16,0},{32,16},{48,32},{64,112},{80,64},{96,80},{112,96},{1... | collective-permute-start | bytes 1572872 | tf_op jit(solution)/shard_map/ppermute | solution.py:30
  52.6 3.4 %collective-permute-start.3 = (bf16[512,512]{1,0:T(8,128)(2,1)S(1)}, bf16[512,512]{1,0:T(8,128)(2,1)S(1)}, u32[]{:S(2)}, u32[]{:S(2)}) collective-permute-start(bf16[512,512]{1,0:T(8,128)(2,1)S(1)} %bitcast.16), channel_id=1, source_target_pairs={{0,16},{16,32},{32,48},{48,0},{64,80},{80,96},{96,112},{112,64},{1... | collective-permute-start | bytes 1572872 | tf_op jit(solution)/shard_map/ppermute | solution.py:30
  56.0 2.0 %collective-permute-start.1 = (bf16[256,512]{1,0:T(8,128)(2,1)S(1)}, bf16[256,512]{1,0:T(8,128)(2,1)S(1)}, u32[]{:S(2)}, u32[]{:S(2)}) collective-permute-start(bf16[256,512]{1,0:T(8,128)(2,1)S(1)} %bitcast.24), channel_id=1, source_target_pairs={{0,64},{16,80},{32,96},{48,112},{64,128},{80,144},{96,160},{112,17... | collective-permute-start | bytes 786440 | tf_op jit(solution)/shard_map/ppermute | solution.py:30
  58.0 4.5 %collective-permute-start.2 = (bf16[256,512]{1,0:T(8,128)(2,1)S(1)}, bf16[256,512]{1,0:T(8,128)(2,1)S(1)}, u32[]{:S(2)}, u32[]{:S(2)}) collective-permute-start(bf16[256,512]{1,0:T(8,128)(2,1)S(1)} %bitcast.23), channel_id=1, source_target_pairs={{0,448},{16,464},{32,480},{48,496},{64,0},{80,16},{96,32},{112,48}... | collective-permute-start | bytes 786440 | tf_op jit(solution)/shard_map/ppermute | solution.py:30
  63.1 2.5 %collective-permute-done.4.wr = bf16[512,512]{1,0:T(8,128)(2,1)S(1)} collective-permute-done((bf16[512,512]{1,0:T(8,128)(2,1)S(1)}, bf16[512,512]{1,0:T(8,128)(2,1)S(1)}, u32[]{:S(2)}, u32[]{:S(2)}) %collective-permute-start.4) | collective-permute-done | bytes 524320 | tf_op jit(solution)/shard_map/ppermute | solution.py:30
  65.6 2.0 %collective-permute-done.3.wl = bf16[512,512]{1,0:T(8,128)(2,1)S(1)} collective-permute-done((bf16[512,512]{1,0:T(8,128)(2,1)S(1)}, bf16[512,512]{1,0:T(8,128)(2,1)S(1)}, u32[]{:S(2)}, u32[]{:S(2)}) %collective-permute-start.3) | collective-permute-done | bytes 524320 | tf_op jit(solution)/shard_map/ppermute | solution.py:30
  69.8 1.9 %collective-permute-start.6 = (bf16[768,128]{1,0:T(8,128)(2,1)S(1)}, bf16[768,128]{1,0:T(8,128)(2,1)S(1)}, u32[]{:S(2)}, u32[]{:S(2)}) collective-permute-start(bf16[768,128]{1,0:T(8,128)(2,1)S(1)} %get-tuple-element.17), channel_id=1, source_target_pairs={{0,14},{1,15},{2,4},{3,5},{4,2},{5,3},{6,8},{7,9},{8,6},{9,7},{10,... | collective-permute-start | bytes 589832 | tf_op jit(solution)/shard_map/ppermute | solution.py:35
  71.7 3.3 %collective-permute-start.7 = (bf16[768,128]{1,0:T(8,128)(2,1)S(1)}, bf16[768,128]{1,0:T(8,128)(2,1)S(1)}, u32[]{:S(2)}, u32[]{:S(2)}) collective-permute-start(bf16[768,128]{1,0:T(8,128)(2,1)S(1)} %get-tuple-element.18), channel_id=1, source_target_pairs={{0,4},{1,5},{2,14},{3,15},{4,8},{5,9},{6,2},{7,3},{8,12},{9,13},{1... | collective-permute-start | bytes 589832 | tf_op jit(solution)/shard_map/ppermute | solution.py:35
  75.0 4.8 %collective-permute-start.8 = (bf16[768,128]{1,0:T(8,128)(2,1)S(1)}, bf16[768,128]{1,0:T(8,128)(2,1)S(1)}, u32[]{:S(2)}, u32[]{:S(2)}) collective-permute-start(bf16[768,128]{1,0:T(8,128)(2,1)S(1)} %get-tuple-element.19), channel_id=1, source_target_pairs={{0,10},{1,11},{2,8},{3,9},{4,14},{5,15},{6,12},{7,13},{8,2},{9,3},... | collective-permute-start | bytes 589832 | tf_op jit(solution)/shard_map/ppermute | solution.py:35
  79.8 1.9 %collective-permute-start.5 = (bf16[768,128]{1,0:T(8,128)(2,1)S(1)}, bf16[768,128]{1,0:T(8,128)(2,1)S(1)}, u32[]{:S(2)}, u32[]{:S(2)}) collective-permute-start(bf16[768,128]{1,0:T(8,128)(2,1)S(1)} %get-tuple-element.16.refs_4_), channel_id=1, source_target_pairs={{0,2},{1,3},{2,0},{3,1},{4,6},{5,7},{6,4},{7,5},{8,10},{9,11},{10,... | collective-permute-start | bytes 589832 | tf_op jit(solution)/shard_map/ppermute | solution.py:35
  81.9 3.5 %collective-permute-start.9 = (bf16[1536,128]{1,0:T(8,128)(2,1)S(1)}, bf16[1536,128]{1,0:T(8,128)(2,1)S(1)}, u32[]{:S(2)}, u32[]{:S(2)}) collective-permute-start(bf16[1536,128]{1,0:T(8,128)(2,1)S(1)} %pad_maximum_fusion), channel_id=1, source_target_pairs={{0,2},{1,3},{2,0},{3,1},{4,6},{5,7},{6,4},{7,5},{8,10},{9,11},{10,... | collective-permute-start | bytes 1179656 | tf_op jit(solution)/shard_map/ppermute | solution.py:35
  85.4 6.7 %collective-permute-done.5.refs_5_ = bf16[768,128]{1,0:T(8,128)(2,1)S(1)} collective-permute-done((bf16[768,128]{1,0:T(8,128)(2,1)S(1)}, bf16[768,128]{1,0:T(8,128)(2,1)S(1)}, u32[]{:S(2)}, u32[]{:S(2)}) %collective-permute-start.5) | collective-permute-done | bytes 196640 | tf_op jit(solution)/shard_map/ppermute | solution.py:35
  92.2 5.9 %collective-permute-done.9.refs_9_ = bf16[1536,128]{1,0:T(8,128)(2,1)S(1)} collective-permute-done((bf16[1536,128]{1,0:T(8,128)(2,1)S(1)}, bf16[1536,128]{1,0:T(8,128)(2,1)S(1)}, u32[]{:S(2)}, u32[]{:S(2)}) %collective-permute-start.9) | collective-permute-done | bytes 393248 | tf_op jit(solution)/shard_map/ppermute | solution.py:35
  98.2 5.0 %collective-permute-start.11 = (bf16[5376,128]{1,0:T(8,128)(2,1)S(1)}, bf16[5376,128]{1,0:T(8,128)(2,1)S(1)}, u32[]{:S(2)}, u32[]{:S(2)}) collective-permute-start(bf16[5376,128]{1,0:T(8,128)(2,1)S(1)} %constant_dynamic-update-slice_fusion), channel_id=1, source_target_pairs={{0,1},{1,0},{2,3},{3,2},{4,5},{5,4},{6,7},{7,6},{8,9},{9,8},{10,11... | collective-permute-start | bytes 4128776 | tf_op jit(solution)/shard_map/ppermute | solution.py:41
  103.2 3.4 %collective-permute-start.10 = (bf16[768,128]{1,0:T(8,128)(2,1)S(1)}, bf16[768,128]{1,0:T(8,128)(2,1)S(1)}, u32[]{:S(2)}, u32[]{:S(2)}) collective-permute-start(bf16[768,128]{1,0:T(8,128)(2,1)S(1)} %collective-permute-done.8.refs_8_), channel_id=1, source_target_pairs={{0,2},{1,3},{2,0},{3,1},{4,6},{5,7},{6,4},{7,5},{8,10},{9,11},{10,... | collective-permute-start | bytes 589832 | tf_op jit(solution)/shard_map/ppermute | solution.py:35
  106.7 5.0 %collective-permute-done.10.refs_10_ = bf16[768,128]{1,0:T(8,128)(2,1)S(1)} collective-permute-done((bf16[768,128]{1,0:T(8,128)(2,1)S(1)}, bf16[768,128]{1,0:T(8,128)(2,1)S(1)}, u32[]{:S(2)}, u32[]{:S(2)}) %collective-permute-start.10) | collective-permute-done | bytes 196640 | tf_op jit(solution)/shard_map/ppermute | solution.py:35
  111.7 2.7 %collective-permute-start.12 = (bf16[768,128]{1,0:T(8,128)(2,1)S(1)}, bf16[768,128]{1,0:T(8,128)(2,1)S(1)}, u32[]{:S(2)}, u32[]{:S(2)}) collective-permute-start(bf16[768,128]{1,0:T(8,128)(2,1)S(1)} %collective-permute-done.10.refs_10_), channel_id=1, source_target_pairs={{0,1},{1,0},{2,3},{3,2},{4,5},{5,4},{6,7},{7,6},{8,9},{9,8},{10,11... | collective-permute-start | bytes 589832 | tf_op jit(solution)/shard_map/ppermute | solution.py:41
  115.5 3.4 %read.1 = (bf16[6144,128]{1,0:T(8,128)(2,1)}, bf16[6144,128]{1,0:T(8,128)(2,1)}, bf16[1,128]{1,0:T(2,128)(2,1)}) custom-call(bf16[1,128]{1,0:T(2,128)(2,1)S(1)} %bitcast.18, f32[1,128]{1,0:T(1,128)S(1)} %bitcast.19, f32[1,128]{1,0:T(1,128)S(1)} %bitcast.20, f32[48,128]{1,0:T(8,128)S(1)} %get-tuple-element.14.refs_3_, ...), custom_call_target="tpu_custom_call" | custom-call | tf_op jit(solution)/shard_map/read/pallas_call | solution.py:377
  (28 shorter events, 4.8 us)
Async XLA Ops:
  2.1 19.3 %all-to-all-start = ((bf16[16,32,128]{2,1,0:T(8,128)(2,1)}), bf16[16,32,128]{2,1,0:T(8,128)(2,1)S(1)}, u32[]{:S(2)}, u32[]{:S(2)}) async-start(bf16[16,32,128]{2,1,0:T(8,128)(2,1)} %pack.1), calls=%async_computation | async-start | bytes 262144 | tf_op jit(solution)/shard_map/all_to_all | solution.py:289
  15.4 47.1 %collective-permute-start = (bf16[384,2048]{1,0:T(8,128)(2,1)S(1)}, bf16[384,2048]{1,0:T(8,128)(2,1)S(1)}, u32[]{:S(2)}, u32[]{:S(2)}) collective-permute-start(bf16[384,2048]{1,0:T(8,128)(2,1)S(1)} %norm.1.own), channel_id=1, source_target_pairs={{0,1},{1,0},{2,3},{3,2},{4,5},{5,4},{6,7},{7,6},{8,9},{9,8},{10,11... | collective-permute-start | bytes 4718600 | tf_op jit(solution)/shard_map/ppermute | solution.py:41
  50.7 14.9 %collective-permute-start.4 = (bf16[512,512]{1,0:T(8,128)(2,1)S(1)}, bf16[512,512]{1,0:T(8,128)(2,1)S(1)}, u32[]{:S(2)}, u32[]{:S(2)}) collective-permute-start(bf16[512,512]{1,0:T(8,128)(2,1)S(1)} %bitcast.15), channel_id=1, source_target_pairs={{0,48},{16,0},{32,16},{48,32},{64,112},{80,64},{96,80},{112,96},{1... | collective-permute-start | bytes 1572872 | tf_op jit(solution)/shard_map/ppermute | solution.py:30
  52.6 15.0 %collective-permute-start.3 = (bf16[512,512]{1,0:T(8,128)(2,1)S(1)}, bf16[512,512]{1,0:T(8,128)(2,1)S(1)}, u32[]{:S(2)}, u32[]{:S(2)}) collective-permute-start(bf16[512,512]{1,0:T(8,128)(2,1)S(1)} %bitcast.16), channel_id=1, source_target_pairs={{0,16},{16,32},{32,48},{48,0},{64,80},{80,96},{96,112},{112,64},{1... | collective-permute-start | bytes 1572872 | tf_op jit(solution)/shard_map/ppermute | solution.py:30
  56.0 12.6 %collective-permute-start.1 = (bf16[256,512]{1,0:T(8,128)(2,1)S(1)}, bf16[256,512]{1,0:T(8,128)(2,1)S(1)}, u32[]{:S(2)}, u32[]{:S(2)}) collective-permute-start(bf16[256,512]{1,0:T(8,128)(2,1)S(1)} %bitcast.24), channel_id=1, source_target_pairs={{0,64},{16,80},{32,96},{48,112},{64,128},{80,144},{96,160},{112,17... | collective-permute-start | bytes 786440 | tf_op jit(solution)/shard_map/ppermute | solution.py:30
  58.0 10.7 %collective-permute-start.2 = (bf16[256,512]{1,0:T(8,128)(2,1)S(1)}, bf16[256,512]{1,0:T(8,128)(2,1)S(1)}, u32[]{:S(2)}, u32[]{:S(2)}) collective-permute-start(bf16[256,512]{1,0:T(8,128)(2,1)S(1)} %bitcast.23), channel_id=1, source_target_pairs={{0,448},{16,464},{32,480},{48,496},{64,0},{80,16},{96,32},{112,48}... | collective-permute-start | bytes 786440 | tf_op jit(solution)/shard_map/ppermute | solution.py:30
  63.1 5.5 %copy-start.3 = (f32[128]{0:T(128)S(1)}, f32[128]{0:T(128)}, u32[]{:S(2)}) copy-start(f32[128]{0:T(128)} %param.13) | copy-start | bytes 1540
  69.8 12.0 %collective-permute-start.6 = (bf16[768,128]{1,0:T(8,128)(2,1)S(1)}, bf16[768,128]{1,0:T(8,128)(2,1)S(1)}, u32[]{:S(2)}, u32[]{:S(2)}) collective-permute-start(bf16[768,128]{1,0:T(8,128)(2,1)S(1)} %get-tuple-element.17), channel_id=1, source_target_pairs={{0,14},{1,15},{2,4},{3,5},{4,2},{5,3},{6,8},{7,9},{8,6},{9,7},{10,... | collective-permute-start | bytes 589832 | tf_op jit(solution)/shard_map/ppermute | solution.py:35
  71.7 10.1 %collective-permute-start.7 = (bf16[768,128]{1,0:T(8,128)(2,1)S(1)}, bf16[768,128]{1,0:T(8,128)(2,1)S(1)}, u32[]{:S(2)}, u32[]{:S(2)}) collective-permute-start(bf16[768,128]{1,0:T(8,128)(2,1)S(1)} %get-tuple-element.18), channel_id=1, source_target_pairs={{0,4},{1,5},{2,14},{3,15},{4,8},{5,9},{6,2},{7,3},{8,12},{9,13},{1... | collective-permute-start | bytes 589832 | tf_op jit(solution)/shard_map/ppermute | solution.py:35
  75.0 17.2 %collective-permute-start.8 = (bf16[768,128]{1,0:T(8,128)(2,1)S(1)}, bf16[768,128]{1,0:T(8,128)(2,1)S(1)}, u32[]{:S(2)}, u32[]{:S(2)}) collective-permute-start(bf16[768,128]{1,0:T(8,128)(2,1)S(1)} %get-tuple-element.19), channel_id=1, source_target_pairs={{0,10},{1,11},{2,8},{3,9},{4,14},{5,15},{6,12},{7,13},{8,2},{9,3},... | collective-permute-start | bytes 589832 | tf_op jit(solution)/shard_map/ppermute | solution.py:35
  79.8 12.3 %collective-permute-start.5 = (bf16[768,128]{1,0:T(8,128)(2,1)S(1)}, bf16[768,128]{1,0:T(8,128)(2,1)S(1)}, u32[]{:S(2)}, u32[]{:S(2)}) collective-permute-start(bf16[768,128]{1,0:T(8,128)(2,1)S(1)} %get-tuple-element.16.refs_4_), channel_id=1, source_target_pairs={{0,2},{1,3},{2,0},{3,1},{4,6},{5,7},{6,4},{7,5},{8,10},{9,11},{10,... | collective-permute-start | bytes 589832 | tf_op jit(solution)/shard_map/ppermute | solution.py:35
  81.8 33.7 %copy-start = (bf16[1,1,128]{2,1,0:T(2,128)(2,1)S(1)}, bf16[1,1,128]{2,1,0:T(2,128)(2,1)}, u32[]{:S(2)}) copy-start(bf16[1,1,128]{2,1,0:T(2,128)(2,1)} %param.15) | copy-start | bytes 772
  81.8 33.6 %copy-start.1 = (f32[128]{0:T(128)S(1)}, f32[128]{0:T(128)}, u32[]{:S(2)}) copy-start(f32[128]{0:T(128)} %param.16) | copy-start | bytes 1540
  81.8 33.6 %copy-start.2 = (f32[128]{0:T(128)S(1)}, f32[128]{0:T(128)}, u32[]{:S(2)}) copy-start(f32[128]{0:T(128)} %param.17) | copy-start | bytes 1540
  81.9 16.3 %collective-permute-start.9 = (bf16[1536,128]{1,0:T(8,128)(2,1)S(1)}, bf16[1536,128]{1,0:T(8,128)(2,1)S(1)}, u32[]{:S(2)}, u32[]{:S(2)}) collective-permute-start(bf16[1536,128]{1,0:T(8,128)(2,1)S(1)} %pad_maximum_fusion), channel_id=1, source_target_pairs={{0,2},{1,3},{2,0},{3,1},{4,6},{5,7},{6,4},{7,5},{8,10},{9,11},{10,... | collective-permute-start | bytes 1179656 | tf_op jit(solution)/shard_map/ppermute | solution.py:35
  98.2 17.3 %collective-permute-start.11 = (bf16[5376,128]{1,0:T(8,128)(2,1)S(1)}, bf16[5376,128]{1,0:T(8,128)(2,1)S(1)}, u32[]{:S(2)}, u32[]{:S(2)}) collective-permute-start(bf16[5376,128]{1,0:T(8,128)(2,1)S(1)} %constant_dynamic-update-slice_fusion), channel_id=1, source_target_pairs={{0,1},{1,0},{2,3},{3,2},{4,5},{5,4},{6,7},{7,6},{8,9},{9,8},{10,11... | collective-permute-start | bytes 4128776 | tf_op jit(solution)/shard_map/ppermute | solution.py:41
  103.2 8.5 %collective-permute-start.10 = (bf16[768,128]{1,0:T(8,128)(2,1)S(1)}, bf16[768,128]{1,0:T(8,128)(2,1)S(1)}, u32[]{:S(2)}, u32[]{:S(2)}) collective-permute-start(bf16[768,128]{1,0:T(8,128)(2,1)S(1)} %collective-permute-done.8.refs_8_), channel_id=1, source_target_pairs={{0,2},{1,3},{2,0},{3,1},{4,6},{5,7},{6,4},{7,5},{8,10},{9,11},{10,... | collective-permute-start | bytes 589832 | tf_op jit(solution)/shard_map/ppermute | solution.py:35
  111.7 3.7 %collective-permute-start.12 = (bf16[768,128]{1,0:T(8,128)(2,1)S(1)}, bf16[768,128]{1,0:T(8,128)(2,1)S(1)}, u32[]{:S(2)}, u32[]{:S(2)}) collective-permute-start(bf16[768,128]{1,0:T(8,128)(2,1)S(1)} %collective-permute-done.10.refs_10_), channel_id=1, source_target_pairs={{0,1},{1,0},{2,3},{3,2},{4,5},{5,4},{6,7},{7,6},{8,9},{9,8},{10,11... | collective-permute-start | bytes 589832 | tf_op jit(solution)/shard_map/ppermute | solution.py:41
